TPU v7x, 1024 devices: a whole 4x4x32 slice. The times are simulated.
1024 devices in a mesh: sp: 128 (over z, y), tp: 8 (over x, core).
Axes of the slice: x: 4, y: 4, z: 32, core: 2. Of those that a mesh axis runs over, the one named last changes fastest.
Arguments:
- tokens: bfloat16 [49152, 2048], P('sp'), may hold values from -6 to 6
- norm_gain: float32 [2048], replicated, may hold values from 0.1 to 12
- w_query: bfloat16 [3, 512, 2048], P(None, 'tp'), may hold values from -0.125 to 0.125
- w_key: bfloat16 [3, 512, 2048], P(None, 'tp'), may hold values from -0.125 to 0.125
- w_value: bfloat16 [3, 512, 2048], P(None, 'tp'), may hold values from -0.125 to 0.125
- w_out: bfloat16 [512, 2048], P(None, 'tp'), may hold values from -0.25 to 0.25
Outputs:
- projected: bfloat16 [49152, 2048], P('sp', 'tp')
- log_weight: float32 [8, 49152], P('tp', 'sp')
All inputs are finite; a program needn't handle non-finite values.
Results may differ from a plain program's by a relative error of at most 0.006.
The roundings to bfloat16 on the way count: a program that leaves them out, or rounds other values in their place, can miss the bound.
Values may be sent and summed in bfloat16 or wider, within the bound.
No kernel may reach another device: no remote copies, remote signals or barrier semaphores. Data moves between devices by JAX's collectives and lax.ppermute only.
A program may use at most 32 MiB of HBM per device.

v0:
```python
import math

import jax
import jax.numpy as jnp
from jax import lax
from jax.sharding import PartitionSpec as P

HEAD_DIM = 64
SLOTS = 8
STEPS = 128
MIDDLE_DILATION = 4
WIDE_DILATION = 16


NEG_BIG = -1e30


def for_sending(value):
    return jax.tree.map(lambda a: a.astype(jnp.bfloat16) if a.dtype == jnp.float32 else a, value)


def from_behind(value, axis, by):
    devices = lax.axis_size(axis)
    pairs = [(i, i + by) for i in range(devices) if 0 <= i + by < devices]
    return lax.ppermute(value, axis, pairs)


def laid_out(pieces, dim):
    dims = list(pieces.shape[1:])
    dims[dim] *= pieces.shape[0]
    return jnp.moveaxis(pieces, 0, dim).reshape(dims)


def from_everyone(value, axis):
    devices = lax.axis_size(axis)
    return lax.all_to_all(
        jnp.broadcast_to(value[None], (devices, *value.shape)), axis, 0, 0, tiled=True
    )


def gathered_copies(value, axis, dim):
    return laid_out(from_everyone(value, axis), dim)


def attend(query, context, first_pos, dilation_step, slopes):
    head_count = slopes.shape[0]
    width = query.shape[1] // head_count
    row_count = query.shape[0]
    query_len = row_count // dilation_step
    key_len = context.shape[0] // dilation_step
    query_heads = query.reshape(query_len, dilation_step, head_count, width).transpose(1, 2, 0, 3)
    split_context = context.reshape(key_len, dilation_step, 2, head_count, width)
    key_heads = split_context[:, :, 0].transpose(1, 2, 0, 3)
    value_heads = split_context[:, :, 1].transpose(1, 2, 0, 3)
    scores = jnp.einsum(
        "rhqe,rhke->rhqk", query_heads, key_heads, preferred_element_type=jnp.float32
    ) * (1.0 / math.sqrt(width))
    query_index = jnp.arange(query_len, dtype=jnp.int32)[:, None]
    key_index = jnp.arange(key_len, dtype=jnp.int32)[None, :]
    distance = query_index + STEPS - key_index
    residue = jnp.arange(dilation_step, dtype=jnp.int32)[:, None, None, None]
    key_pos = first_pos - STEPS * dilation_step + key_index[None, None] * dilation_step + residue
    valid = (distance >= 0) & (distance <= STEPS) & (key_pos >= 0)
    logits = scores - slopes[None, :, None, None] * distance.astype(jnp.float32)
    logits = jnp.where(valid, logits, NEG_BIG)
    row_max = jnp.max(logits, axis=-1, keepdims=True)
    row_sum = jnp.sum(jnp.exp(logits - row_max), axis=-1, keepdims=True)
    log_total = row_max + jnp.log(row_sum)
    weights = jnp.exp(logits - log_total).astype(jnp.bfloat16)
    outputs = jnp.einsum(
        "rhqk,rhke->rhqe", weights, value_heads, preferred_element_type=jnp.float32
    )
    outputs = outputs.transpose(2, 0, 1, 3).reshape(row_count, head_count, width)
    log_total = log_total[..., 0].transpose(2, 0, 1).reshape(row_count, head_count)
    return (outputs, log_total)


def per_device(tokens, norm_gain, w_query, w_key, w_value, w_out):
    row_count = tokens.shape[0]
    first_pos = lax.axis_index("sp") * row_count
    slot_count = w_query.shape[1] // HEAD_DIM
    slot_ids = lax.axis_index("tp") * slot_count + jnp.arange(slot_count, dtype=jnp.int32)
    scaled = tokens.astype(jnp.float32)
    normed = (
        scaled * lax.rsqrt(jnp.mean(scaled * scaled, axis=-1, keepdims=True) + 1e-06) * norm_gain
    ).astype(jnp.bfloat16)
    query_rows = jnp.einsum(
        "td,gcd->gtc", normed, w_query, preferred_element_type=jnp.float32
    ).astype(jnp.bfloat16)
    keys = jnp.einsum("td,gcd->gtc", normed, w_key, preferred_element_type=jnp.float32).astype(
        jnp.bfloat16
    )
    value_rows = jnp.einsum(
        "td,gcd->gtc", normed, w_value, preferred_element_type=jnp.float32
    ).astype(jnp.bfloat16)
    dilation_list = (1, MIDDLE_DILATION, WIDE_DILATION)
    reaches = [
        (STEPS * dilation_step + row_count - 1) // row_count for dilation_step in dilation_list
    ]
    key_value = [
        jnp.concatenate([keys[cohort], value_rows[cohort]], axis=-1) for cohort in range(3)
    ]
    held = list(key_value)
    counts = [1, 1, 1]
    for step_bit in range(max(reaches).bit_length()):
        members = [cohort for cohort in range(3) if counts[cohort] < reaches[cohort] + 1]
        outbound_output = tuple(
            (
                held[cohort][
                    held[cohort].shape[0]
                    - min(counts[cohort], reaches[cohort] + 1 - counts[cohort]) * row_count :
                ]
                for cohort in members
            )
        )
        arrived = jax.tree.map(
            lambda part, own: part.astype(own.dtype),
            from_behind(for_sending(outbound_output), "sp", 1 << step_bit),
            outbound_output,
        )
        for position, cohort in enumerate(members):
            held[cohort] = jnp.concatenate([arrived[position], held[cohort]], axis=0)
            counts[cohort] = counts[cohort] + arrived[position].shape[0] // row_count
    contexts = [
        held[cohort][held[cohort].shape[0] - (STEPS * dilation_list[cohort] + row_count) :]
        for cohort in range(3)
    ]
    outputs_all = []
    logs_all = []
    for cohort in range(3):
        slopes = jnp.exp2(-8.0 * (cohort * SLOTS + slot_ids + 1).astype(jnp.float32) / (3 * SLOTS))
        group_out, group_log = attend(
            query_rows[cohort], contexts[cohort], first_pos, dilation_list[cohort], slopes
        )
        outputs_all.append(group_out)
        logs_all.append(group_log)
    stacked = jnp.stack(logs_all)
    log_weight = jax.nn.logsumexp(stacked, axis=0)
    shares = jnp.exp(stacked - log_weight[None])
    mixture = jnp.sum(shares[..., None] * jnp.stack(outputs_all), axis=0)
    mixture = mixture.reshape(row_count, slot_count * HEAD_DIM).astype(jnp.bfloat16)
    projected = jnp.dot(
        gathered_copies(mixture, "tp", 1), w_out, preferred_element_type=jnp.float32
    )
    return (projected.astype(jnp.bfloat16), log_weight.T)


def solution(mesh):
    in_specs = (
        P("sp", None),
        P(),
        P(None, "tp", None),
        P(None, "tp", None),
        P(None, "tp", None),
        P(None, "tp"),
    )
    out_specs = (P("sp", "tp"), P("tp", "sp"))
    return jax.shard_map(
        per_device, mesh=mesh, in_specs=in_specs, out_specs=out_specs, check_vma=False
    )
```

profile of v0, /device:TPU:392, one launch (start us, length us, event | category | flops | bytes accessed | tf_op | source)
XLA Modules:
  0.0 75.0 jit_solution(8336201353722662243)
XLA Ops:
  0.7 1.9 %fusion = f32[384]{0:T(512)S(1)} fusion(bf16[384,2048]{1,0:T(8,128)(2,1)} %param.6), kind=kLoop, calls=%fused_computation.2 | loop fusion | flops 2358912 | bytes 1574400 | tf_op jit(solution)/shard_map/reduce_sum | solution.py:85
  2.8 1.5 %fusion.12 = bf16[3,384,64]{1,2,0:T(8,128)(2,1)S(1)} fusion(bf16[3,64,2048]{2,1,0:T(8,128)(2,1)S(1)} %copy-done, bf16[384,2048]{1,0:T(8,128)(2,1)S(1)} %copy-done.3, f32[2048]{0:T(1024)} %param.7, f32[384]{0:T(512)S(1)} %add_rsqrt_fusion), kind=kOutput, calls=%fused_computation.22 | convolution fusion | flops 305209344 | bytes 2516480 | tf_op jit(solution)/shard_map/td,gcd->gtc/dot_general | solution.py:93
  4.3 0.8 %fusion.11 = bf16[3,384,64]{1,2,0:T(8,128)(2,1)S(1)} fusion(bf16[3,64,2048]{2,1,0:T(8,128)(2,1)S(1)} %copy-done.6, bf16[384,2048]{1,0:T(8,128)(2,1)S(1)} %copy-done.3, f32[2048]{0:T(1024)S(1)} %copy-done.8, f32[384]{0:T(512)S(1)} %add_rsqrt_fusion), kind=kOutput, calls=%fused_computation.21 | convolution fusion | flops 305209344 | bytes 2516480 | tf_op jit(solution)/shard_map/td,gcd->gtc/dot_general | solution.py:90
  5.8 3.5 %collective-permute-start.2 = (bf16[384,128]{0,1:T(8,128)(2,1)}, bf16[384,128]{0,1:T(8,128)(2,1)S(1)}, u32[]{:S(2)}, u32[]{:S(2)}) collective-permute-start(bf16[384,128]{0,1:T(8,128)(2,1)} %pad_maximum_fusion.10), channel_id=1, source_target_pairs={{0,8},{8,16},{16,24},{24,32},{32,40},{40,48},{48,56},{56,64},{64,7... | collective-permute-start | bytes 294920 | tf_op jit(solution)/shard_map/ppermute | solution.py:25
  9.2 4.2 %collective-permute-start.1 = (bf16[384,128]{0,1:T(8,128)(2,1)}, bf16[384,128]{0,1:T(8,128)(2,1)S(1)}, u32[]{:S(2)}, u32[]{:S(2)}) collective-permute-start(bf16[384,128]{0,1:T(8,128)(2,1)} %pad_maximum_fusion.10), channel_id=1, source_target_pairs={{0,16},{8,24},{16,32},{24,40},{32,48},{40,56},{48,64},{56,72},{64,... | collective-permute-start | bytes 294920 | tf_op jit(solution)/shard_map/ppermute | solution.py:25
  13.5 2.9 %collective-permute-start.3 = (bf16[384,128]{0,1:T(8,128)(2,1)S(1)}, bf16[384,128]{0,1:T(8,128)(2,1)S(1)}, u32[]{:S(2)}, u32[]{:S(2)}) collective-permute-start(bf16[384,128]{0,1:T(8,128)(2,1)S(1)} %pad_maximum_fusion.11), channel_id=1, source_target_pairs={{0,8},{8,16},{16,24},{24,32},{32,40},{40,48},{48,56},{56,64},{64,7... | collective-permute-start | bytes 294920 | tf_op jit(solution)/shard_map/ppermute | solution.py:25
  17.0 4.1 %collective-permute-start = (bf16[384,128]{0,1:T(8,128)(2,1)}, bf16[384,128]{0,1:T(8,128)(2,1)}, u32[]{:S(2)}, u32[]{:S(2)}) collective-permute-start(bf16[384,128]{0,1:T(8,128)(2,1)} %pad_maximum_fusion.9), channel_id=1, source_target_pairs={{0,8},{8,16},{16,24},{24,32},{32,40},{40,48},{48,56},{56,64},{64,7... | collective-permute-start | bytes 294920 | tf_op jit(solution)/shard_map/ppermute | solution.py:25
  21.3 1.9 %fusion.10 = bf16[3,384,64]{1,2,0:T(8,128)(2,1)S(1)} fusion(bf16[3,64,2048]{2,1,0:T(8,128)(2,1)} %param.8, bf16[384,2048]{1,0:T(8,128)(2,1)S(1)} %copy-done.3, f32[2048]{0:T(1024)S(1)} %copy-done.8, f32[384]{0:T(512)S(1)} %add_rsqrt_fusion), kind=kOutput, calls=%fused_computation.20 | convolution fusion | flops 305209344 | bytes 2516480 | tf_op jit(solution)/shard_map/td,gcd->gtc/dot_general | solution.py:87
  27.1 4.2 %collective-permute-start.4 = (bf16[768,128]{0,1:T(8,128)(2,1)S(1)}, bf16[768,128]{0,1:T(8,128)(2,1)S(1)}, u32[]{:S(2)}, u32[]{:S(2)}) collective-permute-start(bf16[768,128]{0,1:T(8,128)(2,1)S(1)} %maximum_maximum_fusion), channel_id=1, source_target_pairs={{0,16},{8,24},{16,32},{24,40},{32,48},{40,56},{48,64},{56,72},{64,... | collective-permute-start | bytes 589832 | tf_op jit(solution)/shard_map/ppermute | solution.py:25
  32.2 0.8 %pad_maximum_fusion.7 = bf16[512,128]{0,1:T(8,128)(2,1)S(1)} fusion(bf16[384,128]{0,1:T(8,128)(2,1)} %collective-permute-done, bf16[384,64]{0,1:T(8,128)(2,1)S(1)} %get-tuple-element.11, bf16[384,64]{0,1:T(8,128)(2,1)S(1)} %get-tuple-element.26), kind=kLoop, calls=%fused_computation.54 | loop fusion | flops 393216 | bytes 327680 | tf_op jit(solution)/shard_map/concatenate | solution.py:122
  33.0 5.2 %collective-permute-done.4 = bf16[768,128]{0,1:T(8,128)(2,1)S(1)} collective-permute-done((bf16[768,128]{0,1:T(8,128)(2,1)S(1)}, bf16[768,128]{0,1:T(8,128)(2,1)S(1)}, u32[]{:S(2)}, u32[]{:S(2)}) %collective-permute-start.4) | collective-permute-done | bytes 196640 | tf_op jit(solution)/shard_map/ppermute | solution.py:25
  38.3 2.6 %collective-permute-start.5 = (bf16[1152,128]{0,1:T(8,128)(2,1)S(1)}, bf16[1152,128]{0,1:T(8,128)(2,1)S(1)}, u32[]{:S(2)}, u32[]{:S(2)}) collective-permute-start(bf16[1152,128]{0,1:T(8,128)(2,1)S(1)} %fusion.21), channel_id=1, source_target_pairs={{0,32},{8,40},{16,48},{24,56},{32,64},{40,72},{48,80},{56,88},{64,... | collective-permute-start | bytes 884744 | tf_op jit(solution)/shard_map/ppermute | solution.py:25
  40.9 1.4 %fusion.50 = (f32[384]{0:T(512)S(1)}, f32[384,512]{1,0:T(8,128)S(1)}) fusion(f32[]{:T(128)S(6)} %exp2.25, bf16[512,1,2,1,64]{0,4,2,3,1:T(8,128)(2,1)S(1)} %bitcast.128, bf16[3,384,64]{1,2,0:T(8,128)(2,1)} %copy-done.5, pred[512]{0:T(512)(128)(4,1)S(1)} %add_compare_fusion.2, s32[384]{0:T(512)S(1)} %iota_add_fusion), kind=kOutput, calls=%fused_computation.110 | convolution fusion | flops 27328128 | bytes 905220 | tf_op jit(solution)/shard_map/rhqe,rhke->rhqk/dot_general | solution.py:55
  42.3 0.9 %copy-done.1 = f32[384,512]{1,0:T(8,128)} copy-done((f32[384,512]{1,0:T(8,128)}, f32[384,512]{1,0:T(8,128)S(1)}, u32[]{:S(2)}) %copy-start.1) | copy-done | bytes 786456
  43.5 4.6 %collective-permute-done.5 = bf16[1152,128]{0,1:T(8,128)(2,1)S(1)} collective-permute-done((bf16[1152,128]{0,1:T(8,128)(2,1)S(1)}, bf16[1152,128]{0,1:T(8,128)(2,1)S(1)}, u32[]{:S(2)}, u32[]{:S(2)}) %collective-permute-start.5) | collective-permute-done | bytes 294944 | tf_op jit(solution)/shard_map/ppermute | solution.py:25
  49.0 2.8 %fusion.45 = (bf16[152,16,1,1,64]{4,2,1,0,3:T(2,128)(2,1)}, bf16[152,16,1,1,64]{4,2,1,0,3:T(2,128)(2,1)S(1)}) fusion(bf16[152,16,2,1,64]{4,2,1,0,3:T(2,128)(2,1)S(1)} %reshape.742), kind=kLoop, calls=%fused_computation.105 | loop fusion | bytes 1245184 | tf_op jit(solution)/shard_map/slice | solution.py:53
  51.7 3.6 %copy.57 = bf16[152,16,1,1,64]{0,4,1,3,2:T(8,128)(2,1)} copy(bf16[152,16,1,1,64]{4,2,1,0,3:T(2,128)(2,1)} %get-tuple-element.4) | data formatting | bytes 622592
  55.4 1.3 %fusion.48 = (f32[16,24]{1,0:T(8,128)S(1)}, f32[16,24,152]{2,1,0:T(8,128)S(1)}) fusion(f32[24,152]{1,0:T(8,128)S(1)} %convert_multiply_fusion.3, bf16[152,16,1,1,64]{0,4,1,3,2:T(8,128)(2,1)} %copy.57, bf16[24,16,1,64]{3,1,0,2:T(8,128)(2,1)S(1)} %bitcast.126, pred[16,152]{1,0:T(8,128)(4,1)S(1)} %add_compare_fusion, pred[24,152]{1,0:T(8,128)(4,1)S(1)} %fusion.39), kind=kOutput, calls=%fused_computation.108 | convolution fusion | flops 7762560 | bytes 616128 | tf_op jit(solution)/shard_map/rhqe,rhke->rhqk/dot_general | solution.py:55
  57.2 1.2 %convolution_bitcast_fusion.2 = f32[1,384,1,64]{1,3,2,0:T(8,128)S(1)} fusion(f32[384,512]{1,0:T(8,128)S(1)} %copy-done.2, f32[384]{0:T(512)S(1)} %get-tuple-element.3, bf16[512,1,2,1,64]{0,4,2,3,1:T(8,128)(2,1)} %bitcast.129), kind=kOutput, calls=%fused_computation.24 | convolution fusion | flops 25559040 | bytes 951808 | tf_op jit(solution)/shard_map/rhqk,rhke->rhqe/dot_general | solution.py:70
  58.5 0.9 %copy.59 = bf16[152,16,1,1,64]{0,4,1,3,2:T(8,128)(2,1)S(1)} copy(bf16[152,16,1,1,64]{4,2,1,0,3:T(2,128)(2,1)S(1)} %get-tuple-element.5) | data formatting | bytes 622592
  60.0 0.8 %broadcast_in_dim.21 = bf16[8,384,64]{1,2,0:T(8,128)(2,1)} broadcast(bf16[384,64]{0,1:T(8,128)(2,1)S(1)} %fusion.22), dimensions={1,2} | broadcast | bytes 442368 | tf_op jit(solution)/shard_map/broadcast_in_dim | solution.py:37
  60.8 4.3 %all-to-all-start = ((bf16[8,384,64]{1,2,0:T(8,128)(2,1)}), bf16[8,384,64]{1,2,0:T(8,128)(2,1)S(1)}, u32[]{:S(2)}, u32[]{:S(2)}) async-start(bf16[8,384,64]{1,2,0:T(8,128)(2,1)} %broadcast_in_dim.21), calls=%async_computation | async-start | bytes 786432 | tf_op jit(solution)/shard_map/all_to_all | solution.py:36
  65.6 8.3 %all-to-all-done = bf16[8,384,64]{1,2,0:T(8,128)(2,1)S(1)} async-done(((bf16[8,384,64]{1,2,0:T(8,128)(2,1)}), bf16[8,384,64]{1,2,0:T(8,128)(2,1)S(1)}, u32[]{:S(2)}, u32[]{:S(2)}) %all-to-all-start) | async-done | bytes 393248 | tf_op jit(solution)/shard_map/all_to_all | solution.py:36
  74.0 1.0 %convolution_convert_fusion = bf16[384,256]{1,0:T(8,128)(2,1)} fusion(bf16[384,512]{0,1:T(8,128)(2,1)S(1)} %bitcast.125, bf16[512,256]{1,0:T(8,128)(2,1)S(1)} %copy-done.7), kind=kOutput, calls=%fused_computation.15 | convolution fusion | flops 100761600 | bytes 851968 | tf_op jit(solution)/shard_map/dot_general | solution.py:142
  (81 shorter events, 9.0 us)
Async XLA Ops:
  0.6 2.0 %copy-start = (bf16[3,64,2048]{2,1,0:T(8,128)(2,1)S(1)}, bf16[3,64,2048]{2,1,0:T(8,128)(2,1)}, u32[]{:S(2)}) copy-start(bf16[3,64,2048]{2,1,0:T(8,128)(2,1)} %param.10) | copy-start | bytes 2359300
  0.6 2.1 %copy-start.3 = (bf16[384,2048]{1,0:T(8,128)(2,1)S(1)}, bf16[384,2048]{1,0:T(8,128)(2,1)}, u32[]{:S(2)}) copy-start(bf16[384,2048]{1,0:T(8,128)(2,1)} %param.6) | copy-start | bytes 4718596
  2.8 1.5 %copy-start.6 = (bf16[3,64,2048]{2,1,0:T(8,128)(2,1)S(1)}, bf16[3,64,2048]{2,1,0:T(8,128)(2,1)}, u32[]{:S(2)}) copy-start(bf16[3,64,2048]{2,1,0:T(8,128)(2,1)} %param.9) | copy-start | bytes 2359300
  2.8 1.5 %copy-start.8 = (f32[2048]{0:T(1024)S(1)}, f32[2048]{0:T(1024)}, u32[]{:S(2)}) copy-start(f32[2048]{0:T(1024)} %param.7) | copy-start | bytes 24580
  5.8 18.6 %collective-permute-start.2 = (bf16[384,128]{0,1:T(8,128)(2,1)}, bf16[384,128]{0,1:T(8,128)(2,1)S(1)}, u32[]{:S(2)}, u32[]{:S(2)}) collective-permute-start(bf16[384,128]{0,1:T(8,128)(2,1)} %pad_maximum_fusion.10), channel_id=1, source_target_pairs={{0,8},{8,16},{16,24},{24,32},{32,40},{40,48},{48,56},{56,64},{64,7... | collective-permute-start | bytes 294920 | tf_op jit(solution)/shard_map/ppermute | solution.py:25
  9.2 15.2 %collective-permute-start.1 = (bf16[384,128]{0,1:T(8,128)(2,1)}, bf16[384,128]{0,1:T(8,128)(2,1)S(1)}, u32[]{:S(2)}, u32[]{:S(2)}) collective-permute-start(bf16[384,128]{0,1:T(8,128)(2,1)} %pad_maximum_fusion.10), channel_id=1, source_target_pairs={{0,16},{8,24},{16,32},{24,40},{32,48},{40,56},{48,64},{56,72},{64,... | collective-permute-start | bytes 294920 | tf_op jit(solution)/shard_map/ppermute | solution.py:25
  13.5 13.5 %collective-permute-start.3 = (bf16[384,128]{0,1:T(8,128)(2,1)S(1)}, bf16[384,128]{0,1:T(8,128)(2,1)S(1)}, u32[]{:S(2)}, u32[]{:S(2)}) collective-permute-start(bf16[384,128]{0,1:T(8,128)(2,1)S(1)} %pad_maximum_fusion.11), channel_id=1, source_target_pairs={{0,8},{8,16},{16,24},{24,32},{32,40},{40,48},{48,56},{56,64},{64,7... | collective-permute-start | bytes 294920 | tf_op jit(solution)/shard_map/ppermute | solution.py:25
  17.0 15.2 %collective-permute-start = (bf16[384,128]{0,1:T(8,128)(2,1)}, bf16[384,128]{0,1:T(8,128)(2,1)}, u32[]{:S(2)}, u32[]{:S(2)}) collective-permute-start(bf16[384,128]{0,1:T(8,128)(2,1)} %pad_maximum_fusion.9), channel_id=1, source_target_pairs={{0,8},{8,16},{16,24},{24,32},{32,40},{40,48},{48,56},{56,64},{64,7... | collective-permute-start | bytes 294920 | tf_op jit(solution)/shard_map/ppermute | solution.py:25
  23.2 0.7 copy-start.5
  27.1 11.2 %collective-permute-start.4 = (bf16[768,128]{0,1:T(8,128)(2,1)S(1)}, bf16[768,128]{0,1:T(8,128)(2,1)S(1)}, u32[]{:S(2)}, u32[]{:S(2)}) collective-permute-start(bf16[768,128]{0,1:T(8,128)(2,1)S(1)} %maximum_maximum_fusion), channel_id=1, source_target_pairs={{0,16},{8,24},{16,32},{24,40},{32,48},{40,56},{48,64},{56,72},{64,... | collective-permute-start | bytes 589832 | tf_op jit(solution)/shard_map/ppermute | solution.py:25
  33.0 15.2 %copy-start.4 = (bf16[512,128]{0,1:T(8,128)(2,1)}, bf16[512,128]{0,1:T(8,128)(2,1)S(1)}, u32[]{:S(2)}) copy-start(bf16[512,128]{0,1:T(8,128)(2,1)S(1)} %pad_maximum_fusion.7) | copy-start | bytes 393220
  38.3 9.8 %collective-permute-start.5 = (bf16[1152,128]{0,1:T(8,128)(2,1)S(1)}, bf16[1152,128]{0,1:T(8,128)(2,1)S(1)}, u32[]{:S(2)}, u32[]{:S(2)}) collective-permute-start(bf16[1152,128]{0,1:T(8,128)(2,1)S(1)} %fusion.21), channel_id=1, source_target_pairs={{0,32},{8,40},{16,48},{24,56},{32,64},{40,72},{48,80},{56,88},{64,... | collective-permute-start | bytes 884744 | tf_op jit(solution)/shard_map/ppermute | solution.py:25
  42.3 0.9 %copy-start.1 = (f32[384,512]{1,0:T(8,128)}, f32[384,512]{1,0:T(8,128)S(1)}, u32[]{:S(2)}) copy-start(f32[384,512]{1,0:T(8,128)S(1)} %get-tuple-element.23) | copy-start | bytes 2359300
  51.7 5.5 %copy-start.2 = (f32[384,512]{1,0:T(8,128)S(1)}, f32[384,512]{1,0:T(8,128)}, u32[]{:S(2)}) copy-start(f32[384,512]{1,0:T(8,128)} %copy-done.1) | copy-start | bytes 2359300
  59.4 14.6 %copy-start.7 = (bf16[512,256]{1,0:T(8,128)(2,1)S(1)}, bf16[512,256]{1,0:T(8,128)(2,1)}, u32[]{:S(2)}) copy-start(bf16[512,256]{1,0:T(8,128)(2,1)} %param.11) | copy-start | bytes 786436
  60.8 13.2 %all-to-all-start = ((bf16[8,384,64]{1,2,0:T(8,128)(2,1)}), bf16[8,384,64]{1,2,0:T(8,128)(2,1)S(1)}, u32[]{:S(2)}, u32[]{:S(2)}) async-start(bf16[8,384,64]{1,2,0:T(8,128)(2,1)} %broadcast_in_dim.21), calls=%async_computation | async-start | bytes 786432 | tf_op jit(solution)/shard_map/all_to_all | solution.py:36
where the time goes:
time: 75.7 us; the launch traced here: 75 us
  starting transfers between devices  25.7 us (34%)
  waiting for transfers between devices  18.2 us (24%)
  local copies, waits for them, and re-layouts  13.8 us (18%)
  matrix products  9.99 us (13%)
  other arithmetic  5.95 us (8%)
  between operations  1.27 us (2%)
    ppermute x6, starting transfers between devices, from_behind(): return lax.ppermute(value, axis, pairs)  21.4 us
    ppermute x6, waiting for transfers between devices, from_behind(): return lax.ppermute(value, axis, pairs)  9.87 us
    all_to_all x1, waiting for transfers between devices, from_everyone(): lax.all_to_all(jnp.broadcast_to(value[None], (devices, *value.shape)), ax...  8.34 us
    unnamed x22, local copies, waits for them, and re-layouts  6.89 us
    all_to_all x1, starting transfers between devices, from_everyone(): lax.all_to_all(jnp.broadcast_to(value[None], (devices, *value.shape)), ax...  4.29 us
    dot_general x3, matrix products, attend(): jnp.einsum('rhqe,rhke->rhqk', query_heads, key_heads, preferred_element_t...  3.05 us
    slice x1, local copies, waits for them, and re-layouts, attend(): key_heads = split_context[:, :, 0].transpose(1, 2, 0, 3)  2.76 us
    reduce_sum x1, other arithmetic, per_device(): jnp.mean(scaled * scaled, axis=-1, keepdims=True) + 1e-06  1.94 us
  transfers between devices with their start and end apart: 7, of which 3 were waited for; matrix products, arithmetic and copies ran while one was open for 13% of the time, Pallas kernels for 0%

commit v1 on v0

v1 whole, which is shorter than its diff:
```python
import jax
import jax.numpy as jnp
from jax import lax
from jax.experimental import pallas as pl
from jax.experimental.pallas import tpu as pltpu
from jax.sharding import PartitionSpec as P

HEAD_DIM = 64
SLOTS = 8
STEPS = 128
GROUPS = 3
MIDDLE_DILATION = 4
WIDE_DILATION = 16
NEG_BIG = -1e30

CLASSES = 4
NT = (((1,), (1,)), ((), ()))
NN = (((1,), (0,)), ((), ()))
TN = (((0,), (0,)), ((), ()))


def dot(a, b, dims):
    return lax.dot_general(a, b, dims, preferred_element_type=jnp.float32)


def iota(shape, dim):
    return lax.broadcasted_iota(jnp.int32, shape, dim)


def position_of_row(p, rows):
    per_class = rows // CLASSES
    per_residue = rows // WIDE_DILATION
    c = p // per_class
    rest = p - c * per_class
    j = rest // per_residue
    i = rest - j * per_residue
    return c, j, i


def project_kernel(tokens_ref, gain_ref, wq_ref, wk_ref, wv_ref, q_ref, kv0_ref, s1_ref, s2_ref, s3_ref, w_ref):
    rows, _ = tokens_ref.shape
    x = tokens_ref[...].astype(jnp.float32)
    mean = jnp.mean(x * x, axis=-1, keepdims=True)
    normed = (x * lax.rsqrt(mean + 1e-6) * gain_ref[...]).astype(jnp.bfloat16)
    for g in range(GROUPS):
        w_ref[g * 128 : g * 128 + 64, :] = wk_ref[g]
        w_ref[g * 128 + 64 : g * 128 + 128, :] = wv_ref[g]
    kv = dot(normed, w_ref[...], NT).astype(jnp.bfloat16)
    c, j, i = position_of_row(iota((rows, rows), 0), rows)
    pick = (16 * i + 4 * j + c == iota((rows, rows), 1)).astype(jnp.bfloat16)
    kv = dot(pick, kv, NN).astype(jnp.bfloat16)
    halo = STEPS // WIDE_DILATION
    per_residue = rows // WIDE_DILATION
    for g, ref, at in ((0, s1_ref, 0), (1, s2_ref, 0)):
        for r in range(WIDE_DILATION):
            lo = r * per_residue + per_residue - halo
            ref[at + r * halo : at + (r + 1) * halo, :] = kv[lo : lo + halo, g * 128 : (g + 1) * 128]
    kv0_ref[...] = kv[:, 0:128]
    s1_ref[STEPS : STEPS + rows, :] = kv[:, 128:256]
    s1_ref[STEPS + rows : STEPS + 2 * rows, :] = kv[:, 256:384]
    s2_ref[STEPS : STEPS + rows, :] = kv[:, 256:384]
    s3_ref[...] = kv[:, 256:384]
    wq = wq_ref[...].reshape(GROUPS * HEAD_DIM, -1)
    q = (dot(normed, wq, NT).astype(jnp.bfloat16) * jnp.bfloat16(0.125)).astype(jnp.bfloat16)
    q_ref[...] = dot(pick, q, NN).astype(jnp.bfloat16)


def softmax_pieces(scores):
    top = jnp.max(scores, axis=-1, keepdims=True)
    e = jnp.exp(scores - top)
    total = jnp.sum(e, axis=-1, keepdims=True)
    return (e / total).astype(jnp.bfloat16), top + jnp.log(total)


def bias_of(distance, valid, slope):
    ok = valid & (distance >= 0) & (distance <= STEPS)
    return jnp.where(ok, -slope * distance.astype(jnp.float32), NEG_BIG)


def key_rows(rows, keys, has_halo):
    del has_halo
    per_class = rows // CLASSES
    per_residue = rows // WIDE_DILATION
    halo = STEPS // WIDE_DILATION
    n = iota((per_class, keys), 1)
    full = keys // per_class
    b = n // per_class
    rest = n - b * per_class
    j = rest // per_residue
    i = rest - j * per_residue
    tail = n - full * per_class
    jt = tail // halo
    it = tail - jt * halo + per_residue - halo
    at_tail = b >= full
    return jnp.where(at_tail, jt, j), jnp.where(at_tail, it, i), b


def near_kernel(sp_ref, slope_ref, q_ref, kv0_ref, s1_ref, r1_ref, r2_ref, o0_ref, l0_ref, o1_ref, l1_ref):
    rows = kv0_ref.shape[0]
    sp = sp_ref[0]
    per_class = rows // CLASSES
    per_residue = rows // WIDE_DILATION
    halo = STEPS // WIDE_DILATION
    c, j, i = position_of_row(iota((rows, rows + STEPS), 0), rows)
    tq = 16 * i + 4 * j + c
    n = iota((rows, rows + STEPS), 1)
    c, j, i = position_of_row(n, rows)
    tail = n - rows
    r = tail // halo
    it = tail - r * halo + per_residue - halo
    t_tail = 16 * it + 4 * (r % 4) + r // 4 - rows
    is_tail = n >= rows
    tk = jnp.where(is_tail, t_tail, 16 * i + 4 * j + c)
    bias = bias_of(tq - tk, jnp.logical_or(jnp.logical_not(is_tail), sp >= 1), slope_ref[0])
    keys = jnp.concatenate([kv0_ref[...], r1_ref[0:STEPS, :]], axis=0)
    scores = dot(q_ref[:, 0:64], keys[:, 0:64], NT) + bias
    p, l = softmax_pieces(scores)
    o0_ref[...] = dot(p, keys[:, 64:128], NN)
    l0_ref[...] = l
    n_keys = 2 * per_class + STEPS // CLASSES
    q_row = iota((per_class, n_keys), 0)
    jq = q_row // per_residue
    iq = q_row - jq * per_residue
    jk, ik, b = key_rows(rows, n_keys, True)
    bias = bias_of(4 * (iq - ik) + jq - jk + per_class * b, b <= sp, slope_ref[1])
    for c in range(CLASSES):
        lo = STEPS + c * per_class
        keys = jnp.concatenate(
            [s1_ref[lo : lo + per_class, :], r1_ref[lo : lo + per_class, :], r2_ref[c * 32 : (c + 1) * 32, :]], axis=0
        )
        q = q_ref[c * per_class : (c + 1) * per_class, 64:128]
        p, l = softmax_pieces(dot(q, keys[:, 0:64], NT) + bias)
        o1_ref[c * per_class : (c + 1) * per_class, :] = dot(p, keys[:, 64:128], NN)
        l1_ref[c * per_class : (c + 1) * per_class, :] = l


def wide_kernel(sp_ref, slope_ref, q_ref, s3_ref, r1_ref, r2_ref, r3_ref, r4_ref, o0_ref, l0_ref, o1_ref, l1_ref, mix_ref, lw_ref, mixed_ref, l_ref):
    rows = s3_ref.shape[0]
    sp = sp_ref[0]
    per_class = rows // CLASSES
    per_residue = rows // WIDE_DILATION
    n_keys = 6 * per_class + STEPS // CLASSES
    q_row = iota((per_class, n_keys), 0)
    jq = q_row // per_residue
    iq = q_row - jq * per_residue
    jk, ik, b = key_rows(rows, n_keys, True)
    bias = bias_of(iq - ik + per_residue * b, (jq == jk) & (b <= sp), slope_ref[2])
    for c in range(CLASSES):
        lo = c * per_class
        run = pl.ds(lo, per_class)
        keys = jnp.concatenate(
            [
                s3_ref[run, :],
                r1_ref[pl.ds(STEPS + rows + lo, per_class), :],
                r2_ref[pl.ds(STEPS + lo, per_class), :],
                r3_ref[run, :],
                r4_ref[run, :],
                r4_ref[pl.ds(rows + lo, per_class), :],
                r4_ref[pl.ds(2 * rows + c * 32, 32), :],
            ],
            axis=0,
        )
        p, l2 = softmax_pieces(dot(q_ref[run, 128:192], keys[:, 0:64], NT) + bias)
        o2 = dot(p, keys[:, 64:128], NN)
        l0 = l0_ref[run, :]
        l1 = l1_ref[run, :]
        top = jnp.maximum(jnp.maximum(l0, l1), l2)
        lw = top + jnp.log(jnp.exp(l0 - top) + jnp.exp(l1 - top) + jnp.exp(l2 - top))
        mixed = (
            jnp.exp(l0 - lw) * o0_ref[run, :] + jnp.exp(l1 - lw) * o1_ref[run, :] + jnp.exp(l2 - lw) * o2
        )
        mixed_ref[run, :] = mixed.astype(jnp.bfloat16)
        l_ref[run, :] = lw
    c, j, i = position_of_row(iota((rows, rows), 0), rows)
    pick = 16 * i + 4 * j + c == iota((rows, rows), 1)
    mix_ref[...] = dot(mixed_ref[...], pick.astype(jnp.bfloat16), TN).astype(jnp.bfloat16)
    lw_ref[...] = jnp.sum(jnp.where(pick, l_ref[...], 0.0), axis=0, keepdims=True)


def in_vmem():
    return pl.BlockSpec(memory_space=pltpu.VMEM)


def in_smem():
    return pl.BlockSpec(memory_space=pltpu.SMEM)


def call(body, operands, outs, name, scalars=0, scratch=()):
    return pl.pallas_call(
        body,
        in_specs=[in_smem()] * scalars + [in_vmem()] * (len(operands) - scalars),
        out_specs=[in_vmem()] * len(outs),
        out_shape=[jax.ShapeDtypeStruct(s, d) for s, d in outs],
        scratch_shapes=list(scratch),
        name=name,
    )(*operands)


def from_behind(value, by):
    devices = lax.axis_size("sp")
    return lax.ppermute(value, "sp", [(i, (i + by) % devices) for i in range(devices)])


def per_device(tokens, norm_gain, w_query, w_key, w_value, w_out):
    rows = tokens.shape[0]
    bf16, f32 = jnp.bfloat16, jnp.float32
    sp = lax.axis_index("sp").reshape(1)
    slot = lax.axis_index("tp")
    slopes = jnp.exp2(-8.0 * (jnp.arange(GROUPS, dtype=jnp.int32) * SLOTS + slot + 1).astype(f32) / (GROUPS * SLOTS))
    q, kv0, s1, s2, s3 = call(
        project_kernel,
        (tokens, norm_gain.reshape(1, -1), w_query, w_key, w_value),
        [
            ((rows, GROUPS * HEAD_DIM), bf16),
            ((rows, 128), bf16),
            ((STEPS + 2 * rows, 128), bf16),
            ((STEPS + rows, 128), bf16),
            ((rows, 128), bf16),
        ],
        "project",
        scratch=[pltpu.VMEM((GROUPS * 128, tokens.shape[1]), bf16)],
    )
    r1 = from_behind(s1, 1)
    r2 = from_behind(s2, 2)
    r3 = from_behind(s3, 3)
    per_residue, halo = rows // WIDE_DILATION, STEPS // WIDE_DILATION
    second = r2[STEPS:].reshape(WIDE_DILATION, per_residue, 128)[:, per_residue - halo :].reshape(STEPS, 128)
    s4 = jnp.concatenate([s3, r1[STEPS + rows :], second], axis=0)
    r4 = from_behind(s4, 4)
    o0, l0, o1, l1 = call(
        near_kernel,
        (sp, slopes, q, kv0, s1, r1, r2),
        [((rows, HEAD_DIM), f32), ((rows, 1), f32), ((rows, HEAD_DIM), f32), ((rows, 1), f32)],
        "near",
        scalars=2,
    )
    mix, log_weight = call(
        wide_kernel,
        (sp, slopes, q, s3, r1, r2, r3, r4, o0, l0, o1, l1),
        [((HEAD_DIM, rows), bf16), ((1, rows), f32)],
        "wide",
        scalars=2,
        scratch=[pltpu.VMEM((rows, HEAD_DIM), bf16), pltpu.VMEM((rows, 1), f32)],
    )
    devices = lax.axis_size("tp")
    everyone = lax.all_to_all(jnp.broadcast_to(mix[None], (devices, *mix.shape)), "tp", 0, 0, tiled=True)
    projected = dot(everyone.reshape(devices * HEAD_DIM, rows), w_out, TN)
    return projected.astype(bf16), log_weight


def solution(mesh):
    in_specs = (P("sp", None), P(), P(None, "tp", None), P(None, "tp", None), P(None, "tp", None), P(None, "tp"))
    out_specs = (P("sp", "tp"), P("tp", "sp"))
    return jax.shard_map(per_device, mesh=mesh, in_specs=in_specs, out_specs=out_specs, check_vma=False)
```

time: 75.7 us -> 69 us (0.911)
  the two profiles are of different devices: /device:TPU:392 before, /device:TPU:8 now
where the time goes in v1:
time: 69 us; the launch traced here: 68.6 us
  waiting for transfers between devices  26.1 us (38%)
  Pallas kernels  13.7 us (20%)
  blocking collectives  13 us (19%)
  starting transfers between devices  10.9 us (16%)
  local copies, waits for them, and re-layouts  1.6 us (2%)
  other arithmetic  1.53 us (2%)
  matrix products  1 us (1%)
  between operations  0.73 us (1%)
    ppermute x4, waiting for transfers between devices, from_behind(): lax.ppermute(value, 'sp', [(i, (i + by) % devices) for i in range(devices)])  26.1 us
    pallas_call x3, Pallas kernels, call(): pl.pallas_call(body, in_specs=[in_smem()] * scalars + [in_vmem()] * (len(...  13.7 us
    all_to_all x1, blocking collectives, per_device(): lax.all_to_all(jnp.broadcast_to(mix[None], (devices, *mix.shape)), 'tp',...  13 us
    ppermute x4, starting transfers between devices, from_behind(): lax.ppermute(value, 'sp', [(i, (i + by) % devices) for i in range(devices)])  10.9 us
  transfers between devices with their start and end apart: 4, of which 2 were waited for; matrix products, arithmetic and copies ran while one was open for 1% of the time, Pallas kernels for 5%

profile of v1, /device:TPU:8, one launch (start us, length us, event | category | flops | bytes accessed | tf_op | source)
XLA Modules:
  0.0 68.6 jit_solution(13821175887291609738)
XLA Ops:
  0.6 0.0 copy-start
  0.6 5.7 %project.1 = (bf16[384,192]{1,0:T(8,128)(2,1)}, bf16[384,128]{1,0:T(8,128)(2,1)}, bf16[896,128]{1,0:T(8,128)(2,1)}, bf16[512,128]{1,0:T(8,128)(2,1)}, bf16[384,128]{1,0:T(8,128)(2,1)}) custom-call(bf16[384,2048]{1,0:T(8,128)(2,1)} %tokens_ref.1, f32[1,2048]{1,0:T(1,128)} %bitcast.10, bf16[3,64,2048]{2,1,0:T(8,128)(2,1)} %wq_ref.1, ...), custom_call_target="tpu_custom_call" | custom-call | tf_op jit(solution)/shard_map/project/pallas_call | solution.py:189
  6.3 4.2 %collective-permute-start.1 = (bf16[512,128]{1,0:T(8,128)(2,1)}, bf16[512,128]{1,0:T(8,128)(2,1)S(1)}, u32[]{:S(2)}, u32[]{:S(2)}) collective-permute-start(bf16[512,128]{1,0:T(8,128)(2,1)} %get-tuple-element.16), channel_id=1, source_target_pairs={{0,16},{8,24},{16,32},{24,40},{32,48},{40,56},{48,64},{56,72},{64,... | collective-permute-start | bytes 393224 | tf_op jit(solution)/shard_map/ppermute | solution.py:201
  10.5 2.9 %collective-permute-start = (bf16[896,128]{1,0:T(8,128)(2,1)}, bf16[896,128]{1,0:T(8,128)(2,1)S(1)}, u32[]{:S(2)}, u32[]{:S(2)}) collective-permute-start(bf16[896,128]{1,0:T(8,128)(2,1)} %get-tuple-element.15.s1_ref), channel_id=1, source_target_pairs={{0,8},{8,16},{16,24},{24,32},{32,40},{40,48},{48,56},{56,64},{64,7... | collective-permute-start | bytes 688136 | tf_op jit(solution)/shard_map/ppermute | solution.py:201
  13.4 17.9 %collective-permute-done.1.r2_ref = bf16[512,128]{1,0:T(8,128)(2,1)S(1)} collective-permute-done((bf16[512,128]{1,0:T(8,128)(2,1)}, bf16[512,128]{1,0:T(8,128)(2,1)S(1)}, u32[]{:S(2)}, u32[]{:S(2)}) %collective-permute-start.1) | collective-permute-done | bytes 131104 | tf_op jit(solution)/shard_map/ppermute | solution.py:201
  31.3 0.0 copy-start.2
  31.3 0.0 collective-permute-done.r1_ref
  31.3 0.0 copy-start.1
  31.3 1.0 %pad_maximum_fusion = bf16[896,128]{1,0:T(8,128)(2,1)S(1)} fusion(bf16[128,128]{1,0:T(8,128)(2,1)S(1)} %slice_bitcast_fusion, bf16[384,128]{1,0:T(8,128)(2,1)S(1)} %slice.12, bf16[384,128]{1,0:T(8,128)(2,1)} %get-tuple-element.14.s3_ref), kind=kLoop, calls=%fused_computation.1 | loop fusion | flops 688128 | bytes 458752 | tf_op jit(solution)/shard_map/concatenate | solution.py:228
  32.3 1.9 %collective-permute-start.3 = (bf16[896,128]{1,0:T(8,128)(2,1)S(1)}, bf16[896,128]{1,0:T(8,128)(2,1)S(1)}, u32[]{:S(2)}, u32[]{:S(2)}) collective-permute-start(bf16[896,128]{1,0:T(8,128)(2,1)S(1)} %pad_maximum_fusion), channel_id=1, source_target_pairs={{0,32},{8,40},{16,48},{24,56},{32,64},{40,72},{48,80},{56,88},{64,... | collective-permute-start | bytes 688136 | tf_op jit(solution)/shard_map/ppermute | solution.py:201
  34.3 1.9 %collective-permute-start.2 = (bf16[384,128]{1,0:T(8,128)(2,1)}, bf16[384,128]{1,0:T(8,128)(2,1)S(1)}, u32[]{:S(2)}, u32[]{:S(2)}) collective-permute-start(bf16[384,128]{1,0:T(8,128)(2,1)} %get-tuple-element.14.s3_ref), channel_id=1, source_target_pairs={{0,24},{8,32},{16,40},{24,48},{32,56},{40,64},{48,72},{56,80},{64,... | collective-permute-start | bytes 294920 | tf_op jit(solution)/shard_map/ppermute | solution.py:201
  36.2 0.5 multiply_exponential_fusion.slope_ref
  36.7 0.0 copy-done.2
  36.7 0.0 copy-done.1
  36.7 3.7 %near.1 = (f32[384,64]{1,0:T(8,128)}, f32[384,1]{1,0:T(8,128)}, f32[384,64]{1,0:T(8,128)}, f32[384,1]{1,0:T(8,128)}) custom-call(s32[1]{0:T(128)} %bitcast.sp_ref, f32[3]{0:T(128)} %multiply_exponential_fusion.slope_ref, bf16[384,192]{1,0:T(8,128)(2,1)} %get-tuple-element.13.q_ref, bf16[384,128]{1,0:T(8,128)(2,1)} %get-tuple-element.17.kv0_ref, ...), custom_call_target="tpu_custom_call" | custom-call | tf_op jit(solution)/shard_map/near/pallas_call | solution.py:189
  40.4 8.3 %collective-permute-done.2.r3_ref = bf16[384,128]{1,0:T(8,128)(2,1)S(1)} collective-permute-done((bf16[384,128]{1,0:T(8,128)(2,1)}, bf16[384,128]{1,0:T(8,128)(2,1)S(1)}, u32[]{:S(2)}, u32[]{:S(2)}) %collective-permute-start.2) | collective-permute-done | bytes 98336 | tf_op jit(solution)/shard_map/ppermute | solution.py:201
  48.7 0.0 collective-permute-done.3.r4_ref
  48.7 0.6 copy-done.4
  49.3 0.1 copy-done.3
  49.4 4.4 %wide.1 = (bf16[64,384]{1,0:T(8,128)(2,1)}, f32[1,384]{1,0:T(1,128)}) custom-call(s32[1]{0:T(128)} %bitcast.sp_ref, f32[3]{0:T(128)} %multiply_exponential_fusion.slope_ref, bf16[384,192]{1,0:T(8,128)(2,1)} %get-tuple-element.13.q_ref, bf16[384,128]{1,0:T(8,128)(2,1)} %get-tuple-element.14.s3_ref, bf16[896,128]{1,0:T(8,128)(2,1)} %copy-done.1, ...), custom_call_target="tpu_custom_call" | custom-call | tf_op jit(solution)/shard_map/wide/pallas_call | solution.py:189
  53.8 0.8 %broadcast_in_dim.2 = bf16[8,64,384]{2,1,0:T(8,128)(2,1)S(1)} broadcast(bf16[64,384]{1,0:T(8,128)(2,1)} %get-tuple-element.22), dimensions={1,2} | broadcast | bytes 442368 | tf_op jit(solution)/shard_map/broadcast_in_dim | solution.py:246
  54.6 13.0 %all_to_all.5 = bf16[8,64,384]{2,1,0:T(8,128)(2,1)S(1)} all-to-all(bf16[8,64,384]{2,1,0:T(8,128)(2,1)S(1)} %broadcast_in_dim.2), channel_id=1, replica_groups=mesh['sp'=128,'tp'=8] {'tp'}, dimensions={0} | all-to-all | bytes 786432 | tf_op jit(solution)/shard_map/all_to_all | solution.py:246
  67.6 0.0 copy-done
  67.6 1.0 %convolution_convert_fusion = bf16[384,256]{1,0:T(8,128)(2,1)} fusion(bf16[512,384]{1,0:T(8,128)(2,1)S(1)} %bitcast.8, bf16[512,256]{1,0:T(8,128)(2,1)S(1)} %copy-done), kind=kOutput, calls=%fused_computation | convolution fusion | flops 100761600 | bytes 851968 | tf_op jit(solution)/shard_map/dot_general | solution.py:23
  (5 shorter events, 0.0 us)
Async XLA Ops:
  0.6 67.0 %copy-start = (bf16[512,256]{1,0:T(8,128)(2,1)S(1)}, bf16[512,256]{1,0:T(8,128)(2,1)}, u32[]{:S(2)}) copy-start(bf16[512,256]{1,0:T(8,128)(2,1)} %param.11) | copy-start | bytes 786436
  6.3 24.9 %collective-permute-start.1 = (bf16[512,128]{1,0:T(8,128)(2,1)}, bf16[512,128]{1,0:T(8,128)(2,1)S(1)}, u32[]{:S(2)}, u32[]{:S(2)}) collective-permute-start(bf16[512,128]{1,0:T(8,128)(2,1)} %get-tuple-element.16), channel_id=1, source_target_pairs={{0,16},{8,24},{16,32},{24,40},{32,48},{40,56},{48,64},{56,72},{64,... | collective-permute-start | bytes 393224 | tf_op jit(solution)/shard_map/ppermute | solution.py:201
  10.5 20.8 %collective-permute-start = (bf16[896,128]{1,0:T(8,128)(2,1)}, bf16[896,128]{1,0:T(8,128)(2,1)S(1)}, u32[]{:S(2)}, u32[]{:S(2)}) collective-permute-start(bf16[896,128]{1,0:T(8,128)(2,1)} %get-tuple-element.15.s1_ref), channel_id=1, source_target_pairs={{0,8},{8,16},{16,24},{24,32},{32,40},{40,48},{48,56},{56,64},{64,7... | collective-permute-start | bytes 688136 | tf_op jit(solution)/shard_map/ppermute | solution.py:201
  31.3 5.5 %copy-start.2 = (bf16[512,128]{1,0:T(8,128)(2,1)}, bf16[512,128]{1,0:T(8,128)(2,1)S(1)}, u32[]{:S(2)}) copy-start(bf16[512,128]{1,0:T(8,128)(2,1)S(1)} %collective-permute-done.1.r2_ref) | copy-start | bytes 393220
  31.3 5.4 %copy-start.1 = (bf16[896,128]{1,0:T(8,128)(2,1)}, bf16[896,128]{1,0:T(8,128)(2,1)S(1)}, u32[]{:S(2)}) copy-start(bf16[896,128]{1,0:T(8,128)(2,1)S(1)} %collective-permute-done.r1_ref) | copy-start | bytes 688132
  32.3 16.3 %collective-permute-start.3 = (bf16[896,128]{1,0:T(8,128)(2,1)S(1)}, bf16[896,128]{1,0:T(8,128)(2,1)S(1)}, u32[]{:S(2)}, u32[]{:S(2)}) collective-permute-start(bf16[896,128]{1,0:T(8,128)(2,1)S(1)} %pad_maximum_fusion), channel_id=1, source_target_pairs={{0,32},{8,40},{16,48},{24,56},{32,64},{40,72},{48,80},{56,88},{64,... | collective-permute-start | bytes 688136 | tf_op jit(solution)/shard_map/ppermute | solution.py:201
  34.3 14.4 %collective-permute-start.2 = (bf16[384,128]{1,0:T(8,128)(2,1)}, bf16[384,128]{1,0:T(8,128)(2,1)S(1)}, u32[]{:S(2)}, u32[]{:S(2)}) collective-permute-start(bf16[384,128]{1,0:T(8,128)(2,1)} %get-tuple-element.14.s3_ref), channel_id=1, source_target_pairs={{0,24},{8,32},{16,40},{24,48},{32,56},{40,64},{48,72},{56,80},{64,... | collective-permute-start | bytes 294920 | tf_op jit(solution)/shard_map/ppermute | solution.py:201
  48.7 0.6 copy-start.4
  48.7 0.7 %copy-start.3 = (bf16[896,128]{1,0:T(8,128)(2,1)}, bf16[896,128]{1,0:T(8,128)(2,1)S(1)}, u32[]{:S(2)}) copy-start(bf16[896,128]{1,0:T(8,128)(2,1)S(1)} %collective-permute-done.3.r4_ref) | copy-start | bytes 688132

commit v2 on v1

v2 whole, which is shorter than its diff:
```python
import jax
import jax.numpy as jnp
from jax import lax
from jax.experimental import pallas as pl
from jax.experimental.pallas import tpu as pltpu
from jax.sharding import PartitionSpec as P


HEAD_DIM = 64
SLOTS = 8
STEPS = 128
GROUPS = 3
WIDE_DILATION = 16
NEG_BIG = -1e30

CLASSES = 4
NT = (((1,), (1,)), ((), ()))
NN = (((1,), (0,)), ((), ()))
TN = (((0,), (0,)), ((), ()))


def dot(a, b, dims):
    return lax.dot_general(a, b, dims, preferred_element_type=jnp.float32)


def iota(shape, dim):
    return lax.broadcasted_iota(jnp.int32, shape, dim)


def position_of_row(p, rows):
    per_class = rows // CLASSES
    per_residue = rows // WIDE_DILATION
    c = p // per_class
    rest = p - c * per_class
    j = rest // per_residue
    i = rest - j * per_residue
    return c, j, i


def to_class_order(rows):
    c, j, i = position_of_row(iota((rows, rows), 0), rows)
    return 16 * i + 4 * j + c == iota((rows, rows), 1)


CHUNK = 128


def project_kernel(tokens_hbm, gain_hbm, wk_hbm, wv_hbm, kv0_ref, s1_ref, s2_ref, s3_ref, normed_ref, x_ref, gain_ref, w_ref, sem):
    rows = x_ref.shape[0]
    chunks = rows // CHUNK
    gain_load = pltpu.make_async_copy(gain_hbm, gain_ref, sem.at[chunks + 2 * GROUPS])
    gain_load.start()
    loads = [
        pltpu.make_async_copy(tokens_hbm.at[pl.ds(n * CHUNK, CHUNK)], x_ref.at[pl.ds(n * CHUNK, CHUNK)], sem.at[n])
        for n in range(chunks)
    ]
    for g in range(GROUPS):
        loads.append(pltpu.make_async_copy(wk_hbm.at[g], w_ref.at[pl.ds(g * 128, 64)], sem.at[chunks + 2 * g]))
        loads.append(pltpu.make_async_copy(wv_hbm.at[g], w_ref.at[pl.ds(g * 128 + 64, 64)], sem.at[chunks + 2 * g + 1]))
    for load in loads:
        load.start()
    gain_load.wait()
    gain = gain_ref[...]
    for n in range(chunks):
        loads[n].wait()
        run = pl.ds(n * CHUNK, CHUNK)
        x = x_ref[run, :].astype(jnp.float32)
        mean = jnp.mean(x * x, axis=-1, keepdims=True)
        normed_ref[run, :] = (x * lax.rsqrt(mean + 1e-6) * gain).astype(jnp.bfloat16)
    for load in loads[chunks:]:
        load.wait()
    kv = dot(normed_ref[...], w_ref[...], NT).astype(jnp.bfloat16)
    kv = dot(to_class_order(rows).astype(jnp.bfloat16), kv, NN).astype(jnp.bfloat16)
    halo = STEPS // WIDE_DILATION
    per_residue = rows // WIDE_DILATION
    for g, ref in ((0, s1_ref), (1, s2_ref)):
        for r in range(WIDE_DILATION):
            lo = r * per_residue + per_residue - halo
            ref[r * halo : (r + 1) * halo, :] = kv[lo : lo + halo, g * 128 : (g + 1) * 128]
    kv0_ref[...] = kv[:, 0:128]
    s1_ref[STEPS : STEPS + rows, :] = kv[:, 128:256]
    s1_ref[STEPS + rows : STEPS + 2 * rows, :] = kv[:, 256:384]
    s2_ref[STEPS : STEPS + rows, :] = kv[:, 256:384]
    s3_ref[...] = kv[:, 256:384]


def query_kernel(normed_ref, wq_ref, q_ref):
    rows = normed_ref.shape[0]
    wq = wq_ref[...].reshape(GROUPS * HEAD_DIM, -1)
    q = (dot(normed_ref[...], wq, NT).astype(jnp.bfloat16) * jnp.bfloat16(0.125)).astype(jnp.bfloat16)
    q_ref[...] = dot(to_class_order(rows).astype(jnp.bfloat16), q, NN).astype(jnp.bfloat16)


def relay_kernel(s3_ref, r1_ref, r2_ref, s4_ref):
    rows = s3_ref.shape[0]
    halo = STEPS // WIDE_DILATION
    per_residue = rows // WIDE_DILATION
    s4_ref[0:rows, :] = s3_ref[...]
    s4_ref[rows : 2 * rows, :] = r1_ref[STEPS + rows : STEPS + 2 * rows, :]
    for r in range(WIDE_DILATION):
        lo = STEPS + r * per_residue + per_residue - halo
        s4_ref[2 * rows + r * halo : 2 * rows + (r + 1) * halo, :] = r2_ref[lo : lo + halo, :]


def slope_of(group, slot):
    n = jnp.full((1, 1), group * SLOTS + 1, jnp.int32) + slot
    return jnp.exp2(-8.0 * n.astype(jnp.float32) / (GROUPS * SLOTS))


def softmax_pieces(scores):
    top = jnp.max(scores, axis=-1, keepdims=True)
    e = jnp.exp(scores - top)
    total = jnp.sum(e, axis=-1, keepdims=True)
    return (e / total).astype(jnp.bfloat16), top + jnp.log(total)


def bias_of(distance, valid, slope):
    ok = valid & (distance >= 0) & (distance <= STEPS)
    return jnp.where(ok, -slope * distance.astype(jnp.float32), NEG_BIG)


def key_rows(rows, keys, has_halo):
    del has_halo
    per_class = rows // CLASSES
    per_residue = rows // WIDE_DILATION
    halo = STEPS // WIDE_DILATION
    n = iota((per_class, keys), 1)
    full = keys // per_class
    b = n // per_class
    rest = n - b * per_class
    j = rest // per_residue
    i = rest - j * per_residue
    tail = n - full * per_class
    jt = tail // halo
    it = tail - jt * halo + per_residue - halo
    at_tail = b >= full
    return jnp.where(at_tail, jt, j), jnp.where(at_tail, it, i), b


def near_kernel(sp_ref, slot_ref, q_ref, kv0_ref, s1_ref, r1_ref, r2_ref, o0_ref, l0_ref, o1_ref, l1_ref):
    rows = kv0_ref.shape[0]
    sp = sp_ref[0]
    per_class = rows // CLASSES
    per_residue = rows // WIDE_DILATION
    halo = STEPS // WIDE_DILATION
    c, j, i = position_of_row(iota((rows, rows + STEPS), 0), rows)
    tq = 16 * i + 4 * j + c
    n = iota((rows, rows + STEPS), 1)
    c, j, i = position_of_row(n, rows)
    tail = n - rows
    r = tail // halo
    it = tail - r * halo + per_residue - halo
    t_tail = 16 * it + 4 * (r % 4) + r // 4 - rows
    is_tail = n >= rows
    tk = jnp.where(is_tail, t_tail, 16 * i + 4 * j + c)
    bias = bias_of(tq - tk, jnp.logical_or(jnp.logical_not(is_tail), sp >= 1), slope_of(0, slot_ref[0]))
    keys = jnp.concatenate([kv0_ref[...], r1_ref[0:STEPS, :]], axis=0)
    scores = dot(q_ref[:, 0:64], keys[:, 0:64], NT) + bias
    p, l = softmax_pieces(scores)
    o0_ref[...] = dot(p, keys[:, 64:128], NN)
    l0_ref[...] = l
    n_keys = 2 * per_class + STEPS // CLASSES
    q_row = iota((per_class, n_keys), 0)
    jq = q_row // per_residue
    iq = q_row - jq * per_residue
    jk, ik, b = key_rows(rows, n_keys, True)
    bias = bias_of(4 * (iq - ik) + jq - jk + per_class * b, b <= sp, slope_of(1, slot_ref[0]))
    for c in range(CLASSES):
        lo = STEPS + c * per_class
        keys = jnp.concatenate(
            [s1_ref[lo : lo + per_class, :], r1_ref[lo : lo + per_class, :], r2_ref[c * 32 : (c + 1) * 32, :]], axis=0
        )
        q = q_ref[c * per_class : (c + 1) * per_class, 64:128]
        p, l = softmax_pieces(dot(q, keys[:, 0:64], NT) + bias)
        o1_ref[c * per_class : (c + 1) * per_class, :] = dot(p, keys[:, 64:128], NN)
        l1_ref[c * per_class : (c + 1) * per_class, :] = l


def wide_kernel(sp_ref, slot_ref, q_ref, s3_ref, r1_ref, r2_ref, r3_ref, r4_ref, o0_ref, l0_ref, o1_ref, l1_ref, mix_ref, lw_ref, mixed_ref, l_ref):
    rows = s3_ref.shape[0]
    sp = sp_ref[0]
    per_class = rows // CLASSES
    per_residue = rows // WIDE_DILATION
    n_keys = 6 * per_class + STEPS // CLASSES
    q_row = iota((per_class, n_keys), 0)
    jq = q_row // per_residue
    iq = q_row - jq * per_residue
    jk, ik, b = key_rows(rows, n_keys, True)
    bias = bias_of(iq - ik + per_residue * b, (jq == jk) & (b <= sp), slope_of(2, slot_ref[0]))
    for c in range(CLASSES):
        lo = c * per_class
        run = pl.ds(lo, per_class)
        keys = jnp.concatenate(
            [
                s3_ref[run, :],
                r1_ref[pl.ds(STEPS + rows + lo, per_class), :],
                r2_ref[pl.ds(STEPS + lo, per_class), :],
                r3_ref[run, :],
                r4_ref[run, :],
                r4_ref[pl.ds(rows + lo, per_class), :],
                r4_ref[pl.ds(2 * rows + c * 32, 32), :],
            ],
            axis=0,
        )
        p, l2 = softmax_pieces(dot(q_ref[run, 128:192], keys[:, 0:64], NT) + bias)
        o2 = dot(p, keys[:, 64:128], NN)
        l0 = l0_ref[run, :]
        l1 = l1_ref[run, :]
        top = jnp.maximum(jnp.maximum(l0, l1), l2)
        lw = top + jnp.log(jnp.exp(l0 - top) + jnp.exp(l1 - top) + jnp.exp(l2 - top))
        mixed = (
            jnp.exp(l0 - lw) * o0_ref[run, :] + jnp.exp(l1 - lw) * o1_ref[run, :] + jnp.exp(l2 - lw) * o2
        )
        mixed_ref[run, :] = mixed.astype(jnp.bfloat16)
        l_ref[run, :] = lw
    pick = to_class_order(rows)
    mix = dot(mixed_ref[...], pick.astype(jnp.bfloat16), TN).astype(jnp.bfloat16)
    for n in range(mix_ref.shape[0]):
        mix_ref[n] = mix
    lw_ref[...] = jnp.sum(jnp.where(pick, l_ref[...], 0.0), axis=0, keepdims=True)


VMEM = pl.BlockSpec(memory_space=pltpu.VMEM)
SMEM = pl.BlockSpec(memory_space=pltpu.SMEM)
HBM = pl.BlockSpec(memory_space=pltpu.HBM)


def call(body, operands, outs, specs=None, scratch=()):
    return pl.pallas_call(
        body,
        in_specs=specs or [VMEM] * len(operands),
        out_specs=[VMEM] * len(outs),
        out_shape=[jax.ShapeDtypeStruct(s, d) for s, d in outs],
        scratch_shapes=list(scratch),
        compiler_params=pltpu.CompilerParams(vmem_limit_bytes=20 * 2**20),
    )(*operands)


def in_hbm(value):
    return pltpu.with_memory_space_constraint(value, pltpu.HBM)


def from_behind(value, by):
    devices = lax.axis_size("sp")
    return lax.ppermute(value, "sp", [(i, i + by) for i in range(devices - by)])


def layer(tokens, norm_gain, w_query, w_key, w_value, w_out):
    rows, width = tokens.shape
    bf16, f32 = jnp.bfloat16, jnp.float32
    sp = lax.axis_index("sp").reshape(1)
    slot = lax.axis_index("tp").reshape(1)
    kv0, s1, s2, s3, normed = call(
        project_kernel,
        (in_hbm(tokens), in_hbm(norm_gain.reshape(1, -1)), in_hbm(w_key), in_hbm(w_value)),
        [
            ((rows, 128), bf16),
            ((STEPS + 2 * rows, 128), bf16),
            ((STEPS + rows, 128), bf16),
            ((rows, 128), bf16),
            ((rows, width), bf16),
        ],
        specs=[HBM] * 4,
        scratch=[
            pltpu.VMEM((rows, width), bf16),
            pltpu.VMEM((1, width), f32),
            pltpu.VMEM((GROUPS * 128, width), bf16),
            pltpu.SemaphoreType.DMA((rows // CHUNK + 2 * GROUPS + 1,)),
        ],
    )
    r2 = from_behind(s2, 2)
    r1 = from_behind(s1, 1)
    r3 = from_behind(s3, 3)
    (q,) = call(query_kernel, (normed, w_query), [((rows, GROUPS * HEAD_DIM), bf16)])
    (s4,) = call(relay_kernel, (s3, r1, r2), [((STEPS + 2 * rows, 128), bf16)])
    r4 = from_behind(s4, 4)
    o0, l0, o1, l1 = call(
        near_kernel,
        (sp, slot, q, kv0, s1, r1, r2),
        [((rows, HEAD_DIM), f32), ((rows, 1), f32), ((rows, HEAD_DIM), f32), ((rows, 1), f32)],
        specs=[SMEM] * 2 + [VMEM] * 5,
    )
    devices = lax.axis_size("tp")
    mix, log_weight = call(
        wide_kernel,
        (sp, slot, q, s3, r1, r2, r3, r4, o0, l0, o1, l1),
        [((devices, HEAD_DIM, rows), bf16), ((1, rows), f32)],
        specs=[SMEM] * 2 + [VMEM] * 10,
        scratch=[pltpu.VMEM((rows, HEAD_DIM), bf16), pltpu.VMEM((rows, 1), f32)],
    )
    everyone = lax.all_to_all(mix, "tp", 0, 0, tiled=True)
    projected = dot(everyone.reshape(devices * HEAD_DIM, rows), w_out, TN)
    return projected.astype(bf16), log_weight


def solution(mesh):
    in_specs = (P("sp", None), P(), P(None, "tp", None), P(None, "tp", None), P(None, "tp", None), P(None, "tp"))
    out_specs = (P("sp", "tp"), P("tp", "sp"))
    return jax.shard_map(layer, mesh=mesh, in_specs=in_specs, out_specs=out_specs, check_vma=False)
```

time: 69 us -> 51.3 us (0.74)
  the two profiles are of different devices: /device:TPU:8 before, /device:TPU:896 now
where the time goes in v2:
time: 51.3 us; the launch traced here: 51.1 us
  blocking collectives  13 us (25%)
  starting transfers between devices  12.8 us (25%)
  waiting for transfers between devices  12.4 us (24%)
  Pallas kernels  10.5 us (20%)
  matrix products  1 us (2%)
  between operations  0.74 us (1%)
  local copies, waits for them, and re-layouts  0.66 us (1%)
    all_to_all x1, blocking collectives, layer(): everyone = lax.all_to_all(mix, 'tp', 0, 0, tiled=True)  13 us
    ppermute x4, starting transfers between devices, from_behind(): return lax.ppermute(value, 'sp', [(i, i + by) for i in range(devices - by)])  12.8 us
    ppermute x4, waiting for transfers between devices, from_behind(): return lax.ppermute(value, 'sp', [(i, i + by) for i in range(devices - by)])  12.4 us
    pallas_call x5, Pallas kernels, call(): pl.pallas_call(body, in_specs=specs or [VMEM] * len(operands), out_specs=...  10.5 us
  transfers between devices with their start and end apart: 4, of which 2 were waited for; matrix products, arithmetic and copies ran while one was open for 0% of the time, Pallas kernels for 5%

profile of v2, /device:TPU:896, one launch (start us, length us, event | category | flops | bytes accessed | tf_op | source)
XLA Modules:
  0.0 51.1 jit_solution(16664081788117530532)
XLA Ops:
  0.6 0.0 copy-start
  0.6 0.0 copy-start.1
  0.7 3.3 %shard_map.77 = (bf16[384,128]{1,0:T(8,128)(2,1)S(1)}, bf16[896,128]{1,0:T(8,128)(2,1)S(1)}, bf16[512,128]{1,0:T(8,128)(2,1)S(1)}, bf16[384,128]{1,0:T(8,128)(2,1)S(1)}, bf16[384,2048]{1,0:T(8,128)(2,1)S(1)}) custom-call(bf16[384,2048]{1,0:T(8,128)(2,1)} %tokens_hbm.1, f32[1,2048]{1,0:T(1,128)} %bitcast.7, bf16[3,64,2048]{2,1,0:T(8,128)(2,1)} %wk_hbm.1, ...), custom_call_target="tpu_custom_call" | custom-call | tf_op jit(solution)/shard_map/pallas_call | solution.py:229
  4.0 0.0 copy-start.2
  4.0 0.6 %copy-done.2 = bf16[384,128]{1,0:T(8,128)(2,1)} copy-done((bf16[384,128]{1,0:T(8,128)(2,1)}, bf16[384,128]{1,0:T(8,128)(2,1)S(1)}, u32[]{:S(2)}) %copy-start.2) | copy-done | bytes 98328
  4.7 3.5 %collective-permute-start = (bf16[896,128]{1,0:T(8,128)(2,1)S(1)}, bf16[896,128]{1,0:T(8,128)(2,1)S(1)}, u32[]{:S(2)}, u32[]{:S(2)}) collective-permute-start(bf16[896,128]{1,0:T(8,128)(2,1)S(1)} %get-tuple-element.15.s1_ref), channel_id=1, source_target_pairs={{0,8},{8,16},{16,24},{24,32},{32,40},{40,48},{48,56},{56,64},{64,7... | collective-permute-start | bytes 688136 | tf_op jit(solution)/shard_map/ppermute | solution.py:245
  8.1 4.8 %collective-permute-start.1 = (bf16[512,128]{1,0:T(8,128)(2,1)S(1)}, bf16[512,128]{1,0:T(8,128)(2,1)S(1)}, u32[]{:S(2)}, u32[]{:S(2)}) collective-permute-start(bf16[512,128]{1,0:T(8,128)(2,1)S(1)} %get-tuple-element.16), channel_id=1, source_target_pairs={{0,16},{8,24},{16,32},{24,40},{32,48},{40,56},{48,64},{56,72},{64,... | collective-permute-start | bytes 393224 | tf_op jit(solution)/shard_map/ppermute | solution.py:245
  13.0 7.1 %collective-permute-done.1.r2_ref = bf16[512,128]{1,0:T(8,128)(2,1)S(1)} collective-permute-done((bf16[512,128]{1,0:T(8,128)(2,1)S(1)}, bf16[512,128]{1,0:T(8,128)(2,1)S(1)}, u32[]{:S(2)}, u32[]{:S(2)}) %collective-permute-start.1) | collective-permute-done | bytes 131104 | tf_op jit(solution)/shard_map/ppermute | solution.py:245
  20.0 0.0 collective-permute-done.r1_ref
  20.0 0.7 %shard_map.79 = bf16[896,128]{1,0:T(8,128)(2,1)} custom-call(bf16[384,128]{1,0:T(8,128)(2,1)S(1)} %get-tuple-element.14.s3_ref, bf16[896,128]{1,0:T(8,128)(2,1)S(1)} %collective-permute-done.r1_ref, bf16[512,128]{1,0:T(8,128)(2,1)S(1)} %collective-permute-done.1.r2_ref), custom_call_target="tpu_custom_call" | custom-call | tf_op jit(solution)/shard_map/pallas_call | solution.py:229
  20.7 1.9 %collective-permute-start.3 = (bf16[896,128]{1,0:T(8,128)(2,1)}, bf16[896,128]{1,0:T(8,128)(2,1)S(1)}, u32[]{:S(2)}, u32[]{:S(2)}) collective-permute-start(bf16[896,128]{1,0:T(8,128)(2,1)} %shard_map.79), channel_id=1, source_target_pairs={{0,32},{8,40},{16,48},{24,56},{32,64},{40,72},{48,80},{56,88},{64,... | collective-permute-start | bytes 688136 | tf_op jit(solution)/shard_map/ppermute | solution.py:245
  22.6 2.6 %collective-permute-start.2 = (bf16[384,128]{1,0:T(8,128)(2,1)S(1)}, bf16[384,128]{1,0:T(8,128)(2,1)}, u32[]{:S(2)}, u32[]{:S(2)}) collective-permute-start(bf16[384,128]{1,0:T(8,128)(2,1)S(1)} %get-tuple-element.14.s3_ref), channel_id=1, source_target_pairs={{0,24},{8,32},{16,40},{24,48},{32,56},{40,64},{48,72},{56,80},{64,... | collective-permute-start | bytes 294920 | tf_op jit(solution)/shard_map/ppermute | solution.py:245
  25.2 0.0 copy-start.3
  25.3 0.0 copy-done.1
  25.3 1.1 %shard_map.78.q_ref = bf16[384,192]{1,0:T(8,128)(2,1)S(1)} custom-call(bf16[384,2048]{1,0:T(8,128)(2,1)S(1)} %get-tuple-element.13.normed_ref, bf16[3,64,2048]{2,1,0:T(8,128)(2,1)S(1)} %copy-done.1), custom_call_target="tpu_custom_call" | custom-call | tf_op jit(solution)/shard_map/pallas_call | solution.py:229
  26.3 0.0 copy-done.3
  26.3 1.7 %shard_map.80 = (f32[384,64]{1,0:T(8,128)S(1)}, f32[384,1]{1,0:T(8,128)S(1)}, f32[384,64]{1,0:T(8,128)S(1)}, f32[384,1]{1,0:T(8,128)S(1)}) custom-call(s32[1]{0:T(128)} %bitcast.sp_ref, s32[1]{0:T(128)} %bitcast.1.slot_ref, bf16[384,192]{1,0:T(8,128)(2,1)S(1)} %shard_map.78.q_ref, bf16[384,128]{1,0:T(8,128)(2,1)S(1)} %copy-done.3, ...), custom_call_target="tpu_custom_call" | custom-call | tf_op jit(solution)/shard_map/pallas_call | solution.py:229
  28.1 5.3 %collective-permute-done.2.r3_ref = bf16[384,128]{1,0:T(8,128)(2,1)} collective-permute-done((bf16[384,128]{1,0:T(8,128)(2,1)S(1)}, bf16[384,128]{1,0:T(8,128)(2,1)}, u32[]{:S(2)}, u32[]{:S(2)}) %collective-permute-start.2) | collective-permute-done | bytes 98336 | tf_op jit(solution)/shard_map/ppermute | solution.py:245
  33.4 0.0 collective-permute-done.3.r4_ref
  33.4 3.6 %shard_map.81 = (bf16[8,64,384]{2,1,0:T(8,128)(2,1)S(1)}, f32[1,384]{1,0:T(1,128)}) custom-call(s32[1]{0:T(128)} %bitcast.sp_ref, s32[1]{0:T(128)} %bitcast.1.slot_ref, bf16[384,192]{1,0:T(8,128)(2,1)S(1)} %shard_map.78.q_ref, bf16[384,128]{1,0:T(8,128)(2,1)S(1)} %get-tuple-element.14.s3_ref, bf16[896,128]{1,0:T(8,128)(2,1)S(1)} %collective-permute-done.r1_ref, ...), custom_call_target="tpu_custom_call" | custom-call | tf_op jit(solution)/shard_map/pallas_call | solution.py:229
  37.1 13.0 %all_to_all.5 = bf16[8,64,384]{2,1,0:T(8,128)(2,1)S(1)} all-to-all(bf16[8,64,384]{2,1,0:T(8,128)(2,1)S(1)} %get-tuple-element.22), channel_id=1, replica_groups=mesh['sp'=128,'tp'=8] {'tp'}, dimensions={0} | all-to-all | bytes 786432 | tf_op jit(solution)/shard_map/all_to_all | solution.py:291
  50.1 0.0 copy-done
  50.1 1.0 %convolution_convert_fusion = bf16[384,256]{1,0:T(8,128)(2,1)} fusion(bf16[512,384]{1,0:T(8,128)(2,1)S(1)} %bitcast.6, bf16[512,256]{1,0:T(8,128)(2,1)S(1)} %copy-done), kind=kOutput, calls=%fused_computation | convolution fusion | flops 100761600 | bytes 851968 | tf_op jit(solution)/shard_map/dot_general | solution.py:23
Async XLA Ops:
  0.6 49.4 %copy-start = (bf16[512,256]{1,0:T(8,128)(2,1)S(1)}, bf16[512,256]{1,0:T(8,128)(2,1)}, u32[]{:S(2)}) copy-start(bf16[512,256]{1,0:T(8,128)(2,1)} %param.11) | copy-start | bytes 786436
  0.6 24.6 %copy-start.1 = (bf16[3,64,2048]{2,1,0:T(8,128)(2,1)S(1)}, bf16[3,64,2048]{2,1,0:T(8,128)(2,1)}, u32[]{:S(2)}) copy-start(bf16[3,64,2048]{2,1,0:T(8,128)(2,1)} %wq_ref.1) | copy-start | bytes 2359300
  4.0 0.6 %copy-start.2 = (bf16[384,128]{1,0:T(8,128)(2,1)}, bf16[384,128]{1,0:T(8,128)(2,1)S(1)}, u32[]{:S(2)}) copy-start(bf16[384,128]{1,0:T(8,128)(2,1)S(1)} %get-tuple-element.17.kv0_ref) | copy-start | bytes 294916
  4.7 15.4 %collective-permute-start = (bf16[896,128]{1,0:T(8,128)(2,1)S(1)}, bf16[896,128]{1,0:T(8,128)(2,1)S(1)}, u32[]{:S(2)}, u32[]{:S(2)}) collective-permute-start(bf16[896,128]{1,0:T(8,128)(2,1)S(1)} %get-tuple-element.15.s1_ref), channel_id=1, source_target_pairs={{0,8},{8,16},{16,24},{24,32},{32,40},{40,48},{48,56},{56,64},{64,7... | collective-permute-start | bytes 688136 | tf_op jit(solution)/shard_map/ppermute | solution.py:245
  8.1 11.9 %collective-permute-start.1 = (bf16[512,128]{1,0:T(8,128)(2,1)S(1)}, bf16[512,128]{1,0:T(8,128)(2,1)S(1)}, u32[]{:S(2)}, u32[]{:S(2)}) collective-permute-start(bf16[512,128]{1,0:T(8,128)(2,1)S(1)} %get-tuple-element.16), channel_id=1, source_target_pairs={{0,16},{8,24},{16,32},{24,40},{32,48},{40,56},{48,64},{56,72},{64,... | collective-permute-start | bytes 393224 | tf_op jit(solution)/shard_map/ppermute | solution.py:245
  20.7 12.7 %collective-permute-start.3 = (bf16[896,128]{1,0:T(8,128)(2,1)}, bf16[896,128]{1,0:T(8,128)(2,1)S(1)}, u32[]{:S(2)}, u32[]{:S(2)}) collective-permute-start(bf16[896,128]{1,0:T(8,128)(2,1)} %shard_map.79), channel_id=1, source_target_pairs={{0,32},{8,40},{16,48},{24,56},{32,64},{40,72},{48,80},{56,88},{64,... | collective-permute-start | bytes 688136 | tf_op jit(solution)/shard_map/ppermute | solution.py:245
  22.6 10.8 %collective-permute-start.2 = (bf16[384,128]{1,0:T(8,128)(2,1)S(1)}, bf16[384,128]{1,0:T(8,128)(2,1)}, u32[]{:S(2)}, u32[]{:S(2)}) collective-permute-start(bf16[384,128]{1,0:T(8,128)(2,1)S(1)} %get-tuple-element.14.s3_ref), channel_id=1, source_target_pairs={{0,24},{8,32},{16,40},{24,48},{32,56},{40,64},{48,72},{56,80},{64,... | collective-permute-start | bytes 294920 | tf_op jit(solution)/shard_map/ppermute | solution.py:245
  25.2 1.1 %copy-start.3 = (bf16[384,128]{1,0:T(8,128)(2,1)S(1)}, bf16[384,128]{1,0:T(8,128)(2,1)}, u32[]{:S(2)}) copy-start(bf16[384,128]{1,0:T(8,128)(2,1)} %copy-done.2) | copy-start | bytes 294916

commit v3 on v2

v3 whole, which is shorter than its diff:
```python
import jax
import jax.numpy as jnp
from jax import lax
from jax.experimental import pallas as pl
from jax.experimental.pallas import tpu as pltpu
from jax.sharding import PartitionSpec as P


HEAD_DIM = 64
SLOTS = 8
STEPS = 128
GROUPS = 3
WIDE_DILATION = 16
NEG_BIG = -1e30

CLASSES = 4
PAIR = 2 * HEAD_DIM
CHUNK = 128
HALO = STEPS // WIDE_DILATION
NT = (((1,), (1,)), ((), ()))
NN = (((1,), (0,)), ((), ()))
TN = (((0,), (0,)), ((), ()))


def dot(a, b, dims):
    return lax.dot_general(a, b, dims, preferred_element_type=jnp.float32)


def line(length, dim):
    return lax.broadcasted_iota(jnp.int32, (length, 1) if dim == 0 else (1, length), dim)


def split(n, size):
    q = jnp.zeros_like(n)
    for k in range(1, 32):
        q = q + (n >= k * size).astype(jnp.int32)
    return q, n - q * size


def run_of_class(per_class, dim):
    return split(line(per_class, dim), per_class // CLASSES)


def run_of_halo(rows_per_residue, dim):
    j, i = split(line(STEPS // CLASSES, dim), HALO)
    return j, i + rows_per_residue - HALO


def positions(rows, dim):
    j, i = run_of_class(rows // CLASSES, dim)
    return jnp.concatenate([16 * i + 4 * j + c for c in range(CLASSES)], axis=dim)


def to_class_order(rows):
    return positions(rows, 0) == line(rows, 1)


def halo_rows(rows):
    per_residue = rows // WIDE_DILATION
    return [r * per_residue + per_residue - HALO for r in range(WIDE_DILATION)]


def project_kernel(
    tokens_hbm, gain_hbm, wk_hbm, wv_hbm, kv0_ref, s1_ref, s3_ref, s6_ref, normed_ref, x_ref, gain_ref, w_ref, sem
):
    rows = x_ref.shape[0]
    chunks = rows // CHUNK
    gain_load = pltpu.make_async_copy(gain_hbm, gain_ref, sem.at[chunks + 2 * GROUPS])
    gain_load.start()
    loads = [
        pltpu.make_async_copy(tokens_hbm.at[pl.ds(n * CHUNK, CHUNK)], x_ref.at[pl.ds(n * CHUNK, CHUNK)], sem.at[n])
        for n in range(chunks)
    ]
    for g in range(GROUPS):
        at = chunks + 2 * g
        loads.append(pltpu.make_async_copy(wk_hbm.at[g], w_ref.at[pl.ds(g * PAIR, HEAD_DIM)], sem.at[at]))
        loads.append(
            pltpu.make_async_copy(wv_hbm.at[g], w_ref.at[pl.ds(g * PAIR + HEAD_DIM, HEAD_DIM)], sem.at[at + 1])
        )
    for load in loads:
        load.start()
    pick = to_class_order(rows).astype(jnp.bfloat16)
    gain_load.wait()
    gain = gain_ref[...]
    for n in range(chunks):
        loads[n].wait()
        run = pl.ds(n * CHUNK, CHUNK)
        x = x_ref[run, :].astype(jnp.float32)
        mean = jnp.mean(x * x, axis=-1, keepdims=True)
        normed_ref[run, :] = (x * lax.rsqrt(mean + 1e-6) * gain).astype(jnp.bfloat16)
    for load in loads[chunks:]:
        load.wait()
    kv = dot(normed_ref[...], w_ref[...], NT).astype(jnp.bfloat16)
    kv = dot(pick, kv, NN).astype(jnp.bfloat16)
    kv0_ref[...] = kv[:, 0:PAIR]
    s1_ref[STEPS : STEPS + rows, :] = kv[:, PAIR : 2 * PAIR]
    s1_ref[STEPS + rows : STEPS + 2 * rows, :] = kv[:, 2 * PAIR : 3 * PAIR]
    s3_ref[...] = kv[:, 2 * PAIR : 3 * PAIR]
    for r, lo in enumerate(halo_rows(rows)):
        s1_ref[r * HALO : (r + 1) * HALO, :] = kv[lo : lo + HALO, 0:PAIR]
        s6_ref[r * HALO : (r + 1) * HALO, :] = kv[lo : lo + HALO, 2 * PAIR : 3 * PAIR]


def query_kernel(normed_ref, wq_ref, q_ref):
    rows = normed_ref.shape[0]
    wq = wq_ref[...].reshape(GROUPS * HEAD_DIM, -1)
    q = (dot(normed_ref[...], wq, NT).astype(jnp.bfloat16) * jnp.bfloat16(0.125)).astype(jnp.bfloat16)
    q_ref[...] = dot(to_class_order(rows).astype(jnp.bfloat16), q, NN).astype(jnp.bfloat16)


def relay_kernel(s3_ref, r1_ref, s4_ref, s1b_ref):
    rows = s3_ref.shape[0]
    before = r1_ref[STEPS + rows : STEPS + 2 * rows, :]
    s4_ref[0:rows, :] = s3_ref[...]
    s4_ref[rows : 2 * rows, :] = before
    s1b_ref[STEPS : STEPS + rows, :] = before
    for r, lo in enumerate(halo_rows(rows)):
        s1b_ref[r * HALO : (r + 1) * HALO, :] = r1_ref[STEPS + lo : STEPS + lo + HALO, :]


def slope_of(group, slot):
    n = jnp.full((1, 1), group * SLOTS + 1, jnp.int32) + slot
    return jnp.exp2(-8.0 * n.astype(jnp.float32) / (GROUPS * SLOTS))


def bias_of(distance, valid, slope):
    ok = valid & (distance >= 0) & (distance <= STEPS)
    return jnp.where(ok, -slope * distance.astype(jnp.float32), NEG_BIG)


def softmax_pieces(scores):
    top = jnp.max(scores, axis=-1, keepdims=True)
    e = jnp.exp(scores - top)
    total = jnp.sum(e, axis=-1, keepdims=True)
    return (e * (1.0 / total)).astype(jnp.bfloat16), top + jnp.log(total)


def wide_bias(rows, blocks, sp, slope, halo_block=None):
    per_class, per_residue = rows // CLASSES, rows // WIDE_DILATION
    jq, iq = run_of_class(per_class, 0)
    jk, ik = run_of_class(per_class, 1)
    js, at, ok = [], [], []
    for b in blocks:
        js.append(jk)
        at.append(ik - per_residue * b)
        ok.append(jnp.full_like(jk, b) <= sp)
    if halo_block is not None:
        jh, ih = run_of_halo(per_residue, 1)
        js.append(jh)
        at.append(ih - per_residue * halo_block)
        ok.append(jnp.full_like(jh, halo_block) <= sp)
    js, at = jnp.concatenate(js, axis=1), jnp.concatenate(at, axis=1)
    ok = jnp.concatenate([o.astype(jnp.int32) for o in ok], axis=1) > 0
    return bias_of(iq - at, (jq == js) & ok, slope)


def early_kernel(sp_ref, slot_ref, q_ref, kv0_ref, s3_ref, r1_ref, r3_ref, o0_ref, l0_ref, e_ref, top_ref, sum_ref):
    rows = kv0_ref.shape[0]
    sp, slot = sp_ref[0], slot_ref[0]
    per_class, per_residue = rows // CLASSES, rows // WIDE_DILATION
    jh, ih = run_of_halo(per_residue, 1)
    tail = jnp.concatenate([16 * ih + 4 * jh + c - rows for c in range(CLASSES)], axis=1)
    tk = jnp.concatenate([positions(rows, 1), tail], axis=1)
    bias = bias_of(positions(rows, 0) - tk, (tk >= 0) | (sp >= 1), slope_of(0, slot))
    keys = jnp.concatenate([kv0_ref[...], r1_ref[0:STEPS, :]], axis=0)
    p, l = softmax_pieces(dot(q_ref[:, 0:HEAD_DIM], keys[:, 0:HEAD_DIM], NT) + bias)
    o0_ref[...] = dot(p, keys[:, HEAD_DIM:PAIR], NN)
    l0_ref[...] = l
    bias = wide_bias(rows, (0, 1, 3), sp, slope_of(2, slot))
    for c in range(CLASSES):
        lo = c * per_class
        run = pl.ds(lo, per_class)
        keys = jnp.concatenate([s3_ref[run, :], r1_ref[pl.ds(STEPS + rows + lo, per_class), :], r3_ref[run, :]], axis=0)
        scores = dot(q_ref[run, 2 * HEAD_DIM : 3 * HEAD_DIM], keys[:, 0:HEAD_DIM], NT) + bias
        top = jnp.max(scores, axis=-1, keepdims=True)
        e = jnp.exp(scores - top)
        e_ref[run, :] = e
        top_ref[run, :] = top
        sum_ref[run, :] = jnp.sum(e, axis=-1, keepdims=True)


def late_kernel(
    sp_ref, slot_ref, q_ref, s1_ref, s3_ref, r1_ref, r3_ref, r1b_ref, r4_ref, r6_ref, o0_ref, l0_ref, e_ref, top_ref,
    sum_ref, mix_ref, lw_ref, mixed_ref, l_ref,
):
    rows = s3_ref.shape[0]
    sp, slot = sp_ref[0], slot_ref[0]
    per_class, per_residue = rows // CLASSES, rows // WIDE_DILATION
    jq, iq = run_of_class(per_class, 0)
    jk, ik = run_of_class(per_class, 1)
    jh, ih = run_of_halo(per_residue, 1)
    own = 4 * ik + jk
    tk = jnp.concatenate([own, own - per_class, 4 * ih + jh - 2 * per_class], axis=1)
    near = jnp.concatenate(
        [jnp.zeros_like(own), jnp.full_like(own, 1), jnp.full_like(jh, 2)], axis=1
    )
    bias1 = bias_of(4 * iq + jq - tk, near <= sp, slope_of(1, slot))
    bias2 = wide_bias(rows, (2, 4, 5), sp, slope_of(2, slot), halo_block=6)
    halo = STEPS // CLASSES
    for c in range(CLASSES):
        lo = c * per_class
        run = pl.ds(lo, per_class)
        keys = jnp.concatenate(
            [s1_ref[pl.ds(STEPS + lo, per_class), :], r1_ref[pl.ds(STEPS + lo, per_class), :], r1b_ref[pl.ds(c * halo, halo), :]],
            axis=0,
        )
        p, l1 = softmax_pieces(dot(q_ref[run, HEAD_DIM : 2 * HEAD_DIM], keys[:, 0:HEAD_DIM], NT) + bias1)
        o1 = dot(p, keys[:, HEAD_DIM:PAIR], NN)
        keys = jnp.concatenate(
            [
                r1b_ref[pl.ds(STEPS + lo, per_class), :],
                r4_ref[run, :],
                r4_ref[pl.ds(rows + lo, per_class), :],
                r6_ref[pl.ds(c * halo, halo), :],
            ],
            axis=0,
        )
        scores = dot(q_ref[run, 2 * HEAD_DIM : 3 * HEAD_DIM], keys[:, 0:HEAD_DIM], NT) + bias2
        top0 = top_ref[run, :]
        top = jnp.maximum(top0, jnp.max(scores, axis=-1, keepdims=True))
        e = jnp.exp(scores - top)
        shrink = jnp.exp(top0 - top)
        total = sum_ref[run, :] * shrink + jnp.sum(e, axis=-1, keepdims=True)
        scale = 1.0 / total
        l2 = top + jnp.log(total)
        early = jnp.concatenate(
            [s3_ref[run, HEAD_DIM:PAIR], r1_ref[pl.ds(STEPS + rows + lo, per_class), HEAD_DIM:PAIR], r3_ref[run, HEAD_DIM:PAIR]],
            axis=0,
        )
        o2 = dot((e * scale).astype(jnp.bfloat16), keys[:, HEAD_DIM:PAIR], NN)
        o2 = o2 + dot((e_ref[run, :] * (shrink * scale)).astype(jnp.bfloat16), early, NN)
        l0 = l0_ref[run, :]
        top = jnp.maximum(jnp.maximum(l0, l1), l2)
        lw = top + jnp.log(jnp.exp(l0 - top) + jnp.exp(l1 - top) + jnp.exp(l2 - top))
        mixed = jnp.exp(l0 - lw) * o0_ref[run, :] + jnp.exp(l1 - lw) * o1 + jnp.exp(l2 - lw) * o2
        mixed_ref[run, :] = mixed.astype(jnp.bfloat16)
        l_ref[run, :] = lw
    pick = to_class_order(rows)
    mix = dot(mixed_ref[...], pick.astype(jnp.bfloat16), TN).astype(jnp.bfloat16)
    for n in range(mix_ref.shape[0]):
        mix_ref[n] = mix
    lw_ref[...] = jnp.sum(jnp.where(pick, l_ref[...], 0.0), axis=0, keepdims=True)


VMEM = pl.BlockSpec(memory_space=pltpu.VMEM)
SMEM = pl.BlockSpec(memory_space=pltpu.SMEM)
HBM = pl.BlockSpec(memory_space=pltpu.HBM)


def call(body, operands, outs, specs=None, scratch=()):
    return pl.pallas_call(
        body,
        in_specs=specs or [VMEM] * len(operands),
        out_specs=[VMEM] * len(outs),
        out_shape=[jax.ShapeDtypeStruct(s, d) for s, d in outs],
        scratch_shapes=list(scratch),
        compiler_params=pltpu.CompilerParams(vmem_limit_bytes=20 * 2**20),
    )(*operands)


def in_hbm(value):
    return pltpu.with_memory_space_constraint(value, pltpu.HBM)


def from_behind(value, by):
    devices = lax.axis_size("sp")
    return lax.ppermute(value, "sp", [(i, i + by) for i in range(devices - by)])


def layer(tokens, norm_gain, w_query, w_key, w_value, w_out):
    rows, width = tokens.shape
    bf16, f32 = jnp.bfloat16, jnp.float32
    sp = lax.axis_index("sp").reshape(1)
    slot = lax.axis_index("tp").reshape(1)
    kv0, s1, s3, s6, normed = call(
        project_kernel,
        (in_hbm(tokens), in_hbm(norm_gain.reshape(1, -1)), in_hbm(w_key), in_hbm(w_value)),
        [
            ((rows, PAIR), bf16),
            ((STEPS + 2 * rows, PAIR), bf16),
            ((rows, PAIR), bf16),
            ((STEPS, PAIR), bf16),
            ((rows, width), bf16),
        ],
        specs=[HBM] * 4,
        scratch=[
            pltpu.VMEM((rows, width), bf16),
            pltpu.VMEM((1, width), f32),
            pltpu.VMEM((GROUPS * PAIR, width), bf16),
            pltpu.SemaphoreType.DMA((rows // CHUNK + 2 * GROUPS + 1,)),
        ],
    )
    r1 = from_behind(s1, 1)
    r3 = from_behind(s3, 3)
    r6 = from_behind(s6, 6)
    (q,) = call(query_kernel, (normed, w_query), [((rows, GROUPS * HEAD_DIM), bf16)])
    s4, s1b = call(relay_kernel, (s3, r1), [((2 * rows, PAIR), bf16), ((STEPS + rows, PAIR), bf16)])
    r4 = from_behind(s4, 4)
    r1b = from_behind(s1b, 1)
    o0, l0, e, top, total = call(
        early_kernel,
        (sp, slot, q, kv0, s3, r1, r3),
        [
            ((rows, HEAD_DIM), f32),
            ((rows, 1), f32),
            ((rows, 3 * rows // CLASSES), f32),
            ((rows, 1), f32),
            ((rows, 1), f32),
        ],
        specs=[SMEM] * 2 + [VMEM] * 5,
    )
    devices = lax.axis_size("tp")
    mix, log_weight = call(
        late_kernel,
        (sp, slot, q, s1, s3, r1, r3, r1b, r4, r6, o0, l0, e, top, total),
        [((devices, HEAD_DIM, rows), bf16), ((1, rows), f32)],
        specs=[SMEM] * 2 + [VMEM] * 13,
        scratch=[pltpu.VMEM((rows, HEAD_DIM), bf16), pltpu.VMEM((rows, 1), f32)],
    )
    everyone = lax.all_to_all(mix, "tp", 0, 0, tiled=True)
    projected = dot(everyone.reshape(devices * HEAD_DIM, rows), w_out, TN)
    return projected.astype(bf16), log_weight


def solution(mesh):
    in_specs = (P("sp", None), P(), P(None, "tp", None), P(None, "tp", None), P(None, "tp", None), P(None, "tp"))
    out_specs = (P("sp", "tp"), P("tp", "sp"))
    return jax.shard_map(layer, mesh=mesh, in_specs=in_specs, out_specs=out_specs, check_vma=False)
```

time: 51.3 us -> 59.5 us (1.16)
  the two profiles are of different devices: /device:TPU:896 before, /device:TPU:64 now
where the time goes in v3:
time: 59.5 us; the launch traced here: 59.3 us
  starting transfers between devices  20 us (34%)
  blocking collectives  13 us (22%)
  waiting for transfers between devices  12.3 us (21%)
  Pallas kernels  12.1 us (20%)
  matrix products  1 us (2%)
  between operations  0.76 us (1%)
    ppermute x5, starting transfers between devices, from_behind(): return lax.ppermute(value, 'sp', [(i, i + by) for i in range(devices - by)])  20 us
    all_to_all x1, blocking collectives, layer(): everyone = lax.all_to_all(mix, 'tp', 0, 0, tiled=True)  13 us
    ppermute x5, waiting for transfers between devices, from_behind(): return lax.ppermute(value, 'sp', [(i, i + by) for i in range(devices - by)])  12.3 us
    pallas_call x5, Pallas kernels, call(): pl.pallas_call(body, in_specs=specs or [VMEM] * len(operands), out_specs=...  12.1 us
  transfers between devices with their start and end apart: 5, of which 2 were waited for; matrix products, arithmetic and copies ran while one was open for 0% of the time, Pallas kernels for 4%

profile of v3, /device:TPU:64, one launch (start us, length us, event | category | flops | bytes accessed | tf_op | source)
XLA Modules:
  0.0 59.3 jit_solution(18151775553923570453)
XLA Ops:
  0.6 0.0 copy-start
  0.6 0.0 copy-start.1
  0.7 3.3 %shard_map.77 = (bf16[384,128]{1,0:T(8,128)(2,1)S(1)}, bf16[896,128]{1,0:T(8,128)(2,1)S(1)}, bf16[384,128]{1,0:T(8,128)(2,1)S(1)}, bf16[128,128]{1,0:T(8,128)(2,1)S(1)}, bf16[384,2048]{1,0:T(8,128)(2,1)S(1)}) custom-call(bf16[384,2048]{1,0:T(8,128)(2,1)} %tokens_hbm.1, f32[1,2048]{1,0:T(1,128)} %bitcast.7, bf16[3,64,2048]{2,1,0:T(8,128)(2,1)} %wk_hbm.1, ...), custom_call_target="tpu_custom_call" | custom-call | tf_op jit(solution)/shard_map/pallas_call | solution.py:251
  4.0 0.0 copy-start.2
  4.0 3.5 %collective-permute-start = (bf16[896,128]{1,0:T(8,128)(2,1)S(1)}, bf16[896,128]{1,0:T(8,128)(2,1)S(1)}, u32[]{:S(2)}, u32[]{:S(2)}) collective-permute-start(bf16[896,128]{1,0:T(8,128)(2,1)S(1)} %get-tuple-element.17.s1_ref), channel_id=1, source_target_pairs={{0,8},{8,16},{16,24},{24,32},{32,40},{40,48},{48,56},{56,64},{64,7... | collective-permute-start | bytes 688136 | tf_op jit(solution)/shard_map/ppermute | solution.py:267
  7.5 7.9 %collective-permute-done.r1_ref = bf16[896,128]{1,0:T(8,128)(2,1)S(1)} collective-permute-done((bf16[896,128]{1,0:T(8,128)(2,1)S(1)}, bf16[896,128]{1,0:T(8,128)(2,1)S(1)}, u32[]{:S(2)}, u32[]{:S(2)}) %collective-permute-start) | collective-permute-done | bytes 229408 | tf_op jit(solution)/shard_map/ppermute | solution.py:267
  15.3 0.8 %shard_map.79 = (bf16[768,128]{1,0:T(8,128)(2,1)}, bf16[512,128]{1,0:T(8,128)(2,1)}) custom-call(bf16[384,128]{1,0:T(8,128)(2,1)S(1)} %get-tuple-element.18.s3_ref, bf16[896,128]{1,0:T(8,128)(2,1)S(1)} %collective-permute-done.r1_ref), custom_call_target="tpu_custom_call" | custom-call | tf_op jit(solution)/shard_map/pallas_call | solution.py:251
  16.1 3.8 %collective-permute-start.3 = (bf16[768,128]{1,0:T(8,128)(2,1)}, bf16[768,128]{1,0:T(8,128)(2,1)S(1)}, u32[]{:S(2)}, u32[]{:S(2)}) collective-permute-start(bf16[768,128]{1,0:T(8,128)(2,1)} %get-tuple-element.20), channel_id=1, source_target_pairs={{0,32},{8,40},{16,48},{24,56},{32,64},{40,72},{48,80},{56,88},{64,... | collective-permute-start | bytes 589832 | tf_op jit(solution)/shard_map/ppermute | solution.py:267
  19.9 0.0 copy-done.2
  19.9 1.9 %collective-permute-start.2 = (bf16[512,128]{1,0:T(8,128)(2,1)}, bf16[512,128]{1,0:T(8,128)(2,1)}, u32[]{:S(2)}, u32[]{:S(2)}) collective-permute-start(bf16[512,128]{1,0:T(8,128)(2,1)} %get-tuple-element.19), channel_id=1, source_target_pairs={{0,8},{8,16},{16,24},{24,32},{32,40},{40,48},{48,56},{56,64},{64,7... | collective-permute-start | bytes 393224 | tf_op jit(solution)/shard_map/ppermute | solution.py:267
  21.8 8.9 %collective-permute-start.1 = (bf16[384,128]{1,0:T(8,128)(2,1)S(1)}, bf16[384,128]{1,0:T(8,128)(2,1)S(1)}, u32[]{:S(2)}, u32[]{:S(2)}) collective-permute-start(bf16[384,128]{1,0:T(8,128)(2,1)S(1)} %get-tuple-element.18.s3_ref), channel_id=1, source_target_pairs={{0,24},{8,32},{16,40},{24,48},{32,56},{40,64},{48,72},{56,80},{64,... | collective-permute-start | bytes 294920 | tf_op jit(solution)/shard_map/ppermute | solution.py:267
  30.8 1.9 %collective-permute-start.4 = (bf16[128,128]{1,0:T(8,128)(2,1)S(1)}, bf16[128,128]{1,0:T(8,128)(2,1)S(1)}, u32[]{:S(2)}, u32[]{:S(2)}) collective-permute-start(bf16[128,128]{1,0:T(8,128)(2,1)S(1)} %get-tuple-element.21), channel_id=1, source_target_pairs={{0,48},{8,56},{16,64},{24,72},{32,80},{40,88},{48,96},{56,104},{64... | collective-permute-start | bytes 98312 | tf_op jit(solution)/shard_map/ppermute | solution.py:267
  32.7 0.0 copy-start.3
  32.7 0.0 copy-done.1
  32.7 1.0 %shard_map.78.q_ref = bf16[384,192]{1,0:T(8,128)(2,1)S(1)} custom-call(bf16[384,2048]{1,0:T(8,128)(2,1)S(1)} %get-tuple-element.16.normed_ref, bf16[3,64,2048]{2,1,0:T(8,128)(2,1)S(1)} %copy-done.1), custom_call_target="tpu_custom_call" | custom-call | tf_op jit(solution)/shard_map/pallas_call | solution.py:251
  33.7 0.0 collective-permute-done.1.r3_ref
  33.7 1.7 %shard_map.80 = (f32[384,64]{1,0:T(8,128)S(1)}, f32[384,1]{1,0:T(8,128)S(1)}, f32[384,288]{1,0:T(8,128)S(1)}, f32[384,1]{1,0:T(8,128)S(1)}, f32[384,1]{1,0:T(8,128)S(1)}) custom-call(s32[1]{0:T(128)} %bitcast.sp_ref, s32[1]{0:T(128)} %bitcast.1.slot_ref, bf16[384,192]{1,0:T(8,128)(2,1)S(1)} %shard_map.78.q_ref, bf16[384,128]{1,0:T(8,128)(2,1)S(1)} %copy-done.3, ...), custom_call_target="tpu_custom_call" | custom-call | tf_op jit(solution)/shard_map/pallas_call | solution.py:251
  35.4 4.5 %collective-permute-done.4.r6_ref = bf16[128,128]{1,0:T(8,128)(2,1)S(1)} collective-permute-done((bf16[128,128]{1,0:T(8,128)(2,1)S(1)}, bf16[128,128]{1,0:T(8,128)(2,1)S(1)}, u32[]{:S(2)}, u32[]{:S(2)}) %collective-permute-start.4) | collective-permute-done | bytes 32800 | tf_op jit(solution)/shard_map/ppermute | solution.py:267
  39.9 0.0 collective-permute-done.2.r1b_ref
  39.9 0.0 collective-permute-done.3.r4_ref
  39.9 5.4 %shard_map.81 = (bf16[8,64,384]{2,1,0:T(8,128)(2,1)S(1)}, f32[1,384]{1,0:T(1,128)}) custom-call(s32[1]{0:T(128)} %bitcast.sp_ref, s32[1]{0:T(128)} %bitcast.1.slot_ref, bf16[384,192]{1,0:T(8,128)(2,1)S(1)} %shard_map.78.q_ref, bf16[896,128]{1,0:T(8,128)(2,1)S(1)} %get-tuple-element.17.s1_ref, bf16[384,128]{1,0:T(8,128)(2,1)S(1)} %get-tuple-element.18.s3_ref, ...), custom_call_target="tpu_custom_call" | custom-call | tf_op jit(solution)/shard_map/pallas_call | solution.py:251
  45.3 13.0 %all_to_all.5 = bf16[8,64,384]{2,1,0:T(8,128)(2,1)S(1)} all-to-all(bf16[8,64,384]{2,1,0:T(8,128)(2,1)S(1)} %get-tuple-element.28), channel_id=1, replica_groups=mesh['sp'=128,'tp'=8] {'tp'}, dimensions={0} | all-to-all | bytes 786432 | tf_op jit(solution)/shard_map/all_to_all | solution.py:320
  58.3 0.0 copy-done
  58.3 1.0 %convolution_convert_fusion = bf16[384,256]{1,0:T(8,128)(2,1)} fusion(bf16[512,384]{1,0:T(8,128)(2,1)S(1)} %bitcast.6, bf16[512,256]{1,0:T(8,128)(2,1)S(1)} %copy-done), kind=kOutput, calls=%fused_computation | convolution fusion | flops 100761600 | bytes 851968 | tf_op jit(solution)/shard_map/dot_general | solution.py:26
  (1 shorter events, 0.0 us)
Async XLA Ops:
  0.6 57.6 %copy-start = (bf16[512,256]{1,0:T(8,128)(2,1)S(1)}, bf16[512,256]{1,0:T(8,128)(2,1)}, u32[]{:S(2)}) copy-start(bf16[512,256]{1,0:T(8,128)(2,1)} %param.11) | copy-start | bytes 786436
  0.6 32.1 %copy-start.1 = (bf16[3,64,2048]{2,1,0:T(8,128)(2,1)S(1)}, bf16[3,64,2048]{2,1,0:T(8,128)(2,1)}, u32[]{:S(2)}) copy-start(bf16[3,64,2048]{2,1,0:T(8,128)(2,1)} %wq_ref.1) | copy-start | bytes 2359300
  4.0 15.9 %copy-start.2 = (bf16[384,128]{1,0:T(8,128)(2,1)}, bf16[384,128]{1,0:T(8,128)(2,1)S(1)}, u32[]{:S(2)}) copy-start(bf16[384,128]{1,0:T(8,128)(2,1)S(1)} %get-tuple-element.22.kv0_ref) | copy-start | bytes 294916
  4.0 11.3 %collective-permute-start = (bf16[896,128]{1,0:T(8,128)(2,1)S(1)}, bf16[896,128]{1,0:T(8,128)(2,1)S(1)}, u32[]{:S(2)}, u32[]{:S(2)}) collective-permute-start(bf16[896,128]{1,0:T(8,128)(2,1)S(1)} %get-tuple-element.17.s1_ref), channel_id=1, source_target_pairs={{0,8},{8,16},{16,24},{24,32},{32,40},{40,48},{48,56},{56,64},{64,7... | collective-permute-start | bytes 688136 | tf_op jit(solution)/shard_map/ppermute | solution.py:267
  16.1 23.8 %collective-permute-start.3 = (bf16[768,128]{1,0:T(8,128)(2,1)}, bf16[768,128]{1,0:T(8,128)(2,1)S(1)}, u32[]{:S(2)}, u32[]{:S(2)}) collective-permute-start(bf16[768,128]{1,0:T(8,128)(2,1)} %get-tuple-element.20), channel_id=1, source_target_pairs={{0,32},{8,40},{16,48},{24,56},{32,64},{40,72},{48,80},{56,88},{64,... | collective-permute-start | bytes 589832 | tf_op jit(solution)/shard_map/ppermute | solution.py:267
  19.9 20.0 %collective-permute-start.2 = (bf16[512,128]{1,0:T(8,128)(2,1)}, bf16[512,128]{1,0:T(8,128)(2,1)}, u32[]{:S(2)}, u32[]{:S(2)}) collective-permute-start(bf16[512,128]{1,0:T(8,128)(2,1)} %get-tuple-element.19), channel_id=1, source_target_pairs={{0,8},{8,16},{16,24},{24,32},{32,40},{40,48},{48,56},{56,64},{64,7... | collective-permute-start | bytes 393224 | tf_op jit(solution)/shard_map/ppermute | solution.py:267
  21.8 11.9 %collective-permute-start.1 = (bf16[384,128]{1,0:T(8,128)(2,1)S(1)}, bf16[384,128]{1,0:T(8,128)(2,1)S(1)}, u32[]{:S(2)}, u32[]{:S(2)}) collective-permute-start(bf16[384,128]{1,0:T(8,128)(2,1)S(1)} %get-tuple-element.18.s3_ref), channel_id=1, source_target_pairs={{0,24},{8,32},{16,40},{24,48},{32,56},{40,64},{48,72},{56,80},{64,... | collective-permute-start | bytes 294920 | tf_op jit(solution)/shard_map/ppermute | solution.py:267
  30.8 9.1 %collective-permute-start.4 = (bf16[128,128]{1,0:T(8,128)(2,1)S(1)}, bf16[128,128]{1,0:T(8,128)(2,1)S(1)}, u32[]{:S(2)}, u32[]{:S(2)}) collective-permute-start(bf16[128,128]{1,0:T(8,128)(2,1)S(1)} %get-tuple-element.21), channel_id=1, source_target_pairs={{0,48},{8,56},{16,64},{24,72},{32,80},{40,88},{48,96},{56,104},{64... | collective-permute-start | bytes 98312 | tf_op jit(solution)/shard_map/ppermute | solution.py:267
  32.7 1.0 %copy-start.3 = (bf16[384,128]{1,0:T(8,128)(2,1)S(1)}, bf16[384,128]{1,0:T(8,128)(2,1)}, u32[]{:S(2)}) copy-start(bf16[384,128]{1,0:T(8,128)(2,1)} %copy-done.2) | copy-start | bytes 294916

commit v4 on v3

v4 whole, which is shorter than its diff:
```python
import jax
import jax.numpy as jnp
from jax import lax
from jax.experimental import pallas as pl
from jax.experimental.pallas import tpu as pltpu
from jax.sharding import PartitionSpec as P


HEAD_DIM = 64
SLOTS = 8
STEPS = 128
GROUPS = 3
WIDE_DILATION = 16
NEG_BIG = -1e30

CLASSES = 4
PAIR = 2 * HEAD_DIM
CHUNK = 128
HALO = STEPS // WIDE_DILATION
NT = (((1,), (1,)), ((), ()))
NN = (((1,), (0,)), ((), ()))
TN = (((0,), (0,)), ((), ()))


def dot(a, b, dims):
    return lax.dot_general(a, b, dims, preferred_element_type=jnp.float32)


def line(length, dim):
    return lax.broadcasted_iota(jnp.int32, (length, 1) if dim == 0 else (1, length), dim)


def split(n, size):
    q = jnp.zeros_like(n)
    for k in range(1, 32):
        q = q + (n >= k * size).astype(jnp.int32)
    return q, n - q * size


def run_of_class(per_class, dim):
    return split(line(per_class, dim), per_class // CLASSES)


def run_of_halo(rows_per_residue, dim):
    j, i = split(line(STEPS // CLASSES, dim), HALO)
    return j, i + rows_per_residue - HALO


def positions(rows, dim):
    j, i = run_of_class(rows // CLASSES, dim)
    return jnp.concatenate([16 * i + 4 * j + c for c in range(CLASSES)], axis=dim)


def to_class_order(rows):
    return positions(rows, 0) == line(rows, 1)


def halo_rows(rows):
    per_residue = rows // WIDE_DILATION
    return [r * per_residue + per_residue - HALO for r in range(WIDE_DILATION)]


def project_kernel(
    tokens_hbm, gain_hbm, wk_hbm, wv_hbm, kv0_ref, s1_ref, s2_ref, s3_ref, normed_ref, x_ref, gain_ref, w_ref, sem
):
    rows = x_ref.shape[0]
    chunks = rows // CHUNK
    gain_load = pltpu.make_async_copy(gain_hbm, gain_ref, sem.at[chunks + 2 * GROUPS])
    gain_load.start()
    loads = [
        pltpu.make_async_copy(tokens_hbm.at[pl.ds(n * CHUNK, CHUNK)], x_ref.at[pl.ds(n * CHUNK, CHUNK)], sem.at[n])
        for n in range(chunks)
    ]
    for g in range(GROUPS):
        at = chunks + 2 * g
        loads.append(pltpu.make_async_copy(wk_hbm.at[g], w_ref.at[pl.ds(g * PAIR, HEAD_DIM)], sem.at[at]))
        loads.append(
            pltpu.make_async_copy(wv_hbm.at[g], w_ref.at[pl.ds(g * PAIR + HEAD_DIM, HEAD_DIM)], sem.at[at + 1])
        )
    for load in loads:
        load.start()
    pick = to_class_order(rows).astype(jnp.bfloat16)
    gain_load.wait()
    gain = gain_ref[...]
    for n in range(chunks):
        loads[n].wait()
        run = pl.ds(n * CHUNK, CHUNK)
        x = x_ref[run, :].astype(jnp.float32)
        mean = jnp.mean(x * x, axis=-1, keepdims=True)
        normed_ref[run, :] = (x * lax.rsqrt(mean + 1e-6) * gain).astype(jnp.bfloat16)
    for load in loads[chunks:]:
        load.wait()
    kv = dot(normed_ref[...], w_ref[...], NT).astype(jnp.bfloat16)
    kv = dot(pick, kv, NN).astype(jnp.bfloat16)
    kv0_ref[...] = kv[:, 0:PAIR]
    s1_ref[STEPS : STEPS + rows, :] = kv[:, PAIR : 2 * PAIR]
    s1_ref[STEPS + rows : STEPS + 2 * rows, :] = kv[:, 2 * PAIR : 3 * PAIR]
    s2_ref[STEPS : STEPS + rows, :] = kv[:, 2 * PAIR : 3 * PAIR]
    s3_ref[...] = kv[:, 2 * PAIR : 3 * PAIR]
    for r, lo in enumerate(halo_rows(rows)):
        s1_ref[r * HALO : (r + 1) * HALO, :] = kv[lo : lo + HALO, 0:PAIR]
        s2_ref[r * HALO : (r + 1) * HALO, :] = kv[lo : lo + HALO, PAIR : 2 * PAIR]


def query_kernel(normed_ref, wq_ref, q_ref):
    rows = normed_ref.shape[0]
    wq = wq_ref[...].reshape(GROUPS * HEAD_DIM, -1)
    q = (dot(normed_ref[...], wq, NT).astype(jnp.bfloat16) * jnp.bfloat16(0.125)).astype(jnp.bfloat16)
    q_ref[...] = dot(to_class_order(rows).astype(jnp.bfloat16), q, NN).astype(jnp.bfloat16)


def relay_kernel(s3_ref, r1_ref, r2_ref, s4_ref):
    rows = s3_ref.shape[0]
    s4_ref[0:rows, :] = s3_ref[...]
    s4_ref[rows : 2 * rows, :] = r1_ref[STEPS + rows : STEPS + 2 * rows, :]
    for r, lo in enumerate(halo_rows(rows)):
        at = 2 * rows + r * HALO
        s4_ref[at : at + HALO, :] = r2_ref[STEPS + lo : STEPS + lo + HALO, :]


def slope_of(group, slot):
    n = jnp.full((1, 1), group * SLOTS + 1, jnp.int32) + slot
    return jnp.exp2(-8.0 * n.astype(jnp.float32) / (GROUPS * SLOTS))


def bias_of(distance, valid, slope):
    ok = valid & (distance >= 0) & (distance <= STEPS)
    return jnp.where(ok, -slope * distance.astype(jnp.float32), NEG_BIG)


def softmax_pieces(scores):
    top = jnp.max(scores, axis=-1, keepdims=True)
    e = jnp.exp(scores - top)
    total = jnp.sum(e, axis=-1, keepdims=True)
    return (e * (1.0 / total)).astype(jnp.bfloat16), top + jnp.log(total)


def wide_bias(rows, blocks, sp, slope, halo_block=None):
    per_class, per_residue = rows // CLASSES, rows // WIDE_DILATION
    jq, iq = run_of_class(per_class, 0)
    jk, ik = run_of_class(per_class, 1)
    js, at, ok = [], [], []
    for b in blocks:
        js.append(jk)
        at.append(ik - per_residue * b)
        ok.append(jnp.full_like(jk, b) <= sp)
    if halo_block is not None:
        jh, ih = run_of_halo(per_residue, 1)
        js.append(jh)
        at.append(ih - per_residue * halo_block)
        ok.append(jnp.full_like(jh, halo_block) <= sp)
    js, at = jnp.concatenate(js, axis=1), jnp.concatenate(at, axis=1)
    ok = jnp.concatenate([o.astype(jnp.int32) for o in ok], axis=1) > 0
    return bias_of(iq - at, (jq == js) & ok, slope)


def early_kernel(
    sp_ref, slot_ref, q_ref, kv0_ref, s1_ref, s3_ref, r1_ref, r2_ref, r3_ref, o_ref, l_ref, e_ref, top_ref, sum_ref
):
    rows = kv0_ref.shape[0]
    sp, slot = sp_ref[0], slot_ref[0]
    per_class, per_residue = rows // CLASSES, rows // WIDE_DILATION
    runs = [pl.ds(c * per_class, per_class) for c in range(CLASSES)]
    jh, ih = run_of_halo(per_residue, 1)
    tail = jnp.concatenate([16 * ih + 4 * jh + c - rows for c in range(CLASSES)], axis=1)
    tk = jnp.concatenate([positions(rows, 1), tail], axis=1)
    bias = bias_of(positions(rows, 0) - tk, (tk >= 0) | (sp >= 1), slope_of(0, slot))
    keys = jnp.concatenate([kv0_ref[...], r1_ref[0:STEPS, :]], axis=0)
    p, l0 = softmax_pieces(dot(q_ref[:, 0:HEAD_DIM], keys[:, 0:HEAD_DIM], NT) + bias)
    o0 = dot(p, keys[:, HEAD_DIM:PAIR], NN)
    jq, iq = run_of_class(per_class, 0)
    jk, ik = run_of_class(per_class, 1)
    own = 4 * ik + jk
    tk = jnp.concatenate([own, own - per_class, 4 * ih + jh - 2 * per_class], axis=1)
    block = jnp.concatenate([jnp.zeros_like(own), jnp.full_like(own, 1), jnp.full_like(jh, 2)], axis=1)
    bias = bias_of(4 * iq + jq - tk, block <= sp, slope_of(1, slot))
    halo = STEPS // CLASSES
    keys = [
        jnp.concatenate(
            [
                s1_ref[pl.ds(STEPS + c * per_class, per_class), :],
                r1_ref[pl.ds(STEPS + c * per_class, per_class), :],
                r2_ref[pl.ds(c * halo, halo), :],
            ],
            axis=0,
        )
        for c in range(CLASSES)
    ]
    scores = [dot(q_ref[runs[c], HEAD_DIM : 2 * HEAD_DIM], keys[c][:, 0:HEAD_DIM], NT) + bias for c in range(CLASSES)]
    p, l1 = softmax_pieces(jnp.concatenate(scores, axis=0))
    o1 = [
        dot(p[c * per_class : (c + 1) * per_class], keys[c][:, HEAD_DIM:PAIR], NN) for c in range(CLASSES)
    ]
    top = jnp.maximum(l0, l1)
    w0, w1 = jnp.exp(l0 - top), jnp.exp(l1 - top)
    both = w0 + w1
    l_ref[...] = top + jnp.log(both)
    both = 1.0 / both
    o_ref[...] = (w0 * both) * o0 + (w1 * both) * jnp.concatenate(o1, axis=0)
    bias = wide_bias(rows, (0, 1, 2, 3), sp, slope_of(2, slot))
    scores = []
    for c in range(CLASSES):
        lo = c * per_class
        keys = jnp.concatenate(
            [
                s3_ref[runs[c], 0:HEAD_DIM],
                r1_ref[pl.ds(STEPS + rows + lo, per_class), 0:HEAD_DIM],
                r2_ref[pl.ds(STEPS + lo, per_class), 0:HEAD_DIM],
                r3_ref[runs[c], 0:HEAD_DIM],
            ],
            axis=0,
        )
        scores.append(dot(q_ref[runs[c], 2 * HEAD_DIM : 3 * HEAD_DIM], keys, NT) + bias)
    scores = jnp.concatenate(scores, axis=0)
    top = jnp.max(scores, axis=-1, keepdims=True)
    e = jnp.exp(scores - top)
    e_ref[...] = e
    top_ref[...] = top
    sum_ref[...] = jnp.sum(e, axis=-1, keepdims=True)


def late_kernel(
    sp_ref, slot_ref, q_ref, s3_ref, r1_ref, r2_ref, r3_ref, r4_ref, o_ref, l_ref, e_ref, top_ref, sum_ref, mix_ref, lw_ref
):
    rows = s3_ref.shape[0]
    sp, slot = sp_ref[0], slot_ref[0]
    per_class = rows // CLASSES
    halo = STEPS // CLASSES
    runs = [pl.ds(c * per_class, per_class) for c in range(CLASSES)]
    bias = wide_bias(rows, (4, 5), sp, slope_of(2, slot), halo_block=6)
    keys = [
        jnp.concatenate(
            [r4_ref[runs[c], :], r4_ref[pl.ds(rows + c * per_class, per_class), :], r4_ref[pl.ds(2 * rows + c * halo, halo), :]],
            axis=0,
        )
        for c in range(CLASSES)
    ]
    scores = jnp.concatenate(
        [dot(q_ref[runs[c], 2 * HEAD_DIM : 3 * HEAD_DIM], keys[c][:, 0:HEAD_DIM], NT) + bias for c in range(CLASSES)], axis=0
    )
    top0 = top_ref[...]
    top = jnp.maximum(top0, jnp.max(scores, axis=-1, keepdims=True))
    e = jnp.exp(scores - top)
    shrink = jnp.exp(top0 - top)
    total = sum_ref[...] * shrink + jnp.sum(e, axis=-1, keepdims=True)
    scale = 1.0 / total
    l2 = top + jnp.log(total)
    p = (e * scale).astype(jnp.bfloat16)
    p_early = (e_ref[...] * (shrink * scale)).astype(jnp.bfloat16)
    out = []
    for c in range(CLASSES):
        lo = c * per_class
        early = jnp.concatenate(
            [
                s3_ref[runs[c], HEAD_DIM:PAIR],
                r1_ref[pl.ds(STEPS + rows + lo, per_class), HEAD_DIM:PAIR],
                r2_ref[pl.ds(STEPS + lo, per_class), HEAD_DIM:PAIR],
                r3_ref[runs[c], HEAD_DIM:PAIR],
            ],
            axis=0,
        )
        out.append(
            dot(p_early[lo : lo + per_class], early, NN) + dot(p[lo : lo + per_class], keys[c][:, HEAD_DIM:PAIR], NN)
        )
    l01 = l_ref[...]
    top = jnp.maximum(l01, l2)
    w01, w2 = jnp.exp(l01 - top), jnp.exp(l2 - top)
    both = w01 + w2
    lw_ref[...] = top + jnp.log(both)
    both = 1.0 / both
    mixed = ((w01 * both) * o_ref[...] + (w2 * both) * jnp.concatenate(out, axis=0)).astype(jnp.bfloat16)
    mix = dot(mixed, to_class_order(rows).astype(jnp.bfloat16), TN).astype(jnp.bfloat16)
    for n in range(mix_ref.shape[0]):
        mix_ref[n] = mix


def slots_of(core, w_ref):
    return jnp.concatenate([w_ref[2 * x + core] for x in range(SLOTS // 2)], axis=0)


def own_slots_kernel(slot_ref, mix_ref, w_ref, lw_ref, acc_ref, log_weight_ref):
    rows = lw_ref.shape[0]
    mixed = mix_ref[...].reshape(-1, rows)
    acc_ref[...] = dot(mixed, slots_of(slot_ref[0] % 2, w_ref), TN)
    log_weight_ref[...] = jnp.sum(jnp.where(to_class_order(rows), lw_ref[...], 0.0), axis=0, keepdims=True)


def other_slots_kernel(slot_ref, mix_ref, w_ref, acc_ref, out_ref):
    mixed = mix_ref[...].reshape(-1, acc_ref.shape[0])
    out_ref[...] = (acc_ref[...] + dot(mixed, slots_of(1 - slot_ref[0] % 2, w_ref), TN)).astype(jnp.bfloat16)


VMEM = pl.BlockSpec(memory_space=pltpu.VMEM)
SMEM = pl.BlockSpec(memory_space=pltpu.SMEM)
HBM = pl.BlockSpec(memory_space=pltpu.HBM)


def call(body, operands, outs, specs=None, scratch=()):
    return pl.pallas_call(
        body,
        in_specs=specs or [VMEM] * len(operands),
        out_specs=[VMEM] * len(outs),
        out_shape=[jax.ShapeDtypeStruct(s, d) for s, d in outs],
        scratch_shapes=list(scratch),
        compiler_params=pltpu.CompilerParams(vmem_limit_bytes=20 * 2**20),
    )(*operands)


def in_hbm(value):
    return pltpu.with_memory_space_constraint(value, pltpu.HBM)


def from_behind(value, by):
    devices = lax.axis_size("sp")
    return lax.ppermute(value, "sp", [(i, i + by) for i in range(devices - by)])


def layer(tokens, norm_gain, w_query, w_key, w_value, w_out):
    rows, width = tokens.shape
    bf16, f32 = jnp.bfloat16, jnp.float32
    sp = lax.axis_index("sp").reshape(1)
    slot = lax.axis_index("tp").reshape(1)
    kv0, s1, s2, s3, normed = call(
        project_kernel,
        (in_hbm(tokens), in_hbm(norm_gain.reshape(1, -1)), in_hbm(w_key), in_hbm(w_value)),
        [
            ((rows, PAIR), bf16),
            ((STEPS + 2 * rows, PAIR), bf16),
            ((STEPS + rows, PAIR), bf16),
            ((rows, PAIR), bf16),
            ((rows, width), bf16),
        ],
        specs=[HBM] * 4,
        scratch=[
            pltpu.VMEM((rows, width), bf16),
            pltpu.VMEM((1, width), f32),
            pltpu.VMEM((GROUPS * PAIR, width), bf16),
            pltpu.SemaphoreType.DMA((rows // CHUNK + 2 * GROUPS + 1,)),
        ],
    )
    r1 = from_behind(s1, 1)
    r2 = from_behind(s2, 2)
    r3 = from_behind(s3, 3)
    (q,) = call(query_kernel, (normed, w_query), [((rows, GROUPS * HEAD_DIM), bf16)])
    (s4,) = call(relay_kernel, (s3, r1, r2), [((STEPS + 2 * rows, PAIR), bf16)])
    r4 = from_behind(s4, 4)
    o, l, e, top, total = call(
        early_kernel,
        (sp, slot, q, kv0, s1, s3, r1, r2, r3),
        [((rows, HEAD_DIM), f32), ((rows, 1), f32), ((rows, rows), f32), ((rows, 1), f32), ((rows, 1), f32)],
        specs=[SMEM] * 2 + [VMEM] * 7,
    )
    devices = lax.axis_size("tp")
    mix, lw = call(
        late_kernel,
        (sp, slot, q, s3, r1, r2, r3, r4, o, l, e, top, total),
        [((devices // 2, HEAD_DIM, rows), bf16), ((rows, 1), f32)],
        specs=[SMEM] * 2 + [VMEM] * 11,
    )
    same_core = [[2 * x + core for x in range(devices // 2)] for core in range(2)]
    own = lax.all_to_all(mix, "tp", 0, 0, tiled=True, axis_index_groups=same_core)
    other = lax.ppermute(own, "tp", [(i, i ^ 1) for i in range(devices)])
    w = w_out.reshape(devices, HEAD_DIM, -1)
    acc, log_weight = call(
        own_slots_kernel, (slot, own, w, lw), [((rows, w.shape[2]), f32), ((1, rows), f32)], specs=[SMEM] + [VMEM] * 3
    )
    (projected,) = call(
        other_slots_kernel, (slot, other, w, acc), [((rows, w.shape[2]), bf16)], specs=[SMEM] + [VMEM] * 3
    )
    return projected, log_weight


def solution(mesh):
    in_specs = (P("sp", None), P(), P(None, "tp", None), P(None, "tp", None), P(None, "tp", None), P(None, "tp"))
    out_specs = (P("sp", "tp"), P("tp", "sp"))
    return jax.shard_map(layer, mesh=mesh, in_specs=in_specs, out_specs=out_specs, check_vma=False)
```

time: 59.5 us -> 51.4 us (0.86)
  the two profiles are of different devices: /device:TPU:64 before, /device:TPU:897 now
where the time goes in v4:
time: 51.4 us; the launch traced here: 51.1 us
  starting transfers between devices  17.1 us (33%)
  waiting for transfers between devices  14 us (27%)
  Pallas kernels  10.2 us (20%)
  blocking collectives  9 us (18%)
  between operations  0.75 us (1%)
    ppermute x4, waiting for transfers between devices, from_behind(): return lax.ppermute(value, 'sp', [(i, i + by) for i in range(devices - by)])  13.8 us
    ppermute x4, starting transfers between devices, from_behind(): return lax.ppermute(value, 'sp', [(i, i + by) for i in range(devices - by)])  11.6 us
    pallas_call x7, Pallas kernels, call(): pl.pallas_call(body, in_specs=specs or [VMEM] * len(operands), out_specs=...  10.2 us
    all_to_all x1, blocking collectives, layer(): lax.all_to_all(mix, 'tp', 0, 0, tiled=True, axis_index_groups=same_core)  9 us
    ppermute x1, starting transfers between devices, layer(): other = lax.ppermute(own, 'tp', [(i, i ^ 1) for i in range(devices)])  5.59 us
  transfers between devices with their start and end apart: 5, of which 3 were waited for; matrix products, arithmetic and copies ran while one was open for 0% of the time, Pallas kernels for 8%

profile of v4, /device:TPU:897, one launch (start us, length us, event | category | flops | bytes accessed | tf_op | source)
XLA Modules:
  0.0 51.1 jit_solution(9068134067583356797)
XLA Ops:
  0.6 0.0 copy-start.1
  0.6 3.3 %shard_map.77 = (bf16[384,128]{1,0:T(8,128)(2,1)S(1)}, bf16[896,128]{1,0:T(8,128)(2,1)S(1)}, bf16[512,128]{1,0:T(8,128)(2,1)S(1)}, bf16[384,128]{1,0:T(8,128)(2,1)S(1)}, bf16[384,2048]{1,0:T(8,128)(2,1)S(1)}) custom-call(bf16[384,2048]{1,0:T(8,128)(2,1)} %tokens_hbm.1, f32[1,2048]{1,0:T(1,128)} %bitcast.6, bf16[3,64,2048]{2,1,0:T(8,128)(2,1)} %wk_hbm.1, ...), custom_call_target="tpu_custom_call" | custom-call | tf_op jit(solution)/shard_map/pallas_call | solution.py:299
  3.9 3.2 %collective-permute-start = (bf16[896,128]{1,0:T(8,128)(2,1)S(1)}, bf16[896,128]{1,0:T(8,128)(2,1)S(1)}, u32[]{:S(2)}, u32[]{:S(2)}) collective-permute-start(bf16[896,128]{1,0:T(8,128)(2,1)S(1)} %get-tuple-element.18.s1_ref), channel_id=1, source_target_pairs={{0,8},{8,16},{16,24},{24,32},{32,40},{40,48},{48,56},{56,64},{64,7... | collective-permute-start | bytes 688136 | tf_op jit(solution)/shard_map/ppermute | solution.py:315
  7.1 4.5 %collective-permute-start.1 = (bf16[512,128]{1,0:T(8,128)(2,1)S(1)}, bf16[512,128]{1,0:T(8,128)(2,1)S(1)}, u32[]{:S(2)}, u32[]{:S(2)}) collective-permute-start(bf16[512,128]{1,0:T(8,128)(2,1)S(1)} %get-tuple-element.19), channel_id=1, source_target_pairs={{0,16},{8,24},{16,32},{24,40},{32,48},{40,56},{48,64},{56,72},{64,... | collective-permute-start | bytes 393224 | tf_op jit(solution)/shard_map/ppermute | solution.py:315
  11.7 6.0 %collective-permute-done.1.r2_ref = bf16[512,128]{1,0:T(8,128)(2,1)S(1)} collective-permute-done((bf16[512,128]{1,0:T(8,128)(2,1)S(1)}, bf16[512,128]{1,0:T(8,128)(2,1)S(1)}, u32[]{:S(2)}, u32[]{:S(2)}) %collective-permute-start.1) | collective-permute-done | bytes 131104 | tf_op jit(solution)/shard_map/ppermute | solution.py:315
  17.6 0.0 collective-permute-done.r1_ref
  17.6 0.7 %shard_map.79 = bf16[896,128]{1,0:T(8,128)(2,1)} custom-call(bf16[384,128]{1,0:T(8,128)(2,1)S(1)} %get-tuple-element.17.s3_ref, bf16[896,128]{1,0:T(8,128)(2,1)S(1)} %collective-permute-done.r1_ref, bf16[512,128]{1,0:T(8,128)(2,1)S(1)} %collective-permute-done.1.r2_ref), custom_call_target="tpu_custom_call" | custom-call | tf_op jit(solution)/shard_map/pallas_call | solution.py:299
  18.4 1.9 %collective-permute-start.3 = (bf16[896,128]{1,0:T(8,128)(2,1)}, bf16[896,128]{1,0:T(8,128)(2,1)S(1)}, u32[]{:S(2)}, u32[]{:S(2)}) collective-permute-start(bf16[896,128]{1,0:T(8,128)(2,1)} %shard_map.79), channel_id=1, source_target_pairs={{0,32},{8,40},{16,48},{24,56},{32,64},{40,72},{48,80},{56,88},{64,... | collective-permute-start | bytes 688136 | tf_op jit(solution)/shard_map/ppermute | solution.py:315
  20.3 1.9 %collective-permute-start.2 = (bf16[384,128]{1,0:T(8,128)(2,1)S(1)}, bf16[384,128]{1,0:T(8,128)(2,1)S(1)}, u32[]{:S(2)}, u32[]{:S(2)}) collective-permute-start(bf16[384,128]{1,0:T(8,128)(2,1)S(1)} %get-tuple-element.17.s3_ref), channel_id=1, source_target_pairs={{0,24},{8,32},{16,40},{24,48},{32,56},{40,64},{48,72},{56,80},{64,... | collective-permute-start | bytes 294920 | tf_op jit(solution)/shard_map/ppermute | solution.py:315
  22.2 0.0 copy-done.1
  22.2 1.0 %shard_map.78.q_ref = bf16[384,192]{1,0:T(8,128)(2,1)S(1)} custom-call(bf16[384,2048]{1,0:T(8,128)(2,1)S(1)} %get-tuple-element.16.normed_ref, bf16[3,64,2048]{2,1,0:T(8,128)(2,1)S(1)} %copy-done.1), custom_call_target="tpu_custom_call" | custom-call | tf_op jit(solution)/shard_map/pallas_call | solution.py:299
  23.2 7.8 %collective-permute-done.2.r3_ref = bf16[384,128]{1,0:T(8,128)(2,1)S(1)} collective-permute-done((bf16[384,128]{1,0:T(8,128)(2,1)S(1)}, bf16[384,128]{1,0:T(8,128)(2,1)S(1)}, u32[]{:S(2)}, u32[]{:S(2)}) %collective-permute-start.2) | collective-permute-done | bytes 98336 | tf_op jit(solution)/shard_map/ppermute | solution.py:315
  31.0 2.3 %shard_map.80 = (f32[384,64]{1,0:T(8,128)S(1)}, f32[384,1]{1,0:T(8,128)S(1)}, f32[384,384]{1,0:T(8,128)S(1)}, f32[384,1]{1,0:T(8,128)S(1)}, f32[384,1]{1,0:T(8,128)S(1)}) custom-call(s32[1]{0:T(128)} %bitcast.1.sp_ref, s32[1]{0:T(128)} %bitcast.slot_ref, bf16[384,192]{1,0:T(8,128)(2,1)S(1)} %shard_map.78.q_ref, ...), custom_call_target="tpu_custom_call" | custom-call | tf_op jit(solution)/shard_map/pallas_call | solution.py:299
  33.4 0.0 copy-start
  33.4 0.0 collective-permute-done.3.r4_ref
  33.4 1.1 %shard_map.81 = (bf16[4,64,384]{2,1,0:T(8,128)(2,1)S(1)}, f32[384,1]{1,0:T(8,128)S(1)}) custom-call(s32[1]{0:T(128)} %bitcast.1.sp_ref, s32[1]{0:T(128)} %bitcast.slot_ref, bf16[384,192]{1,0:T(8,128)(2,1)S(1)} %shard_map.78.q_ref, bf16[384,128]{1,0:T(8,128)(2,1)S(1)} %get-tuple-element.17.s3_ref, bf16[896,128]{1,0:T(8,128)(2,1)S(1)} %collective-permute-done.r1_ref, ...), custom_call_target="tpu_custom_call" | custom-call | tf_op jit(solution)/shard_map/pallas_call | solution.py:299
  34.5 9.0 %all_to_all.5.mix_ref = bf16[4,64,384]{2,1,0:T(8,128)(2,1)S(1)} all-to-all(bf16[4,64,384]{2,1,0:T(8,128)(2,1)S(1)} %get-tuple-element.26), channel_id=1, replica_groups={{0,2,4,6},{1,3,5,7},{8,10,12,14},{9,11,13,15},{16,18,20,22},{17,19,21,2..., dimensions={0} | all-to-all | bytes 393216 | tf_op jit(solution)/shard_map/all_to_all | solution.py:361
  43.5 5.6 %collective-permute-start.4 = (bf16[4,64,384]{2,1,0:T(8,128)(2,1)S(1)}, bf16[4,64,384]{2,1,0:T(8,128)(2,1)S(1)}, u32[]{:S(2)}, u32[]{:S(2)}) collective-permute-start(bf16[4,64,384]{2,1,0:T(8,128)(2,1)S(1)} %all_to_all.5.mix_ref), channel_id=1, source_target_pairs={{0,1},{1,0},{2,3},{3,2},{4,5},{5,4},{6,7},{7,6},{8,9},{9,8},{10,11... | collective-permute-start | bytes 589832 | tf_op jit(solution)/shard_map/ppermute | solution.py:362
  49.1 0.0 copy-done
  49.1 0.8 %shard_map.82 = (f32[384,256]{1,0:T(8,128)S(1)}, f32[1,384]{1,0:T(1,128)}) custom-call(s32[1]{0:T(128)} %bitcast.slot_ref, bf16[4,64,384]{2,1,0:T(8,128)(2,1)S(1)} %all_to_all.5.mix_ref, bf16[8,64,256]{2,1,0:T(8,128)(2,1)S(1)} %bitcast.4, f32[384,1]{1,0:T(8,128)S(1)} %get-tuple-element.27.lw_ref), custom_call_target="tpu_custom_call" | custom-call | tf_op jit(solution)/shard_map/pallas_call | solution.py:299
  49.9 0.2 collective-permute-done.4.mix_ref
  50.2 0.9 %shard_map.83 = bf16[384,256]{1,0:T(8,128)(2,1)} custom-call(s32[1]{0:T(128)} %bitcast.slot_ref, bf16[4,64,384]{2,1,0:T(8,128)(2,1)S(1)} %collective-permute-done.4.mix_ref, bf16[8,64,256]{2,1,0:T(8,128)(2,1)S(1)} %bitcast.5, f32[384,256]{1,0:T(8,128)S(1)} %get-tuple-element.28.acc_ref), custom_call_target="tpu_custom_call" | custom-call | tf_op jit(solution)/shard_map/pallas_call | solution.py:299
Async XLA Ops:
  0.6 21.6 %copy-start.1 = (bf16[3,64,2048]{2,1,0:T(8,128)(2,1)S(1)}, bf16[3,64,2048]{2,1,0:T(8,128)(2,1)}, u32[]{:S(2)}) copy-start(bf16[3,64,2048]{2,1,0:T(8,128)(2,1)} %wq_ref.1) | copy-start | bytes 2359300
  3.9 13.7 %collective-permute-start = (bf16[896,128]{1,0:T(8,128)(2,1)S(1)}, bf16[896,128]{1,0:T(8,128)(2,1)S(1)}, u32[]{:S(2)}, u32[]{:S(2)}) collective-permute-start(bf16[896,128]{1,0:T(8,128)(2,1)S(1)} %get-tuple-element.18.s1_ref), channel_id=1, source_target_pairs={{0,8},{8,16},{16,24},{24,32},{32,40},{40,48},{48,56},{56,64},{64,7... | collective-permute-start | bytes 688136 | tf_op jit(solution)/shard_map/ppermute | solution.py:315
  7.1 10.5 %collective-permute-start.1 = (bf16[512,128]{1,0:T(8,128)(2,1)S(1)}, bf16[512,128]{1,0:T(8,128)(2,1)S(1)}, u32[]{:S(2)}, u32[]{:S(2)}) collective-permute-start(bf16[512,128]{1,0:T(8,128)(2,1)S(1)} %get-tuple-element.19), channel_id=1, source_target_pairs={{0,16},{8,24},{16,32},{24,40},{32,48},{40,56},{48,64},{56,72},{64,... | collective-permute-start | bytes 393224 | tf_op jit(solution)/shard_map/ppermute | solution.py:315
  18.4 15.0 %collective-permute-start.3 = (bf16[896,128]{1,0:T(8,128)(2,1)}, bf16[896,128]{1,0:T(8,128)(2,1)S(1)}, u32[]{:S(2)}, u32[]{:S(2)}) collective-permute-start(bf16[896,128]{1,0:T(8,128)(2,1)} %shard_map.79), channel_id=1, source_target_pairs={{0,32},{8,40},{16,48},{24,56},{32,64},{40,72},{48,80},{56,88},{64,... | collective-permute-start | bytes 688136 | tf_op jit(solution)/shard_map/ppermute | solution.py:315
  20.3 10.7 %collective-permute-start.2 = (bf16[384,128]{1,0:T(8,128)(2,1)S(1)}, bf16[384,128]{1,0:T(8,128)(2,1)S(1)}, u32[]{:S(2)}, u32[]{:S(2)}) collective-permute-start(bf16[384,128]{1,0:T(8,128)(2,1)S(1)} %get-tuple-element.17.s3_ref), channel_id=1, source_target_pairs={{0,24},{8,32},{16,40},{24,48},{32,56},{40,64},{48,72},{56,80},{64,... | collective-permute-start | bytes 294920 | tf_op jit(solution)/shard_map/ppermute | solution.py:315
  33.4 15.8 %copy-start = (bf16[512,256]{1,0:T(8,128)(2,1)S(1)}, bf16[512,256]{1,0:T(8,128)(2,1)}, u32[]{:S(2)}) copy-start(bf16[512,256]{1,0:T(8,128)(2,1)} %param.11) | copy-start | bytes 786436
  43.5 6.6 %collective-permute-start.4 = (bf16[4,64,384]{2,1,0:T(8,128)(2,1)S(1)}, bf16[4,64,384]{2,1,0:T(8,128)(2,1)S(1)}, u32[]{:S(2)}, u32[]{:S(2)}) collective-permute-start(bf16[4,64,384]{2,1,0:T(8,128)(2,1)S(1)} %all_to_all.5.mix_ref), channel_id=1, source_target_pairs={{0,1},{1,0},{2,3},{3,2},{4,5},{5,4},{6,7},{7,6},{8,9},{9,8},{10,11... | collective-permute-start | bytes 589832 | tf_op jit(solution)/shard_map/ppermute | solution.py:362

commit v5 on v4

--- a/solution.py
+++ b/solution.py
@@ -109,12 +109,11 @@
     q_ref[...] = dot(to_class_order(rows).astype(jnp.bfloat16), q, NN).astype(jnp.bfloat16)
 
 
-def relay_kernel(s3_ref, r1_ref, r2_ref, s4_ref):
-    rows = s3_ref.shape[0]
-    s4_ref[0:rows, :] = s3_ref[...]
-    s4_ref[rows : 2 * rows, :] = r1_ref[STEPS + rows : STEPS + 2 * rows, :]
+def relay_kernel(r1_ref, r2_ref, s4_ref):
+    rows = r1_ref.shape[0] // 2 - STEPS // 2
+    s4_ref[0:rows, :] = r1_ref[STEPS + rows : STEPS + 2 * rows, :]
     for r, lo in enumerate(halo_rows(rows)):
-        at = 2 * rows + r * HALO
+        at = rows + r * HALO
         s4_ref[at : at + HALO, :] = r2_ref[STEPS + lo : STEPS + lo + HALO, :]
 
 
@@ -155,7 +154,8 @@
 
 
 def early_kernel(
-    sp_ref, slot_ref, q_ref, kv0_ref, s1_ref, s3_ref, r1_ref, r2_ref, r3_ref, o_ref, l_ref, e_ref, top_ref, sum_ref
+    sp_ref, slot_ref, q_ref, kv0_ref, s1_ref, s3_ref, r1_ref, r2_ref, r3_ref, r4_ref, o_ref, l_ref, e_ref, top_ref,
+    sum_ref,
 ):
     rows = kv0_ref.shape[0]
     sp, slot = sp_ref[0], slot_ref[0]
@@ -197,7 +197,7 @@
     l_ref[...] = top + jnp.log(both)
     both = 1.0 / both
     o_ref[...] = (w0 * both) * o0 + (w1 * both) * jnp.concatenate(o1, axis=0)
-    bias = wide_bias(rows, (0, 1, 2, 3), sp, slope_of(2, slot))
+    bias = wide_bias(rows, (0, 1, 2, 3, 4), sp, slope_of(2, slot))
     scores = []
     for c in range(CLASSES):
         lo = c * per_class
@@ -207,6 +207,7 @@
                 r1_ref[pl.ds(STEPS + rows + lo, per_class), 0:HEAD_DIM],
                 r2_ref[pl.ds(STEPS + lo, per_class), 0:HEAD_DIM],
                 r3_ref[runs[c], 0:HEAD_DIM],
+                r4_ref[runs[c], 0:HEAD_DIM],
             ],
             axis=0,
         )
@@ -220,17 +221,18 @@
 
 
 def late_kernel(
-    sp_ref, slot_ref, q_ref, s3_ref, r1_ref, r2_ref, r3_ref, r4_ref, o_ref, l_ref, e_ref, top_ref, sum_ref, mix_ref, lw_ref
+    sp_ref, slot_ref, q_ref, s3_ref, r1_ref, r2_ref, r3_ref, r4_ref, far_ref, o_ref, l_ref, e_ref, top_ref, sum_ref,
+    mix_ref, lw_ref,
 ):
     rows = s3_ref.shape[0]
     sp, slot = sp_ref[0], slot_ref[0]
     per_class = rows // CLASSES
     halo = STEPS // CLASSES
     runs = [pl.ds(c * per_class, per_class) for c in range(CLASSES)]
-    bias = wide_bias(rows, (4, 5), sp, slope_of(2, slot), halo_block=6)
+    bias = wide_bias(rows, (5,), sp, slope_of(2, slot), halo_block=6)
     keys = [
         jnp.concatenate(
-            [r4_ref[runs[c], :], r4_ref[pl.ds(rows + c * per_class, per_class), :], r4_ref[pl.ds(2 * rows + c * halo, halo), :]],
+            [far_ref[runs[c], :], far_ref[pl.ds(rows + c * halo, halo), :]],
             axis=0,
         )
         for c in range(CLASSES)
@@ -256,6 +258,7 @@
                 r1_ref[pl.ds(STEPS + rows + lo, per_class), HEAD_DIM:PAIR],
                 r2_ref[pl.ds(STEPS + lo, per_class), HEAD_DIM:PAIR],
                 r3_ref[runs[c], HEAD_DIM:PAIR],
+                r4_ref[runs[c], HEAD_DIM:PAIR],
             ],
             axis=0,
         )
@@ -266,28 +269,19 @@
     top = jnp.maximum(l01, l2)
     w01, w2 = jnp.exp(l01 - top), jnp.exp(l2 - top)
     both = w01 + w2
-    lw_ref[...] = top + jnp.log(both)
+    lw = top + jnp.log(both)
     both = 1.0 / both
     mixed = ((w01 * both) * o_ref[...] + (w2 * both) * jnp.concatenate(out, axis=0)).astype(jnp.bfloat16)
-    mix = dot(mixed, to_class_order(rows).astype(jnp.bfloat16), TN).astype(jnp.bfloat16)
+    pick = to_class_order(rows)
+    mix = dot(mixed, pick.astype(jnp.bfloat16), TN).astype(jnp.bfloat16)
     for n in range(mix_ref.shape[0]):
         mix_ref[n] = mix
-
-
-def slots_of(core, w_ref):
-    return jnp.concatenate([w_ref[2 * x + core] for x in range(SLOTS // 2)], axis=0)
-
-
-def own_slots_kernel(slot_ref, mix_ref, w_ref, lw_ref, acc_ref, log_weight_ref):
-    rows = lw_ref.shape[0]
-    mixed = mix_ref[...].reshape(-1, rows)
-    acc_ref[...] = dot(mixed, slots_of(slot_ref[0] % 2, w_ref), TN)
-    log_weight_ref[...] = jnp.sum(jnp.where(to_class_order(rows), lw_ref[...], 0.0), axis=0, keepdims=True)
-
-
-def other_slots_kernel(slot_ref, mix_ref, w_ref, acc_ref, out_ref):
-    mixed = mix_ref[...].reshape(-1, acc_ref.shape[0])
-    out_ref[...] = (acc_ref[...] + dot(mixed, slots_of(1 - slot_ref[0] % 2, w_ref), TN)).astype(jnp.bfloat16)
+    lw_ref[...] = jnp.sum(jnp.where(pick, lw, 0.0), axis=0, keepdims=True)
+
+
+def output_kernel(mix_ref, w_ref, out_ref):
+    mixed = mix_ref[...].reshape(-1, out_ref.shape[0])
+    out_ref[...] = dot(mixed, w_ref[...], TN).astype(jnp.bfloat16)
 
 
 VMEM = pl.BlockSpec(memory_space=pltpu.VMEM)
@@ -341,32 +335,25 @@
     r1 = from_behind(s1, 1)
     r2 = from_behind(s2, 2)
     r3 = from_behind(s3, 3)
+    r4 = from_behind(s3, 4)
     (q,) = call(query_kernel, (normed, w_query), [((rows, GROUPS * HEAD_DIM), bf16)])
-    (s4,) = call(relay_kernel, (s3, r1, r2), [((STEPS + 2 * rows, PAIR), bf16)])
-    r4 = from_behind(s4, 4)
+    (s4,) = call(relay_kernel, (r1, r2), [((STEPS + rows, PAIR), bf16)])
+    far = from_behind(s4, 4)
     o, l, e, top, total = call(
         early_kernel,
-        (sp, slot, q, kv0, s1, s3, r1, r2, r3),
-        [((rows, HEAD_DIM), f32), ((rows, 1), f32), ((rows, rows), f32), ((rows, 1), f32), ((rows, 1), f32)],
-        specs=[SMEM] * 2 + [VMEM] * 7,
+        (sp, slot, q, kv0, s1, s3, r1, r2, r3, r4),
+        [((rows, HEAD_DIM), f32), ((rows, 1), f32), ((rows, 5 * rows // CLASSES), f32), ((rows, 1), f32), ((rows, 1), f32)],
+        specs=[SMEM] * 2 + [VMEM] * 8,
     )
     devices = lax.axis_size("tp")
-    mix, lw = call(
+    mix, log_weight = call(
         late_kernel,
-        (sp, slot, q, s3, r1, r2, r3, r4, o, l, e, top, total),
-        [((devices // 2, HEAD_DIM, rows), bf16), ((rows, 1), f32)],
-        specs=[SMEM] * 2 + [VMEM] * 11,
+        (sp, slot, q, s3, r1, r2, r3, r4, far, o, l, e, top, total),
+        [((devices, HEAD_DIM, rows), bf16), ((1, rows), f32)],
+        specs=[SMEM] * 2 + [VMEM] * 12,
     )
-    same_core = [[2 * x + core for x in range(devices // 2)] for core in range(2)]
-    own = lax.all_to_all(mix, "tp", 0, 0, tiled=True, axis_index_groups=same_core)
-    other = lax.ppermute(own, "tp", [(i, i ^ 1) for i in range(devices)])
-    w = w_out.reshape(devices, HEAD_DIM, -1)
-    acc, log_weight = call(
-        own_slots_kernel, (slot, own, w, lw), [((rows, w.shape[2]), f32), ((1, rows), f32)], specs=[SMEM] + [VMEM] * 3
-    )
-    (projected,) = call(
-        other_slots_kernel, (slot, other, w, acc), [((rows, w.shape[2]), bf16)], specs=[SMEM] + [VMEM] * 3
-    )
+    everyone = lax.all_to_all(mix, "tp", 0, 0, tiled=True)
+    (projected,) = call(output_kernel, (everyone, w_out), [((rows, w_out.shape[1]), bf16)])
     return projected, log_weight
 
 

time: 51.4 us -> 54.9 us (1.068)
  the two profiles are of different devices: /device:TPU:897 before, /device:TPU:320 now
where the time goes in v5:
time: 54.9 us; the launch traced here: 54.6 us
  starting transfers between devices  20.3 us (37%)
  blocking collectives  13 us (24%)
  waiting for transfers between devices  10.3 us (19%)
  Pallas kernels  9.64 us (18%)
  between operations  0.76 us (1%)
  local copies, waits for them, and re-layouts  0.65 us (1%)
    ppermute x5, starting transfers between devices, from_behind(): return lax.ppermute(value, 'sp', [(i, i + by) for i in range(devices - by)])  20.3 us
    all_to_all x1, blocking collectives, layer(): everyone = lax.all_to_all(mix, 'tp', 0, 0, tiled=True)  13 us
    ppermute x5, waiting for transfers between devices, from_behind(): return lax.ppermute(value, 'sp', [(i, i + by) for i in range(devices - by)])  10.3 us
    pallas_call x6, Pallas kernels, call(): pl.pallas_call(body, in_specs=specs or [VMEM] * len(operands), out_specs=...  9.64 us
  transfers between devices with their start and end apart: 5, of which 2 were waited for; matrix products, arithmetic and copies ran while one was open for 0% of the time, Pallas kernels for 7%

profile of v5, /device:TPU:320, one launch (start us, length us, event | category | flops | bytes accessed | tf_op | source)
XLA Modules:
  0.0 54.6 jit_solution(2184210941304764546)
XLA Ops:
  0.6 0.0 copy-start
  0.6 3.3 %shard_map.77 = (bf16[384,128]{1,0:T(8,128)(2,1)S(1)}, bf16[896,128]{1,0:T(8,128)(2,1)S(1)}, bf16[512,128]{1,0:T(8,128)(2,1)S(1)}, bf16[384,128]{1,0:T(8,128)(2,1)S(1)}, bf16[384,2048]{1,0:T(8,128)(2,1)S(1)}) custom-call(bf16[384,2048]{1,0:T(8,128)(2,1)} %tokens_hbm.1, f32[1,2048]{1,0:T(1,128)} %bitcast.3, bf16[3,64,2048]{2,1,0:T(8,128)(2,1)} %wk_hbm.1, ...), custom_call_target="tpu_custom_call" | custom-call | tf_op jit(solution)/shard_map/pallas_call | solution.py:293
  3.9 0.0 copy-start.2
  4.0 0.6 %copy-done.2 = bf16[384,128]{1,0:T(8,128)(2,1)} copy-done((bf16[384,128]{1,0:T(8,128)(2,1)}, bf16[384,128]{1,0:T(8,128)(2,1)S(1)}, u32[]{:S(2)}) %copy-start.2) | copy-done | bytes 98328
  4.6 3.5 %collective-permute-start = (bf16[896,128]{1,0:T(8,128)(2,1)S(1)}, bf16[896,128]{1,0:T(8,128)(2,1)S(1)}, u32[]{:S(2)}, u32[]{:S(2)}) collective-permute-start(bf16[896,128]{1,0:T(8,128)(2,1)S(1)} %get-tuple-element.16.s1_ref), channel_id=1, source_target_pairs={{0,8},{8,16},{16,24},{24,32},{32,40},{40,48},{48,56},{56,64},{64,7... | collective-permute-start | bytes 688136 | tf_op jit(solution)/shard_map/ppermute | solution.py:309
  8.1 4.8 %collective-permute-start.1 = (bf16[512,128]{1,0:T(8,128)(2,1)S(1)}, bf16[512,128]{1,0:T(8,128)(2,1)S(1)}, u32[]{:S(2)}, u32[]{:S(2)}) collective-permute-start(bf16[512,128]{1,0:T(8,128)(2,1)S(1)} %get-tuple-element.17), channel_id=1, source_target_pairs={{0,16},{8,24},{16,32},{24,40},{32,48},{40,56},{48,64},{56,72},{64,... | collective-permute-start | bytes 393224 | tf_op jit(solution)/shard_map/ppermute | solution.py:309
  12.9 5.8 %collective-permute-done.1.r2_ref = bf16[512,128]{1,0:T(8,128)(2,1)S(1)} collective-permute-done((bf16[512,128]{1,0:T(8,128)(2,1)S(1)}, bf16[512,128]{1,0:T(8,128)(2,1)S(1)}, u32[]{:S(2)}, u32[]{:S(2)}) %collective-permute-start.1) | collective-permute-done | bytes 131104 | tf_op jit(solution)/shard_map/ppermute | solution.py:309
  18.7 0.0 collective-permute-done.r1_ref
  18.7 3.8 %collective-permute-start.4 = (bf16[512,128]{1,0:T(8,128)(2,1)S(1)}, bf16[512,128]{1,0:T(8,128)(2,1)S(1)}, u32[]{:S(2)}, u32[]{:S(2)}) collective-permute-start(bf16[512,128]{1,0:T(8,128)(2,1)S(1)} %shard_map.79), channel_id=1, source_target_pairs={{0,32},{8,40},{16,48},{24,56},{32,64},{40,72},{48,80},{56,88},{64,... | collective-permute-start | bytes 393224 | tf_op jit(solution)/shard_map/ppermute | solution.py:309
  22.6 6.2 %collective-permute-start.3 = (bf16[384,128]{1,0:T(8,128)(2,1)S(1)}, bf16[384,128]{1,0:T(8,128)(2,1)S(1)}, u32[]{:S(2)}, u32[]{:S(2)}) collective-permute-start(bf16[384,128]{1,0:T(8,128)(2,1)S(1)} %get-tuple-element.15.s3_ref), channel_id=1, source_target_pairs={{0,32},{8,40},{16,48},{24,56},{32,64},{40,72},{48,80},{56,88},{64,... | collective-permute-start | bytes 294920 | tf_op jit(solution)/shard_map/ppermute | solution.py:309
  28.8 1.9 %collective-permute-start.2 = (bf16[384,128]{1,0:T(8,128)(2,1)S(1)}, bf16[384,128]{1,0:T(8,128)(2,1)S(1)}, u32[]{:S(2)}, u32[]{:S(2)}) collective-permute-start(bf16[384,128]{1,0:T(8,128)(2,1)S(1)} %get-tuple-element.15.s3_ref), channel_id=1, source_target_pairs={{0,24},{8,32},{16,40},{24,48},{32,56},{40,64},{48,72},{56,80},{64,... | collective-permute-start | bytes 294920 | tf_op jit(solution)/shard_map/ppermute | solution.py:309
  30.8 0.0 copy-start.3
  30.8 0.0 copy-done
  30.8 1.0 %shard_map.78.q_ref = bf16[384,192]{1,0:T(8,128)(2,1)S(1)} custom-call(bf16[384,2048]{1,0:T(8,128)(2,1)S(1)} %get-tuple-element.14.normed_ref, bf16[3,64,2048]{2,1,0:T(8,128)(2,1)S(1)} %copy-done), custom_call_target="tpu_custom_call" | custom-call | tf_op jit(solution)/shard_map/pallas_call | solution.py:293
  31.8 0.0 collective-permute-done.3.r4_ref
  31.8 4.5 %collective-permute-done.2.r3_ref = bf16[384,128]{1,0:T(8,128)(2,1)S(1)} collective-permute-done((bf16[384,128]{1,0:T(8,128)(2,1)S(1)}, bf16[384,128]{1,0:T(8,128)(2,1)S(1)}, u32[]{:S(2)}, u32[]{:S(2)}) %collective-permute-start.2) | collective-permute-done | bytes 98336 | tf_op jit(solution)/shard_map/ppermute | solution.py:309
  36.2 0.0 copy-done.3
  36.2 2.8 %shard_map.80 = (f32[384,64]{1,0:T(8,128)S(1)}, f32[384,1]{1,0:T(8,128)S(1)}, f32[384,480]{1,0:T(8,128)S(1)}, f32[384,1]{1,0:T(8,128)S(1)}, f32[384,1]{1,0:T(8,128)S(1)}) custom-call(s32[1]{0:T(128)} %bitcast.sp_ref, s32[1]{0:T(128)} %bitcast.1.slot_ref, bf16[384,192]{1,0:T(8,128)(2,1)S(1)} %shard_map.78.q_ref, bf16[384,128]{1,0:T(8,128)(2,1)S(1)} %copy-done.3, ...), custom_call_target="tpu_custom_call" | custom-call | tf_op jit(solution)/shard_map/pallas_call | solution.py:293
  39.1 0.0 collective-permute-done.4.far_ref
  39.1 0.0 copy-start.1
  39.1 1.6 %shard_map.81 = (bf16[8,64,384]{2,1,0:T(8,128)(2,1)S(1)}, f32[1,384]{1,0:T(1,128)}) custom-call(s32[1]{0:T(128)} %bitcast.sp_ref, s32[1]{0:T(128)} %bitcast.1.slot_ref, bf16[384,192]{1,0:T(8,128)(2,1)S(1)} %shard_map.78.q_ref, bf16[384,128]{1,0:T(8,128)(2,1)S(1)} %get-tuple-element.15.s3_ref, bf16[896,128]{1,0:T(8,128)(2,1)S(1)} %collective-permute-done.r1_ref, ...), custom_call_target="tpu_custom_call" | custom-call | tf_op jit(solution)/shard_map/pallas_call | solution.py:293
  40.6 13.0 %all_to_all.5.mix_ref = bf16[8,64,384]{2,1,0:T(8,128)(2,1)S(1)} all-to-all(bf16[8,64,384]{2,1,0:T(8,128)(2,1)S(1)} %get-tuple-element.24), channel_id=1, replica_groups=mesh['sp'=128,'tp'=8] {'tp'}, dimensions={0} | all-to-all | bytes 786432 | tf_op jit(solution)/shard_map/all_to_all | solution.py:355
  53.6 0.0 copy-done.1
  53.6 1.0 %shard_map.82 = bf16[384,256]{1,0:T(8,128)(2,1)} custom-call(bf16[8,64,384]{2,1,0:T(8,128)(2,1)S(1)} %all_to_all.5.mix_ref, bf16[512,256]{1,0:T(8,128)(2,1)S(1)} %copy-done.1), custom_call_target="tpu_custom_call" | custom-call | tf_op jit(solution)/shard_map/pallas_call | solution.py:293
  (1 shorter events, 0.0 us)
Async XLA Ops:
  0.6 30.1 %copy-start = (bf16[3,64,2048]{2,1,0:T(8,128)(2,1)S(1)}, bf16[3,64,2048]{2,1,0:T(8,128)(2,1)}, u32[]{:S(2)}) copy-start(bf16[3,64,2048]{2,1,0:T(8,128)(2,1)} %wq_ref.1) | copy-start | bytes 2359300
  3.9 0.6 %copy-start.2 = (bf16[384,128]{1,0:T(8,128)(2,1)}, bf16[384,128]{1,0:T(8,128)(2,1)S(1)}, u32[]{:S(2)}) copy-start(bf16[384,128]{1,0:T(8,128)(2,1)S(1)} %get-tuple-element.18.kv0_ref) | copy-start | bytes 294916
  4.6 14.1 %collective-permute-start = (bf16[896,128]{1,0:T(8,128)(2,1)S(1)}, bf16[896,128]{1,0:T(8,128)(2,1)S(1)}, u32[]{:S(2)}, u32[]{:S(2)}) collective-permute-start(bf16[896,128]{1,0:T(8,128)(2,1)S(1)} %get-tuple-element.16.s1_ref), channel_id=1, source_target_pairs={{0,8},{8,16},{16,24},{24,32},{32,40},{40,48},{48,56},{56,64},{64,7... | collective-permute-start | bytes 688136 | tf_op jit(solution)/shard_map/ppermute | solution.py:309
  8.1 10.7 %collective-permute-start.1 = (bf16[512,128]{1,0:T(8,128)(2,1)S(1)}, bf16[512,128]{1,0:T(8,128)(2,1)S(1)}, u32[]{:S(2)}, u32[]{:S(2)}) collective-permute-start(bf16[512,128]{1,0:T(8,128)(2,1)S(1)} %get-tuple-element.17), channel_id=1, source_target_pairs={{0,16},{8,24},{16,32},{24,40},{32,48},{40,56},{48,64},{56,72},{64,... | collective-permute-start | bytes 393224 | tf_op jit(solution)/shard_map/ppermute | solution.py:309
  18.7 20.3 %collective-permute-start.4 = (bf16[512,128]{1,0:T(8,128)(2,1)S(1)}, bf16[512,128]{1,0:T(8,128)(2,1)S(1)}, u32[]{:S(2)}, u32[]{:S(2)}) collective-permute-start(bf16[512,128]{1,0:T(8,128)(2,1)S(1)} %shard_map.79), channel_id=1, source_target_pairs={{0,32},{8,40},{16,48},{24,56},{32,64},{40,72},{48,80},{56,88},{64,... | collective-permute-start | bytes 393224 | tf_op jit(solution)/shard_map/ppermute | solution.py:309
  22.6 9.2 %collective-permute-start.3 = (bf16[384,128]{1,0:T(8,128)(2,1)S(1)}, bf16[384,128]{1,0:T(8,128)(2,1)S(1)}, u32[]{:S(2)}, u32[]{:S(2)}) collective-permute-start(bf16[384,128]{1,0:T(8,128)(2,1)S(1)} %get-tuple-element.15.s3_ref), channel_id=1, source_target_pairs={{0,32},{8,40},{16,48},{24,56},{32,64},{40,72},{48,80},{56,88},{64,... | collective-permute-start | bytes 294920 | tf_op jit(solution)/shard_map/ppermute | solution.py:309
  28.8 7.4 %collective-permute-start.2 = (bf16[384,128]{1,0:T(8,128)(2,1)S(1)}, bf16[384,128]{1,0:T(8,128)(2,1)S(1)}, u32[]{:S(2)}, u32[]{:S(2)}) collective-permute-start(bf16[384,128]{1,0:T(8,128)(2,1)S(1)} %get-tuple-element.15.s3_ref), channel_id=1, source_target_pairs={{0,24},{8,32},{16,40},{24,48},{32,56},{40,64},{48,72},{56,80},{64,... | collective-permute-start | bytes 294920 | tf_op jit(solution)/shard_map/ppermute | solution.py:309
  30.8 5.5 %copy-start.3 = (bf16[384,128]{1,0:T(8,128)(2,1)S(1)}, bf16[384,128]{1,0:T(8,128)(2,1)}, u32[]{:S(2)}) copy-start(bf16[384,128]{1,0:T(8,128)(2,1)} %copy-done.2) | copy-start | bytes 294916
  39.1 14.6 %copy-start.1 = (bf16[512,256]{1,0:T(8,128)(2,1)S(1)}, bf16[512,256]{1,0:T(8,128)(2,1)}, u32[]{:S(2)}) copy-start(bf16[512,256]{1,0:T(8,128)(2,1)} %w_ref.1) | copy-start | bytes 786436

commit v6 on v5

--- a/solution.py
+++ b/solution.py
@@ -109,12 +109,15 @@
     q_ref[...] = dot(to_class_order(rows).astype(jnp.bfloat16), q, NN).astype(jnp.bfloat16)
 
 
-def relay_kernel(r1_ref, r2_ref, s4_ref):
-    rows = r1_ref.shape[0] // 2 - STEPS // 2
-    s4_ref[0:rows, :] = r1_ref[STEPS + rows : STEPS + 2 * rows, :]
-    for r, lo in enumerate(halo_rows(rows)):
-        at = rows + r * HALO
-        s4_ref[at : at + HALO, :] = r2_ref[STEPS + lo : STEPS + lo + HALO, :]
+def relay_kernel(s3_ref, r1_ref, s4_ref):
+    rows = s3_ref.shape[0]
+    s4_ref[0:rows, :] = s3_ref[...]
+    s4_ref[rows : 2 * rows, :] = r1_ref[STEPS + rows : STEPS + 2 * rows, :]
+
+
+def relay_tail_kernel(r2_ref, s6_ref):
+    for r, lo in enumerate(halo_rows(r2_ref.shape[0] - STEPS)):
+        s6_ref[r * HALO : (r + 1) * HALO, :] = r2_ref[STEPS + lo : STEPS + lo + HALO, :]
 
 
 def slope_of(group, slot):
@@ -154,8 +157,7 @@
 
 
 def early_kernel(
-    sp_ref, slot_ref, q_ref, kv0_ref, s1_ref, s3_ref, r1_ref, r2_ref, r3_ref, r4_ref, o_ref, l_ref, e_ref, top_ref,
-    sum_ref,
+    sp_ref, slot_ref, q_ref, kv0_ref, s1_ref, s3_ref, r1_ref, r2_ref, r3_ref, o_ref, l_ref, e_ref, top_ref, sum_ref
 ):
     rows = kv0_ref.shape[0]
     sp, slot = sp_ref[0], slot_ref[0]
@@ -197,7 +199,7 @@
     l_ref[...] = top + jnp.log(both)
     both = 1.0 / both
     o_ref[...] = (w0 * both) * o0 + (w1 * both) * jnp.concatenate(o1, axis=0)
-    bias = wide_bias(rows, (0, 1, 2, 3, 4), sp, slope_of(2, slot))
+    bias = wide_bias(rows, (0, 1, 2, 3), sp, slope_of(2, slot))
     scores = []
     for c in range(CLASSES):
         lo = c * per_class
@@ -207,7 +209,6 @@
                 r1_ref[pl.ds(STEPS + rows + lo, per_class), 0:HEAD_DIM],
                 r2_ref[pl.ds(STEPS + lo, per_class), 0:HEAD_DIM],
                 r3_ref[runs[c], 0:HEAD_DIM],
-                r4_ref[runs[c], 0:HEAD_DIM],
             ],
             axis=0,
         )
@@ -221,7 +222,7 @@
 
 
 def late_kernel(
-    sp_ref, slot_ref, q_ref, s3_ref, r1_ref, r2_ref, r3_ref, r4_ref, far_ref, o_ref, l_ref, e_ref, top_ref, sum_ref,
+    sp_ref, slot_ref, q_ref, s3_ref, r1_ref, r2_ref, r3_ref, r4_ref, r6_ref, o_ref, l_ref, e_ref, top_ref, sum_ref,
     mix_ref, lw_ref,
 ):
     rows = s3_ref.shape[0]
@@ -229,10 +230,10 @@
     per_class = rows // CLASSES
     halo = STEPS // CLASSES
     runs = [pl.ds(c * per_class, per_class) for c in range(CLASSES)]
-    bias = wide_bias(rows, (5,), sp, slope_of(2, slot), halo_block=6)
+    bias = wide_bias(rows, (4, 5), sp, slope_of(2, slot), halo_block=6)
     keys = [
         jnp.concatenate(
-            [far_ref[runs[c], :], far_ref[pl.ds(rows + c * halo, halo), :]],
+            [r4_ref[runs[c], :], r4_ref[pl.ds(rows + c * per_class, per_class), :], r6_ref[pl.ds(c * halo, halo), :]],
             axis=0,
         )
         for c in range(CLASSES)
@@ -258,7 +259,6 @@
                 r1_ref[pl.ds(STEPS + rows + lo, per_class), HEAD_DIM:PAIR],
                 r2_ref[pl.ds(STEPS + lo, per_class), HEAD_DIM:PAIR],
                 r3_ref[runs[c], HEAD_DIM:PAIR],
-                r4_ref[runs[c], HEAD_DIM:PAIR],
             ],
             axis=0,
         )
@@ -335,20 +335,21 @@
     r1 = from_behind(s1, 1)
     r2 = from_behind(s2, 2)
     r3 = from_behind(s3, 3)
-    r4 = from_behind(s3, 4)
+    (s4,) = call(relay_kernel, (s3, r1), [((2 * rows, PAIR), bf16)])
+    r4 = from_behind(s4, 4)
     (q,) = call(query_kernel, (normed, w_query), [((rows, GROUPS * HEAD_DIM), bf16)])
-    (s4,) = call(relay_kernel, (r1, r2), [((STEPS + rows, PAIR), bf16)])
-    far = from_behind(s4, 4)
+    (s6,) = call(relay_tail_kernel, (r2,), [((STEPS, PAIR), bf16)])
+    r6 = from_behind(s6, 4)
     o, l, e, top, total = call(
         early_kernel,
-        (sp, slot, q, kv0, s1, s3, r1, r2, r3, r4),
-        [((rows, HEAD_DIM), f32), ((rows, 1), f32), ((rows, 5 * rows // CLASSES), f32), ((rows, 1), f32), ((rows, 1), f32)],
-        specs=[SMEM] * 2 + [VMEM] * 8,
+        (sp, slot, q, kv0, s1, s3, r1, r2, r3),
+        [((rows, HEAD_DIM), f32), ((rows, 1), f32), ((rows, rows), f32), ((rows, 1), f32), ((rows, 1), f32)],
+        specs=[SMEM] * 2 + [VMEM] * 7,
     )
     devices = lax.axis_size("tp")
     mix, log_weight = call(
         late_kernel,
-        (sp, slot, q, s3, r1, r2, r3, r4, far, o, l, e, top, total),
+        (sp, slot, q, s3, r1, r2, r3, r4, r6, o, l, e, top, total),
         [((devices, HEAD_DIM, rows), bf16), ((1, rows), f32)],
         specs=[SMEM] * 2 + [VMEM] * 12,
     )

time: 54.9 us -> 56.1 us (1.022)
  the two profiles are of different devices: /device:TPU:320 before, /device:TPU:224 now
where the time goes in v6:
time: 56.1 us; the launch traced here: 55.9 us
  starting transfers between devices  19.7 us (35%)
  blocking collectives  13 us (23%)
  waiting for transfers between devices  11.7 us (21%)
  Pallas kernels  10.7 us (19%)
  between operations  0.78 us (1%)
    ppermute x5, starting transfers between devices, from_behind(): return lax.ppermute(value, 'sp', [(i, i + by) for i in range(devices - by)])  19.7 us
    all_to_all x1, blocking collectives, layer(): everyone = lax.all_to_all(mix, 'tp', 0, 0, tiled=True)  13 us
    ppermute x5, waiting for transfers between devices, from_behind(): return lax.ppermute(value, 'sp', [(i, i + by) for i in range(devices - by)])  11.7 us
    pallas_call x7, Pallas kernels, call(): pl.pallas_call(body, in_specs=specs or [VMEM] * len(operands), out_specs=...  10.7 us
  transfers between devices with their start and end apart: 5, of which 2 were waited for; matrix products, arithmetic and copies ran while one was open for 0% of the time, Pallas kernels for 7%

profile of v6, /device:TPU:224, one launch (start us, length us, event | category | flops | bytes accessed | tf_op | source)
XLA Modules:
  0.0 55.9 jit_solution(4809552985812740305)
XLA Ops:
  0.6 0.0 copy-start
  0.6 3.3 %shard_map.77 = (bf16[384,128]{1,0:T(8,128)(2,1)S(1)}, bf16[896,128]{1,0:T(8,128)(2,1)S(1)}, bf16[512,128]{1,0:T(8,128)(2,1)S(1)}, bf16[384,128]{1,0:T(8,128)(2,1)S(1)}, bf16[384,2048]{1,0:T(8,128)(2,1)S(1)}) custom-call(bf16[384,2048]{1,0:T(8,128)(2,1)} %tokens_hbm.1, f32[1,2048]{1,0:T(1,128)} %bitcast.3, bf16[3,64,2048]{2,1,0:T(8,128)(2,1)} %wk_hbm.1, ...), custom_call_target="tpu_custom_call" | custom-call | tf_op jit(solution)/shard_map/pallas_call | solution.py:293
  3.9 0.0 copy-start.2
  4.0 3.5 %collective-permute-start = (bf16[896,128]{1,0:T(8,128)(2,1)S(1)}, bf16[896,128]{1,0:T(8,128)(2,1)S(1)}, u32[]{:S(2)}, u32[]{:S(2)}) collective-permute-start(bf16[896,128]{1,0:T(8,128)(2,1)S(1)} %get-tuple-element.16.s1_ref), channel_id=1, source_target_pairs={{0,8},{8,16},{16,24},{24,32},{32,40},{40,48},{48,56},{56,64},{64,7... | collective-permute-start | bytes 688136 | tf_op jit(solution)/shard_map/ppermute | solution.py:309
  7.4 7.9 %collective-permute-done.r1_ref = bf16[896,128]{1,0:T(8,128)(2,1)S(1)} collective-permute-done((bf16[896,128]{1,0:T(8,128)(2,1)S(1)}, bf16[896,128]{1,0:T(8,128)(2,1)S(1)}, u32[]{:S(2)}, u32[]{:S(2)}) %collective-permute-start) | collective-permute-done | bytes 229408 | tf_op jit(solution)/shard_map/ppermute | solution.py:309
  15.3 6.2 %collective-permute-start.3 = (bf16[768,128]{1,0:T(8,128)(2,1)S(1)}, bf16[768,128]{1,0:T(8,128)(2,1)S(1)}, u32[]{:S(2)}, u32[]{:S(2)}) collective-permute-start(bf16[768,128]{1,0:T(8,128)(2,1)S(1)} %shard_map.79), channel_id=1, source_target_pairs={{0,32},{8,40},{16,48},{24,56},{32,64},{40,72},{48,80},{56,88},{64,... | collective-permute-start | bytes 589832 | tf_op jit(solution)/shard_map/ppermute | solution.py:309
  21.6 0.0 copy-done.2
  21.6 1.9 %collective-permute-start.1 = (bf16[512,128]{1,0:T(8,128)(2,1)S(1)}, bf16[512,128]{1,0:T(8,128)(2,1)S(1)}, u32[]{:S(2)}, u32[]{:S(2)}) collective-permute-start(bf16[512,128]{1,0:T(8,128)(2,1)S(1)} %get-tuple-element.17), channel_id=1, source_target_pairs={{0,16},{8,24},{16,32},{24,40},{32,48},{40,56},{48,64},{56,72},{64,... | collective-permute-start | bytes 393224 | tf_op jit(solution)/shard_map/ppermute | solution.py:309
  23.5 4.2 %collective-permute-start.2 = (bf16[384,128]{1,0:T(8,128)(2,1)S(1)}, bf16[384,128]{1,0:T(8,128)(2,1)S(1)}, u32[]{:S(2)}, u32[]{:S(2)}) collective-permute-start(bf16[384,128]{1,0:T(8,128)(2,1)S(1)} %get-tuple-element.15.s3_ref), channel_id=1, source_target_pairs={{0,24},{8,32},{16,40},{24,48},{32,56},{40,64},{48,72},{56,80},{64,... | collective-permute-start | bytes 294920 | tf_op jit(solution)/shard_map/ppermute | solution.py:309
  27.7 3.9 %collective-permute-done.1.r2_ref = bf16[512,128]{1,0:T(8,128)(2,1)S(1)} collective-permute-done((bf16[512,128]{1,0:T(8,128)(2,1)S(1)}, bf16[512,128]{1,0:T(8,128)(2,1)S(1)}, u32[]{:S(2)}, u32[]{:S(2)}) %collective-permute-start.1) | collective-permute-done | bytes 131104 | tf_op jit(solution)/shard_map/ppermute | solution.py:309
  31.6 0.6 %shard_map.80 = bf16[128,128]{1,0:T(8,128)(2,1)} custom-call(bf16[512,128]{1,0:T(8,128)(2,1)S(1)} %collective-permute-done.1.r2_ref), custom_call_target="tpu_custom_call" | custom-call | tf_op jit(solution)/shard_map/pallas_call | solution.py:293
  32.2 3.8 %collective-permute-start.4 = (bf16[128,128]{1,0:T(8,128)(2,1)}, bf16[128,128]{1,0:T(8,128)(2,1)}, u32[]{:S(2)}, u32[]{:S(2)}) collective-permute-start(bf16[128,128]{1,0:T(8,128)(2,1)} %shard_map.80), channel_id=1, source_target_pairs={{0,32},{8,40},{16,48},{24,56},{32,64},{40,72},{48,80},{56,88},{64,... | collective-permute-start | bytes 98312 | tf_op jit(solution)/shard_map/ppermute | solution.py:309
  36.0 0.0 copy-start.3
  36.0 0.0 copy-done
  36.0 1.0 %shard_map.78.q_ref = bf16[384,192]{1,0:T(8,128)(2,1)S(1)} custom-call(bf16[384,2048]{1,0:T(8,128)(2,1)S(1)} %get-tuple-element.14.normed_ref, bf16[3,64,2048]{2,1,0:T(8,128)(2,1)S(1)} %copy-done), custom_call_target="tpu_custom_call" | custom-call | tf_op jit(solution)/shard_map/pallas_call | solution.py:293
  37.0 0.0 collective-permute-done.2.r3_ref
  37.0 0.0 copy-done.3
  37.0 2.3 %shard_map.81 = (f32[384,64]{1,0:T(8,128)S(1)}, f32[384,1]{1,0:T(8,128)S(1)}, f32[384,384]{1,0:T(8,128)S(1)}, f32[384,1]{1,0:T(8,128)S(1)}, f32[384,1]{1,0:T(8,128)S(1)}) custom-call(s32[1]{0:T(128)} %bitcast.sp_ref, s32[1]{0:T(128)} %bitcast.1.slot_ref, bf16[384,192]{1,0:T(8,128)(2,1)S(1)} %shard_map.78.q_ref, bf16[384,128]{1,0:T(8,128)(2,1)S(1)} %copy-done.3, ...), custom_call_target="tpu_custom_call" | custom-call | tf_op jit(solution)/shard_map/pallas_call | solution.py:293
  39.4 0.0 collective-permute-done.4.r6_ref
  39.4 0.0 collective-permute-done.3.r4_ref
  39.4 0.0 copy-start.1
  39.4 2.5 %shard_map.82 = (bf16[8,64,384]{2,1,0:T(8,128)(2,1)S(1)}, f32[1,384]{1,0:T(1,128)}) custom-call(s32[1]{0:T(128)} %bitcast.sp_ref, s32[1]{0:T(128)} %bitcast.1.slot_ref, bf16[384,192]{1,0:T(8,128)(2,1)S(1)} %shard_map.78.q_ref, bf16[384,128]{1,0:T(8,128)(2,1)S(1)} %get-tuple-element.15.s3_ref, bf16[896,128]{1,0:T(8,128)(2,1)S(1)} %collective-permute-done.r1_ref, ...), custom_call_target="tpu_custom_call" | custom-call | tf_op jit(solution)/shard_map/pallas_call | solution.py:293
  41.9 13.0 %all_to_all.5.mix_ref = bf16[8,64,384]{2,1,0:T(8,128)(2,1)S(1)} all-to-all(bf16[8,64,384]{2,1,0:T(8,128)(2,1)S(1)} %get-tuple-element.24), channel_id=1, replica_groups=mesh['sp'=128,'tp'=8] {'tp'}, dimensions={0} | all-to-all | bytes 786432 | tf_op jit(solution)/shard_map/all_to_all | solution.py:356
  54.9 1.0 %shard_map.83 = bf16[384,256]{1,0:T(8,128)(2,1)} custom-call(bf16[8,64,384]{2,1,0:T(8,128)(2,1)S(1)} %all_to_all.5.mix_ref, bf16[512,256]{1,0:T(8,128)(2,1)S(1)} %copy-done.1), custom_call_target="tpu_custom_call" | custom-call | tf_op jit(solution)/shard_map/pallas_call | solution.py:293
  (2 shorter events, 0.0 us)
Async XLA Ops:
  0.6 35.4 %copy-start = (bf16[3,64,2048]{2,1,0:T(8,128)(2,1)S(1)}, bf16[3,64,2048]{2,1,0:T(8,128)(2,1)}, u32[]{:S(2)}) copy-start(bf16[3,64,2048]{2,1,0:T(8,128)(2,1)} %wq_ref.1) | copy-start | bytes 2359300
  3.9 17.6 %copy-start.2 = (bf16[384,128]{1,0:T(8,128)(2,1)}, bf16[384,128]{1,0:T(8,128)(2,1)S(1)}, u32[]{:S(2)}) copy-start(bf16[384,128]{1,0:T(8,128)(2,1)S(1)} %get-tuple-element.18.kv0_ref) | copy-start | bytes 294916
  4.0 11.3 %collective-permute-start = (bf16[896,128]{1,0:T(8,128)(2,1)S(1)}, bf16[896,128]{1,0:T(8,128)(2,1)S(1)}, u32[]{:S(2)}, u32[]{:S(2)}) collective-permute-start(bf16[896,128]{1,0:T(8,128)(2,1)S(1)} %get-tuple-element.16.s1_ref), channel_id=1, source_target_pairs={{0,8},{8,16},{16,24},{24,32},{32,40},{40,48},{48,56},{56,64},{64,7... | collective-permute-start | bytes 688136 | tf_op jit(solution)/shard_map/ppermute | solution.py:309
  15.3 24.1 %collective-permute-start.3 = (bf16[768,128]{1,0:T(8,128)(2,1)S(1)}, bf16[768,128]{1,0:T(8,128)(2,1)S(1)}, u32[]{:S(2)}, u32[]{:S(2)}) collective-permute-start(bf16[768,128]{1,0:T(8,128)(2,1)S(1)} %shard_map.79), channel_id=1, source_target_pairs={{0,32},{8,40},{16,48},{24,56},{32,64},{40,72},{48,80},{56,88},{64,... | collective-permute-start | bytes 589832 | tf_op jit(solution)/shard_map/ppermute | solution.py:309
  21.6 10.0 %collective-permute-start.1 = (bf16[512,128]{1,0:T(8,128)(2,1)S(1)}, bf16[512,128]{1,0:T(8,128)(2,1)S(1)}, u32[]{:S(2)}, u32[]{:S(2)}) collective-permute-start(bf16[512,128]{1,0:T(8,128)(2,1)S(1)} %get-tuple-element.17), channel_id=1, source_target_pairs={{0,16},{8,24},{16,32},{24,40},{32,48},{40,56},{48,64},{56,72},{64,... | collective-permute-start | bytes 393224 | tf_op jit(solution)/shard_map/ppermute | solution.py:309
  23.5 13.5 %collective-permute-start.2 = (bf16[384,128]{1,0:T(8,128)(2,1)S(1)}, bf16[384,128]{1,0:T(8,128)(2,1)S(1)}, u32[]{:S(2)}, u32[]{:S(2)}) collective-permute-start(bf16[384,128]{1,0:T(8,128)(2,1)S(1)} %get-tuple-element.15.s3_ref), channel_id=1, source_target_pairs={{0,24},{8,32},{16,40},{24,48},{32,56},{40,64},{48,72},{56,80},{64,... | collective-permute-start | bytes 294920 | tf_op jit(solution)/shard_map/ppermute | solution.py:309
  32.2 7.2 %collective-permute-start.4 = (bf16[128,128]{1,0:T(8,128)(2,1)}, bf16[128,128]{1,0:T(8,128)(2,1)}, u32[]{:S(2)}, u32[]{:S(2)}) collective-permute-start(bf16[128,128]{1,0:T(8,128)(2,1)} %shard_map.80), channel_id=1, source_target_pairs={{0,32},{8,40},{16,48},{24,56},{32,64},{40,72},{48,80},{56,88},{64,... | collective-permute-start | bytes 98312 | tf_op jit(solution)/shard_map/ppermute | solution.py:309
  36.0 1.0 %copy-start.3 = (bf16[384,128]{1,0:T(8,128)(2,1)S(1)}, bf16[384,128]{1,0:T(8,128)(2,1)}, u32[]{:S(2)}) copy-start(bf16[384,128]{1,0:T(8,128)(2,1)} %copy-done.2) | copy-start | bytes 294916
  39.4 15.5 %copy-start.1 = (bf16[512,256]{1,0:T(8,128)(2,1)S(1)}, bf16[512,256]{1,0:T(8,128)(2,1)}, u32[]{:S(2)}) copy-start(bf16[512,256]{1,0:T(8,128)(2,1)} %w_ref.1) | copy-start | bytes 786436

commit v7 on v4

--- a/solution.py
+++ b/solution.py
@@ -274,20 +274,13 @@
         mix_ref[n] = mix
 
 
-def slots_of(core, w_ref):
-    return jnp.concatenate([w_ref[2 * x + core] for x in range(SLOTS // 2)], axis=0)
-
-
-def own_slots_kernel(slot_ref, mix_ref, w_ref, lw_ref, acc_ref, log_weight_ref):
-    rows = lw_ref.shape[0]
-    mixed = mix_ref[...].reshape(-1, rows)
-    acc_ref[...] = dot(mixed, slots_of(slot_ref[0] % 2, w_ref), TN)
-    log_weight_ref[...] = jnp.sum(jnp.where(to_class_order(rows), lw_ref[...], 0.0), axis=0, keepdims=True)
-
-
-def other_slots_kernel(slot_ref, mix_ref, w_ref, acc_ref, out_ref):
-    mixed = mix_ref[...].reshape(-1, acc_ref.shape[0])
-    out_ref[...] = (acc_ref[...] + dot(mixed, slots_of(1 - slot_ref[0] % 2, w_ref), TN)).astype(jnp.bfloat16)
+def log_weight_kernel(lw_ref, out_ref):
+    out_ref[...] = jnp.sum(jnp.where(to_class_order(lw_ref.shape[0]), lw_ref[...], 0.0), axis=0, keepdims=True)
+
+
+def output_kernel(mix_ref, w_ref, out_ref):
+    mixed = mix_ref[...].reshape(-1, out_ref.shape[0])
+    out_ref[...] = dot(mixed, w_ref[...], TN).astype(jnp.bfloat16)
 
 
 VMEM = pl.BlockSpec(memory_space=pltpu.VMEM)
@@ -354,19 +347,12 @@
     mix, lw = call(
         late_kernel,
         (sp, slot, q, s3, r1, r2, r3, r4, o, l, e, top, total),
-        [((devices // 2, HEAD_DIM, rows), bf16), ((rows, 1), f32)],
+        [((devices, HEAD_DIM, rows), bf16), ((rows, 1), f32)],
         specs=[SMEM] * 2 + [VMEM] * 11,
     )
-    same_core = [[2 * x + core for x in range(devices // 2)] for core in range(2)]
-    own = lax.all_to_all(mix, "tp", 0, 0, tiled=True, axis_index_groups=same_core)
-    other = lax.ppermute(own, "tp", [(i, i ^ 1) for i in range(devices)])
-    w = w_out.reshape(devices, HEAD_DIM, -1)
-    acc, log_weight = call(
-        own_slots_kernel, (slot, own, w, lw), [((rows, w.shape[2]), f32), ((1, rows), f32)], specs=[SMEM] + [VMEM] * 3
-    )
-    (projected,) = call(
-        other_slots_kernel, (slot, other, w, acc), [((rows, w.shape[2]), bf16)], specs=[SMEM] + [VMEM] * 3
-    )
+    everyone = lax.all_to_all(mix, "tp", 0, 0, tiled=True)
+    (log_weight,) = call(log_weight_kernel, (lw,), [((1, rows), f32)])
+    (projected,) = call(output_kernel, (everyone, w_out), [((rows, w_out.shape[1]), bf16)])
     return projected, log_weight
 
 

time: 51.4 us -> 51.4 us (level)
  the two profiles are of different devices: /device:TPU:897 before, /device:TPU:896 now
where the time goes in v7:
time: 51.4 us; the launch traced here: 51.1 us
  waiting for transfers between devices  22.3 us (43%)
  starting transfers between devices  17.1 us (33%)
  Pallas kernels  10.9 us (21%)
  between operations  0.72 us (1%)
    ppermute x4, waiting for transfers between devices, from_behind(): return lax.ppermute(value, 'sp', [(i, i + by) for i in range(devices - by)])  14.1 us
    ppermute x4, starting transfers between devices, from_behind(): return lax.ppermute(value, 'sp', [(i, i + by) for i in range(devices - by)])  12.8 us
    pallas_call x7, Pallas kernels, call(): pl.pallas_call(body, in_specs=specs or [VMEM] * len(operands), out_specs=...  10.9 us
    all_to_all x1, waiting for transfers between devices, layer(): everyone = lax.all_to_all(mix, 'tp', 0, 0, tiled=True)  8.15 us
    all_to_all x1, starting transfers between devices, layer(): everyone = lax.all_to_all(mix, 'tp', 0, 0, tiled=True)  4.3 us
  transfers between devices with their start and end apart: 5, of which 3 were waited for; matrix products, arithmetic and copies ran while one was open for 0% of the time, Pallas kernels for 8%

profile of v7, /device:TPU:896, one launch (start us, length us, event | category | flops | bytes accessed | tf_op | source)
XLA Modules:
  0.0 51.1 jit_solution(6058327901725425075)
XLA Ops:
  0.6 0.0 copy-start
  0.6 3.3 %shard_map.77 = (bf16[384,128]{1,0:T(8,128)(2,1)S(1)}, bf16[896,128]{1,0:T(8,128)(2,1)S(1)}, bf16[512,128]{1,0:T(8,128)(2,1)S(1)}, bf16[384,128]{1,0:T(8,128)(2,1)S(1)}, bf16[384,2048]{1,0:T(8,128)(2,1)S(1)}) custom-call(bf16[384,2048]{1,0:T(8,128)(2,1)} %tokens_hbm.1, f32[1,2048]{1,0:T(1,128)} %bitcast.3, bf16[3,64,2048]{2,1,0:T(8,128)(2,1)} %wk_hbm.1, ...), custom_call_target="tpu_custom_call" | custom-call | tf_op jit(solution)/shard_map/pallas_call | solution.py:292
  3.9 3.5 %collective-permute-start = (bf16[896,128]{1,0:T(8,128)(2,1)S(1)}, bf16[896,128]{1,0:T(8,128)(2,1)S(1)}, u32[]{:S(2)}, u32[]{:S(2)}) collective-permute-start(bf16[896,128]{1,0:T(8,128)(2,1)S(1)} %get-tuple-element.16.s1_ref), channel_id=1, source_target_pairs={{0,8},{8,16},{16,24},{24,32},{32,40},{40,48},{48,56},{56,64},{64,7... | collective-permute-start | bytes 688136 | tf_op jit(solution)/shard_map/ppermute | solution.py:308
  7.4 4.8 %collective-permute-start.1 = (bf16[512,128]{1,0:T(8,128)(2,1)S(1)}, bf16[512,128]{1,0:T(8,128)(2,1)S(1)}, u32[]{:S(2)}, u32[]{:S(2)}) collective-permute-start(bf16[512,128]{1,0:T(8,128)(2,1)S(1)} %get-tuple-element.17), channel_id=1, source_target_pairs={{0,16},{8,24},{16,32},{24,40},{32,48},{40,56},{48,64},{56,72},{64,... | collective-permute-start | bytes 393224 | tf_op jit(solution)/shard_map/ppermute | solution.py:308
  12.3 7.1 %collective-permute-done.1.r2_ref = bf16[512,128]{1,0:T(8,128)(2,1)S(1)} collective-permute-done((bf16[512,128]{1,0:T(8,128)(2,1)S(1)}, bf16[512,128]{1,0:T(8,128)(2,1)S(1)}, u32[]{:S(2)}, u32[]{:S(2)}) %collective-permute-start.1) | collective-permute-done | bytes 131104 | tf_op jit(solution)/shard_map/ppermute | solution.py:308
  19.3 0.0 collective-permute-done.r1_ref
  19.3 0.7 %shard_map.79 = bf16[896,128]{1,0:T(8,128)(2,1)} custom-call(bf16[384,128]{1,0:T(8,128)(2,1)S(1)} %get-tuple-element.15.s3_ref, bf16[896,128]{1,0:T(8,128)(2,1)S(1)} %collective-permute-done.r1_ref, bf16[512,128]{1,0:T(8,128)(2,1)S(1)} %collective-permute-done.1.r2_ref), custom_call_target="tpu_custom_call" | custom-call | tf_op jit(solution)/shard_map/pallas_call | solution.py:292
  20.0 1.9 %collective-permute-start.3 = (bf16[896,128]{1,0:T(8,128)(2,1)}, bf16[896,128]{1,0:T(8,128)(2,1)S(1)}, u32[]{:S(2)}, u32[]{:S(2)}) collective-permute-start(bf16[896,128]{1,0:T(8,128)(2,1)} %shard_map.79), channel_id=1, source_target_pairs={{0,32},{8,40},{16,48},{24,56},{32,64},{40,72},{48,80},{56,88},{64,... | collective-permute-start | bytes 688136 | tf_op jit(solution)/shard_map/ppermute | solution.py:308
  21.9 2.6 %collective-permute-start.2 = (bf16[384,128]{1,0:T(8,128)(2,1)S(1)}, bf16[384,128]{1,0:T(8,128)(2,1)S(1)}, u32[]{:S(2)}, u32[]{:S(2)}) collective-permute-start(bf16[384,128]{1,0:T(8,128)(2,1)S(1)} %get-tuple-element.15.s3_ref), channel_id=1, source_target_pairs={{0,24},{8,32},{16,40},{24,48},{32,56},{40,64},{48,72},{56,80},{64,... | collective-permute-start | bytes 294920 | tf_op jit(solution)/shard_map/ppermute | solution.py:308
  24.5 0.0 copy-done
  24.6 1.0 %shard_map.78.q_ref = bf16[384,192]{1,0:T(8,128)(2,1)S(1)} custom-call(bf16[384,2048]{1,0:T(8,128)(2,1)S(1)} %get-tuple-element.14.normed_ref, bf16[3,64,2048]{2,1,0:T(8,128)(2,1)S(1)} %copy-done), custom_call_target="tpu_custom_call" | custom-call | tf_op jit(solution)/shard_map/pallas_call | solution.py:292
  25.5 7.1 %collective-permute-done.2.r3_ref = bf16[384,128]{1,0:T(8,128)(2,1)S(1)} collective-permute-done((bf16[384,128]{1,0:T(8,128)(2,1)S(1)}, bf16[384,128]{1,0:T(8,128)(2,1)S(1)}, u32[]{:S(2)}, u32[]{:S(2)}) %collective-permute-start.2) | collective-permute-done | bytes 98336 | tf_op jit(solution)/shard_map/ppermute | solution.py:308
  32.6 2.3 %shard_map.80 = (f32[384,64]{1,0:T(8,128)S(1)}, f32[384,1]{1,0:T(8,128)S(1)}, f32[384,384]{1,0:T(8,128)S(1)}, f32[384,1]{1,0:T(8,128)S(1)}, f32[384,1]{1,0:T(8,128)S(1)}) custom-call(s32[1]{0:T(128)} %bitcast.sp_ref, s32[1]{0:T(128)} %bitcast.1.slot_ref, bf16[384,192]{1,0:T(8,128)(2,1)S(1)} %shard_map.78.q_ref, ...), custom_call_target="tpu_custom_call" | custom-call | tf_op jit(solution)/shard_map/pallas_call | solution.py:292
  34.9 0.0 collective-permute-done.3.r4_ref
  35.0 0.0 copy-start.1
  35.0 1.9 %shard_map.81 = (bf16[8,64,384]{2,1,0:T(8,128)(2,1)}, f32[384,1]{1,0:T(8,128)S(1)}) custom-call(s32[1]{0:T(128)} %bitcast.sp_ref, s32[1]{0:T(128)} %bitcast.1.slot_ref, bf16[384,192]{1,0:T(8,128)(2,1)S(1)} %shard_map.78.q_ref, bf16[384,128]{1,0:T(8,128)(2,1)S(1)} %get-tuple-element.15.s3_ref, bf16[896,128]{1,0:T(8,128)(2,1)S(1)} %collective-permute-done.r1_ref, ...), custom_call_target="tpu_custom_call" | custom-call | tf_op jit(solution)/shard_map/pallas_call | solution.py:292
  36.9 4.3 %all-to-all-start = ((bf16[8,64,384]{2,1,0:T(8,128)(2,1)}), bf16[8,64,384]{2,1,0:T(8,128)(2,1)S(1)}, u32[]{:S(2)}, u32[]{:S(2)}) async-start(bf16[8,64,384]{2,1,0:T(8,128)(2,1)} %get-tuple-element.24), calls=%async_computation | async-start | bytes 786432 | tf_op jit(solution)/shard_map/all_to_all | solution.py:353
  41.2 0.8 %shard_map.83 = f32[1,384]{1,0:T(1,128)} custom-call(f32[384,1]{1,0:T(8,128)S(1)} %get-tuple-element.25.lw_ref), custom_call_target="tpu_custom_call" | custom-call | tf_op jit(solution)/shard_map/pallas_call | solution.py:292
  41.9 8.2 %all-to-all-done.mix_ref = bf16[8,64,384]{2,1,0:T(8,128)(2,1)S(1)} async-done(((bf16[8,64,384]{2,1,0:T(8,128)(2,1)}), bf16[8,64,384]{2,1,0:T(8,128)(2,1)S(1)}, u32[]{:S(2)}, u32[]{:S(2)}) %all-to-all-start) | async-done | bytes 393248 | tf_op jit(solution)/shard_map/all_to_all | solution.py:353
  50.1 0.0 copy-done.1
  50.1 1.0 %shard_map.82 = bf16[384,256]{1,0:T(8,128)(2,1)} custom-call(bf16[8,64,384]{2,1,0:T(8,128)(2,1)S(1)} %all-to-all-done.mix_ref, bf16[512,256]{1,0:T(8,128)(2,1)S(1)} %copy-done.1), custom_call_target="tpu_custom_call" | custom-call | tf_op jit(solution)/shard_map/pallas_call | solution.py:292
Async XLA Ops:
  0.6 23.9 %copy-start = (bf16[3,64,2048]{2,1,0:T(8,128)(2,1)S(1)}, bf16[3,64,2048]{2,1,0:T(8,128)(2,1)}, u32[]{:S(2)}) copy-start(bf16[3,64,2048]{2,1,0:T(8,128)(2,1)} %wq_ref.1) | copy-start | bytes 2359300
  3.9 15.4 %collective-permute-start = (bf16[896,128]{1,0:T(8,128)(2,1)S(1)}, bf16[896,128]{1,0:T(8,128)(2,1)S(1)}, u32[]{:S(2)}, u32[]{:S(2)}) collective-permute-start(bf16[896,128]{1,0:T(8,128)(2,1)S(1)} %get-tuple-element.16.s1_ref), channel_id=1, source_target_pairs={{0,8},{8,16},{16,24},{24,32},{32,40},{40,48},{48,56},{56,64},{64,7... | collective-permute-start | bytes 688136 | tf_op jit(solution)/shard_map/ppermute | solution.py:308
  7.4 11.9 %collective-permute-start.1 = (bf16[512,128]{1,0:T(8,128)(2,1)S(1)}, bf16[512,128]{1,0:T(8,128)(2,1)S(1)}, u32[]{:S(2)}, u32[]{:S(2)}) collective-permute-start(bf16[512,128]{1,0:T(8,128)(2,1)S(1)} %get-tuple-element.17), channel_id=1, source_target_pairs={{0,16},{8,24},{16,32},{24,40},{32,48},{40,56},{48,64},{56,72},{64,... | collective-permute-start | bytes 393224 | tf_op jit(solution)/shard_map/ppermute | solution.py:308
  20.0 14.9 %collective-permute-start.3 = (bf16[896,128]{1,0:T(8,128)(2,1)}, bf16[896,128]{1,0:T(8,128)(2,1)S(1)}, u32[]{:S(2)}, u32[]{:S(2)}) collective-permute-start(bf16[896,128]{1,0:T(8,128)(2,1)} %shard_map.79), channel_id=1, source_target_pairs={{0,32},{8,40},{16,48},{24,56},{32,64},{40,72},{48,80},{56,88},{64,... | collective-permute-start | bytes 688136 | tf_op jit(solution)/shard_map/ppermute | solution.py:308
  21.9 10.7 %collective-permute-start.2 = (bf16[384,128]{1,0:T(8,128)(2,1)S(1)}, bf16[384,128]{1,0:T(8,128)(2,1)S(1)}, u32[]{:S(2)}, u32[]{:S(2)}) collective-permute-start(bf16[384,128]{1,0:T(8,128)(2,1)S(1)} %get-tuple-element.15.s3_ref), channel_id=1, source_target_pairs={{0,24},{8,32},{16,40},{24,48},{32,56},{40,64},{48,72},{56,80},{64,... | collective-permute-start | bytes 294920 | tf_op jit(solution)/shard_map/ppermute | solution.py:308
  35.0 15.1 %copy-start.1 = (bf16[512,256]{1,0:T(8,128)(2,1)S(1)}, bf16[512,256]{1,0:T(8,128)(2,1)}, u32[]{:S(2)}) copy-start(bf16[512,256]{1,0:T(8,128)(2,1)} %w_ref.1) | copy-start | bytes 786436
  36.9 13.2 %all-to-all-start = ((bf16[8,64,384]{2,1,0:T(8,128)(2,1)}), bf16[8,64,384]{2,1,0:T(8,128)(2,1)S(1)}, u32[]{:S(2)}, u32[]{:S(2)}) async-start(bf16[8,64,384]{2,1,0:T(8,128)(2,1)} %get-tuple-element.24), calls=%async_computation | async-start | bytes 786432 | tf_op jit(solution)/shard_map/all_to_all | solution.py:353

commit v8 on v7

--- a/solution.py
+++ b/solution.py
@@ -60,8 +60,15 @@
     return [r * per_residue + per_residue - HALO for r in range(WIDE_DILATION)]
 
 
+def queries(normed, wq_ref):
+    wq = wq_ref[...].reshape(GROUPS * HEAD_DIM, -1)
+    q = (dot(normed, wq, NT).astype(jnp.bfloat16) * jnp.bfloat16(0.125)).astype(jnp.bfloat16)
+    return dot(to_class_order(normed.shape[0]).astype(jnp.bfloat16), q, NN).astype(jnp.bfloat16)
+
+
 def project_kernel(
-    tokens_hbm, gain_hbm, wk_hbm, wv_hbm, kv0_ref, s1_ref, s2_ref, s3_ref, normed_ref, x_ref, gain_ref, w_ref, sem
+    slot_ref, tokens_hbm, gain_hbm, wk_hbm, wv_hbm, wq_hbm, kv0_ref, s1_ref, s2_ref, s3_ref, normed_ref, q_ref, x_ref, gain_ref, w_ref,
+    wq_ref, sem,
 ):
     rows = x_ref.shape[0]
     chunks = rows // CHUNK
@@ -79,6 +86,8 @@
         )
     for load in loads:
         load.start()
+    wq_load = pltpu.make_async_copy(wq_hbm, wq_ref, sem.at[chunks + 2 * GROUPS + 1])
+    wq_load.start()
     pick = to_class_order(rows).astype(jnp.bfloat16)
     gain_load.wait()
     gain = gain_ref[...]
@@ -100,13 +109,21 @@
     for r, lo in enumerate(halo_rows(rows)):
         s1_ref[r * HALO : (r + 1) * HALO, :] = kv[lo : lo + HALO, 0:PAIR]
         s2_ref[r * HALO : (r + 1) * HALO, :] = kv[lo : lo + HALO, PAIR : 2 * PAIR]
-
-
-def query_kernel(normed_ref, wq_ref, q_ref):
-    rows = normed_ref.shape[0]
-    wq = wq_ref[...].reshape(GROUPS * HEAD_DIM, -1)
-    q = (dot(normed_ref[...], wq, NT).astype(jnp.bfloat16) * jnp.bfloat16(0.125)).astype(jnp.bfloat16)
-    q_ref[...] = dot(to_class_order(rows).astype(jnp.bfloat16), q, NN).astype(jnp.bfloat16)
+    wq_load.wait()
+
+    @pl.when(slot_ref[0] % 2 == 1)
+    def _():
+        q_ref[...] = queries(normed_ref[...], wq_ref)
+
+
+def query_kernel(slot_ref, normed_ref, wq_ref, done_ref, q_ref):
+    @pl.when(slot_ref[0] % 2 == 1)
+    def _():
+        q_ref[...] = done_ref[...]
+
+    @pl.when(slot_ref[0] % 2 == 0)
+    def _():
+        q_ref[...] = queries(normed_ref[...], wq_ref)
 
 
 def relay_kernel(s3_ref, r1_ref, r2_ref, s4_ref):
@@ -274,13 +291,10 @@
         mix_ref[n] = mix
 
 
-def log_weight_kernel(lw_ref, out_ref):
-    out_ref[...] = jnp.sum(jnp.where(to_class_order(lw_ref.shape[0]), lw_ref[...], 0.0), axis=0, keepdims=True)
-
-
-def output_kernel(mix_ref, w_ref, out_ref):
-    mixed = mix_ref[...].reshape(-1, out_ref.shape[0])
-    out_ref[...] = dot(mixed, w_ref[...], TN).astype(jnp.bfloat16)
+def output_kernel(mix_ref, w_ref, lw_ref, out_ref, log_weight_ref):
+    rows = out_ref.shape[0]
+    log_weight_ref[...] = jnp.sum(jnp.where(to_class_order(rows), lw_ref[...], 0.0), axis=0, keepdims=True)
+    out_ref[...] = dot(mix_ref[...].reshape(-1, rows), w_ref[...], TN).astype(jnp.bfloat16)
 
 
 VMEM = pl.BlockSpec(memory_space=pltpu.VMEM)
@@ -313,28 +327,32 @@
     bf16, f32 = jnp.bfloat16, jnp.float32
     sp = lax.axis_index("sp").reshape(1)
     slot = lax.axis_index("tp").reshape(1)
-    kv0, s1, s2, s3, normed = call(
+    kv0, s1, s2, s3, normed, q = call(
         project_kernel,
-        (in_hbm(tokens), in_hbm(norm_gain.reshape(1, -1)), in_hbm(w_key), in_hbm(w_value)),
+        (slot, in_hbm(tokens), in_hbm(norm_gain.reshape(1, -1)), in_hbm(w_key), in_hbm(w_value), in_hbm(w_query)),
         [
             ((rows, PAIR), bf16),
             ((STEPS + 2 * rows, PAIR), bf16),
             ((STEPS + rows, PAIR), bf16),
             ((rows, PAIR), bf16),
             ((rows, width), bf16),
+            ((rows, GROUPS * HEAD_DIM), bf16),
         ],
-        specs=[HBM] * 4,
+        specs=[SMEM] + [HBM] * 5,
         scratch=[
             pltpu.VMEM((rows, width), bf16),
             pltpu.VMEM((1, width), f32),
             pltpu.VMEM((GROUPS * PAIR, width), bf16),
-            pltpu.SemaphoreType.DMA((rows // CHUNK + 2 * GROUPS + 1,)),
+            pltpu.VMEM(w_query.shape, bf16),
+            pltpu.SemaphoreType.DMA((rows // CHUNK + 2 * GROUPS + 2,)),
         ],
     )
     r1 = from_behind(s1, 1)
     r2 = from_behind(s2, 2)
     r3 = from_behind(s3, 3)
-    (q,) = call(query_kernel, (normed, w_query), [((rows, GROUPS * HEAD_DIM), bf16)])
+    (q,) = call(
+        query_kernel, (slot, normed, w_query, q), [((rows, GROUPS * HEAD_DIM), bf16)], specs=[SMEM] + [VMEM] * 3
+    )
     (s4,) = call(relay_kernel, (s3, r1, r2), [((STEPS + 2 * rows, PAIR), bf16)])
     r4 = from_behind(s4, 4)
     o, l, e, top, total = call(
@@ -351,8 +369,9 @@
         specs=[SMEM] * 2 + [VMEM] * 11,
     )
     everyone = lax.all_to_all(mix, "tp", 0, 0, tiled=True)
-    (log_weight,) = call(log_weight_kernel, (lw,), [((1, rows), f32)])
-    (projected,) = call(output_kernel, (everyone, w_out), [((rows, w_out.shape[1]), bf16)])
+    projected, log_weight = call(
+        output_kernel, (everyone, w_out, lw), [((rows, w_out.shape[1]), bf16), ((1, rows), f32)]
+    )
     return projected, log_weight
 
 

time: 51.4 us -> 52 us (1.012)
  the two profiles are of different devices: /device:TPU:896 before, /device:TPU:768 now
where the time goes in v8:
time: 52 us; the launch traced here: 51.7 us
  waiting for transfers between devices  14.7 us (28%)
  blocking collectives  13 us (25%)
  starting transfers between devices  12.8 us (25%)
  Pallas kernels  9.48 us (18%)
  local copies, waits for them, and re-layouts  0.94 us (2%)
  between operations  0.75 us (1%)
    ppermute x4, waiting for transfers between devices, from_behind(): return lax.ppermute(value, 'sp', [(i, i + by) for i in range(devices - by)])  14.7 us
    all_to_all x1, blocking collectives, layer(): everyone = lax.all_to_all(mix, 'tp', 0, 0, tiled=True)  13 us
    ppermute x4, starting transfers between devices, from_behind(): return lax.ppermute(value, 'sp', [(i, i + by) for i in range(devices - by)])  12.8 us
    pallas_call x6, Pallas kernels, call(): pl.pallas_call(body, in_specs=specs or [VMEM] * len(operands), out_specs=...  9.48 us
  transfers between devices with their start and end apart: 4, of which 2 were waited for; matrix products, arithmetic and copies ran while one was open for 0% of the time, Pallas kernels for 6%

profile of v8, /device:TPU:768, one launch (start us, length us, event | category | flops | bytes accessed | tf_op | source)
XLA Modules:
  0.0 51.7 jit_solution(16839701926651232772)
XLA Ops:
  0.6 0.0 copy-start
  0.6 3.3 %shard_map.77 = (bf16[384,128]{1,0:T(8,128)(2,1)S(1)}, bf16[896,128]{1,0:T(8,128)(2,1)S(1)}, bf16[512,128]{1,0:T(8,128)(2,1)S(1)}, bf16[384,128]{1,0:T(8,128)(2,...) custom-call(s32[1]{0:T(128)} %bitcast.1.slot_ref, bf16[384,2048]{1,0:T(8,128)(2,1)} %tokens_hbm.1, ...), custom_call_target="tpu_custom_call" | custom-call | tf_op jit(solution)/shard_map/pallas_call | solution.py:306
  4.0 0.0 copy-start.2
  4.0 3.5 %collective-permute-start = (bf16[896,128]{1,0:T(8,128)(2,1)S(1)}, bf16[896,128]{1,0:T(8,128)(2,1)S(1)}, u32[]{:S(2)}, u32[]{:S(2)}) collective-permute-start(bf16[896,128]{1,0:T(8,128)(2,1)S(1)} %get-tuple-element.18.s1_ref), channel_id=1, source_target_pairs={{0,8},{8,16},{16,24},{24,32},{32,40},{40,48},{48,56},{56,64},{64,7... | collective-permute-start | bytes 688136 | tf_op jit(solution)/shard_map/ppermute | solution.py:322
  7.5 4.8 %collective-permute-start.1 = (bf16[512,128]{1,0:T(8,128)(2,1)S(1)}, bf16[512,128]{1,0:T(8,128)(2,1)S(1)}, u32[]{:S(2)}, u32[]{:S(2)}) collective-permute-start(bf16[512,128]{1,0:T(8,128)(2,1)S(1)} %get-tuple-element.19), channel_id=1, source_target_pairs={{0,16},{8,24},{16,32},{24,40},{32,48},{40,56},{48,64},{56,72},{64,... | collective-permute-start | bytes 393224 | tf_op jit(solution)/shard_map/ppermute | solution.py:322
  12.3 8.0 %collective-permute-done.1.r2_ref = bf16[512,128]{1,0:T(8,128)(2,1)S(1)} collective-permute-done((bf16[512,128]{1,0:T(8,128)(2,1)S(1)}, bf16[512,128]{1,0:T(8,128)(2,1)S(1)}, u32[]{:S(2)}, u32[]{:S(2)}) %collective-permute-start.1) | collective-permute-done | bytes 131104 | tf_op jit(solution)/shard_map/ppermute | solution.py:322
  20.3 0.0 collective-permute-done.r1_ref
  20.3 0.7 %shard_map.79 = bf16[896,128]{1,0:T(8,128)(2,1)} custom-call(bf16[384,128]{1,0:T(8,128)(2,1)S(1)} %get-tuple-element.17.s3_ref, bf16[896,128]{1,0:T(8,128)(2,1)S(1)} %collective-permute-done.r1_ref, bf16[512,128]{1,0:T(8,128)(2,1)S(1)} %collective-permute-done.1.r2_ref), custom_call_target="tpu_custom_call" | custom-call | tf_op jit(solution)/shard_map/pallas_call | solution.py:306
  21.0 0.0 copy-done.2
  21.0 1.9 %collective-permute-start.3 = (bf16[896,128]{1,0:T(8,128)(2,1)}, bf16[896,128]{1,0:T(8,128)(2,1)S(1)}, u32[]{:S(2)}, u32[]{:S(2)}) collective-permute-start(bf16[896,128]{1,0:T(8,128)(2,1)} %shard_map.79), channel_id=1, source_target_pairs={{0,32},{8,40},{16,48},{24,56},{32,64},{40,72},{48,80},{56,88},{64,... | collective-permute-start | bytes 688136 | tf_op jit(solution)/shard_map/ppermute | solution.py:322
  22.9 2.6 %collective-permute-start.2 = (bf16[384,128]{1,0:T(8,128)(2,1)S(1)}, bf16[384,128]{1,0:T(8,128)(2,1)S(1)}, u32[]{:S(2)}, u32[]{:S(2)}) collective-permute-start(bf16[384,128]{1,0:T(8,128)(2,1)S(1)} %get-tuple-element.17.s3_ref), channel_id=1, source_target_pairs={{0,24},{8,32},{16,40},{24,48},{32,56},{40,64},{48,72},{56,80},{64,... | collective-permute-start | bytes 294920 | tf_op jit(solution)/shard_map/ppermute | solution.py:322
  25.6 0.0 copy-done
  25.6 0.0 copy-start.3
  25.6 0.9 %copy-done.3 = bf16[384,192]{1,0:T(8,128)(2,1)S(1)} copy-done((bf16[384,192]{1,0:T(8,128)(2,1)S(1)}, bf16[384,192]{1,0:T(8,128)(2,1)}, u32[]{:S(2)}) %copy-start.3) | copy-done | bytes 147480
  26.5 1.0 %shard_map.78.q_ref = bf16[384,192]{1,0:T(8,128)(2,1)S(1)} custom-call(s32[1]{0:T(128)} %bitcast.1.slot_ref, bf16[384,2048]{1,0:T(8,128)(2,1)S(1)} %get-tuple-element.15.normed_ref, bf16[3,64,2048]{2,1,0:T(8,128)(2,1)S(1)} %copy-done, bf16[384,192]{1,0:T(8,128)(2,1)S(1)} %copy-done.3), custom_call_target="tpu_custom_call" | custom-call | tf_op jit(solution)/shard_map/pallas_call | solution.py:306
  27.5 6.7 %collective-permute-done.2.r3_ref = bf16[384,128]{1,0:T(8,128)(2,1)S(1)} collective-permute-done((bf16[384,128]{1,0:T(8,128)(2,1)S(1)}, bf16[384,128]{1,0:T(8,128)(2,1)S(1)}, u32[]{:S(2)}, u32[]{:S(2)}) %collective-permute-start.2) | collective-permute-done | bytes 98336 | tf_op jit(solution)/shard_map/ppermute | solution.py:322
  34.2 2.3 %shard_map.80 = (f32[384,64]{1,0:T(8,128)S(1)}, f32[384,1]{1,0:T(8,128)S(1)}, f32[384,384]{1,0:T(8,128)S(1)}, f32[384,1]{1,0:T(8,128)S(1)}, f32[384,1]{1,0:T(8,128)S(1)}) custom-call(s32[1]{0:T(128)} %bitcast.sp_ref, s32[1]{0:T(128)} %bitcast.1.slot_ref, bf16[384,192]{1,0:T(8,128)(2,1)S(1)} %shard_map.78.q_ref, ...), custom_call_target="tpu_custom_call" | custom-call | tf_op jit(solution)/shard_map/pallas_call | solution.py:306
  36.5 0.0 collective-permute-done.3.r4_ref
  36.5 0.0 copy-start.1
  36.6 1.1 %shard_map.81 = (bf16[8,64,384]{2,1,0:T(8,128)(2,1)S(1)}, f32[384,1]{1,0:T(8,128)S(1)}) custom-call(s32[1]{0:T(128)} %bitcast.sp_ref, s32[1]{0:T(128)} %bitcast.1.slot_ref, bf16[384,192]{1,0:T(8,128)(2,1)S(1)} %shard_map.78.q_ref, bf16[384,128]{1,0:T(8,128)(2,1)S(1)} %get-tuple-element.17.s3_ref, bf16[896,128]{1,0:T(8,128)(2,1)S(1)} %collective-permute-done.r1_ref, ...), custom_call_target="tpu_custom_call" | custom-call | tf_op jit(solution)/shard_map/pallas_call | solution.py:306
  37.7 13.0 %all_to_all.5.mix_ref = bf16[8,64,384]{2,1,0:T(8,128)(2,1)S(1)} all-to-all(bf16[8,64,384]{2,1,0:T(8,128)(2,1)S(1)} %get-tuple-element.26), channel_id=1, replica_groups=mesh['sp'=128,'tp'=8] {'tp'}, dimensions={0} | all-to-all | bytes 786432 | tf_op jit(solution)/shard_map/all_to_all | solution.py:371
  50.7 0.0 copy-done.1
  50.7 1.0 %shard_map.82 = (bf16[384,256]{1,0:T(8,128)(2,1)}, f32[1,384]{1,0:T(1,128)}) custom-call(bf16[8,64,384]{2,1,0:T(8,128)(2,1)S(1)} %all_to_all.5.mix_ref, bf16[512,256]{1,0:T(8,128)(2,1)S(1)} %copy-done.1, f32[384,1]{1,0:T(8,128)S(1)} %get-tuple-element.27.lw_ref), custom_call_target="tpu_custom_call" | custom-call | tf_op jit(solution)/shard_map/pallas_call | solution.py:306
Async XLA Ops:
  0.6 24.9 %copy-start = (bf16[3,64,2048]{2,1,0:T(8,128)(2,1)S(1)}, bf16[3,64,2048]{2,1,0:T(8,128)(2,1)}, u32[]{:S(2)}) copy-start(bf16[3,64,2048]{2,1,0:T(8,128)(2,1)} %wq_ref.1) | copy-start | bytes 2359300
  4.0 17.1 %copy-start.2 = (bf16[384,192]{1,0:T(8,128)(2,1)}, bf16[384,192]{1,0:T(8,128)(2,1)S(1)}, u32[]{:S(2)}) copy-start(bf16[384,192]{1,0:T(8,128)(2,1)S(1)} %get-tuple-element.16.done_ref) | copy-start | bytes 442372
  4.0 16.3 %collective-permute-start = (bf16[896,128]{1,0:T(8,128)(2,1)S(1)}, bf16[896,128]{1,0:T(8,128)(2,1)S(1)}, u32[]{:S(2)}, u32[]{:S(2)}) collective-permute-start(bf16[896,128]{1,0:T(8,128)(2,1)S(1)} %get-tuple-element.18.s1_ref), channel_id=1, source_target_pairs={{0,8},{8,16},{16,24},{24,32},{32,40},{40,48},{48,56},{56,64},{64,7... | collective-permute-start | bytes 688136 | tf_op jit(solution)/shard_map/ppermute | solution.py:322
  7.5 12.8 %collective-permute-start.1 = (bf16[512,128]{1,0:T(8,128)(2,1)S(1)}, bf16[512,128]{1,0:T(8,128)(2,1)S(1)}, u32[]{:S(2)}, u32[]{:S(2)}) collective-permute-start(bf16[512,128]{1,0:T(8,128)(2,1)S(1)} %get-tuple-element.19), channel_id=1, source_target_pairs={{0,16},{8,24},{16,32},{24,40},{32,48},{40,56},{48,64},{56,72},{64,... | collective-permute-start | bytes 393224 | tf_op jit(solution)/shard_map/ppermute | solution.py:322
  21.0 15.5 %collective-permute-start.3 = (bf16[896,128]{1,0:T(8,128)(2,1)}, bf16[896,128]{1,0:T(8,128)(2,1)S(1)}, u32[]{:S(2)}, u32[]{:S(2)}) collective-permute-start(bf16[896,128]{1,0:T(8,128)(2,1)} %shard_map.79), channel_id=1, source_target_pairs={{0,32},{8,40},{16,48},{24,56},{32,64},{40,72},{48,80},{56,88},{64,... | collective-permute-start | bytes 688136 | tf_op jit(solution)/shard_map/ppermute | solution.py:322
  22.9 11.3 %collective-permute-start.2 = (bf16[384,128]{1,0:T(8,128)(2,1)S(1)}, bf16[384,128]{1,0:T(8,128)(2,1)S(1)}, u32[]{:S(2)}, u32[]{:S(2)}) collective-permute-start(bf16[384,128]{1,0:T(8,128)(2,1)S(1)} %get-tuple-element.17.s3_ref), channel_id=1, source_target_pairs={{0,24},{8,32},{16,40},{24,48},{32,56},{40,64},{48,72},{56,80},{64,... | collective-permute-start | bytes 294920 | tf_op jit(solution)/shard_map/ppermute | solution.py:322
  25.6 0.9 %copy-start.3 = (bf16[384,192]{1,0:T(8,128)(2,1)S(1)}, bf16[384,192]{1,0:T(8,128)(2,1)}, u32[]{:S(2)}) copy-start(bf16[384,192]{1,0:T(8,128)(2,1)} %copy-done.2) | copy-start | bytes 442372
  36.5 14.2 %copy-start.1 = (bf16[512,256]{1,0:T(8,128)(2,1)S(1)}, bf16[512,256]{1,0:T(8,128)(2,1)}, u32[]{:S(2)}) copy-start(bf16[512,256]{1,0:T(8,128)(2,1)} %w_ref.1) | copy-start | bytes 786436

commit v9 on v7

--- a/solution.py
+++ b/solution.py
@@ -274,13 +274,10 @@
         mix_ref[n] = mix
 
 
-def log_weight_kernel(lw_ref, out_ref):
-    out_ref[...] = jnp.sum(jnp.where(to_class_order(lw_ref.shape[0]), lw_ref[...], 0.0), axis=0, keepdims=True)
-
-
-def output_kernel(mix_ref, w_ref, out_ref):
-    mixed = mix_ref[...].reshape(-1, out_ref.shape[0])
-    out_ref[...] = dot(mixed, w_ref[...], TN).astype(jnp.bfloat16)
+def output_kernel(mix_ref, w_ref, lw_ref, out_ref, log_weight_ref):
+    rows = out_ref.shape[0]
+    log_weight_ref[...] = jnp.sum(jnp.where(to_class_order(rows), lw_ref[...], 0.0), axis=0, keepdims=True)
+    out_ref[...] = dot(mix_ref[...].reshape(-1, rows), w_ref[...], TN).astype(jnp.bfloat16)
 
 
 VMEM = pl.BlockSpec(memory_space=pltpu.VMEM)
@@ -351,8 +348,9 @@
         specs=[SMEM] * 2 + [VMEM] * 11,
     )
     everyone = lax.all_to_all(mix, "tp", 0, 0, tiled=True)
-    (log_weight,) = call(log_weight_kernel, (lw,), [((1, rows), f32)])
-    (projected,) = call(output_kernel, (everyone, w_out), [((rows, w_out.shape[1]), bf16)])
+    projected, log_weight = call(
+        output_kernel, (everyone, w_out, lw), [((rows, w_out.shape[1]), bf16), ((1, rows), f32)]
+    )
     return projected, log_weight
 
 

time: 51.4 us -> 50.4 us (0.981)
  blocking collectives: 0 us -> 13 us
  waiting for transfers between devices: 22.3 us -> 14.1 us
  starting transfers between devices: 17.1 us -> 12.8 us
  Pallas kernels: 10.9 us -> 9.47 us
    all_to_all x0 -> x1, blocking collectives: none -> 13 us  [layer(): everyone = lax.all_to_all(mix, 'tp', 0, 0, tiled=True)]
    all_to_all x1 -> x0, waiting for transfers between devices: 8.15 us -> none  [layer(): everyone = lax.all_to_all(mix, 'tp', 0, 0, tiled=True)]
    all_to_all x1 -> x0, starting transfers between devices: 4.3 us -> none  [layer(): everyone = lax.all_to_all(mix, 'tp', 0, 0, tiled=True)]
    pallas_call x7 -> x6, Pallas kernels: 10.9 us -> 9.47 us  [call(): pl.pallas_call(body, in_specs=specs or [VMEM] * len(operands), out_specs=...]
  transfers between devices with their start and end apart: 5 -> 4, of which waited for: 3 -> 2; matrix products, arithmetic and copies ran while one was open for 0% -> 0% of each run, Pallas kernels for 8% -> 7%
where the time goes in v9:
time: 50.4 us; the launch traced here: 50.2 us
  waiting for transfers between devices  14.1 us (28%)
  blocking collectives  13 us (26%)
  starting transfers between devices  12.8 us (25%)
  Pallas kernels  9.47 us (19%)
  between operations  0.73 us (1%)
    ppermute x4, waiting for transfers between devices, from_behind(): return lax.ppermute(value, 'sp', [(i, i + by) for i in range(devices - by)])  14.1 us
    all_to_all x1, blocking collectives, layer(): everyone = lax.all_to_all(mix, 'tp', 0, 0, tiled=True)  13 us
    ppermute x4, starting transfers between devices, from_behind(): return lax.ppermute(value, 'sp', [(i, i + by) for i in range(devices - by)])  12.8 us
    pallas_call x6, Pallas kernels, call(): pl.pallas_call(body, in_specs=specs or [VMEM] * len(operands), out_specs=...  9.47 us
  transfers between devices with their start and end apart: 4, of which 2 were waited for; matrix products, arithmetic and copies ran while one was open for 0% of the time, Pallas kernels for 7%

profile of v9, /device:TPU:896, one launch (start us, length us, event | category | flops | bytes accessed | tf_op | source)
XLA Modules:
  0.0 50.2 jit_solution(14747351397132518764)
XLA Ops:
  0.6 0.0 copy-start
  0.6 3.3 %shard_map.77 = (bf16[384,128]{1,0:T(8,128)(2,1)S(1)}, bf16[896,128]{1,0:T(8,128)(2,1)S(1)}, bf16[512,128]{1,0:T(8,128)(2,1)S(1)}, bf16[384,128]{1,0:T(8,128)(2,1)S(1)}, bf16[384,2048]{1,0:T(8,128)(2,1)S(1)}) custom-call(bf16[384,2048]{1,0:T(8,128)(2,1)} %tokens_hbm.1, f32[1,2048]{1,0:T(1,128)} %bitcast.3, bf16[3,64,2048]{2,1,0:T(8,128)(2,1)} %wk_hbm.1, ...), custom_call_target="tpu_custom_call" | custom-call | tf_op jit(solution)/shard_map/pallas_call | solution.py:289
  3.9 3.5 %collective-permute-start = (bf16[896,128]{1,0:T(8,128)(2,1)S(1)}, bf16[896,128]{1,0:T(8,128)(2,1)S(1)}, u32[]{:S(2)}, u32[]{:S(2)}) collective-permute-start(bf16[896,128]{1,0:T(8,128)(2,1)S(1)} %get-tuple-element.16.s1_ref), channel_id=1, source_target_pairs={{0,8},{8,16},{16,24},{24,32},{32,40},{40,48},{48,56},{56,64},{64,7... | collective-permute-start | bytes 688136 | tf_op jit(solution)/shard_map/ppermute | solution.py:305
  7.4 4.8 %collective-permute-start.1 = (bf16[512,128]{1,0:T(8,128)(2,1)S(1)}, bf16[512,128]{1,0:T(8,128)(2,1)S(1)}, u32[]{:S(2)}, u32[]{:S(2)}) collective-permute-start(bf16[512,128]{1,0:T(8,128)(2,1)S(1)} %get-tuple-element.17), channel_id=1, source_target_pairs={{0,16},{8,24},{16,32},{24,40},{32,48},{40,56},{48,64},{56,72},{64,... | collective-permute-start | bytes 393224 | tf_op jit(solution)/shard_map/ppermute | solution.py:305
  12.3 7.1 %collective-permute-done.1.r2_ref = bf16[512,128]{1,0:T(8,128)(2,1)S(1)} collective-permute-done((bf16[512,128]{1,0:T(8,128)(2,1)S(1)}, bf16[512,128]{1,0:T(8,128)(2,1)S(1)}, u32[]{:S(2)}, u32[]{:S(2)}) %collective-permute-start.1) | collective-permute-done | bytes 131104 | tf_op jit(solution)/shard_map/ppermute | solution.py:305
  19.3 0.0 collective-permute-done.r1_ref
  19.3 0.7 %shard_map.79 = bf16[896,128]{1,0:T(8,128)(2,1)} custom-call(bf16[384,128]{1,0:T(8,128)(2,1)S(1)} %get-tuple-element.15.s3_ref, bf16[896,128]{1,0:T(8,128)(2,1)S(1)} %collective-permute-done.r1_ref, bf16[512,128]{1,0:T(8,128)(2,1)S(1)} %collective-permute-done.1.r2_ref), custom_call_target="tpu_custom_call" | custom-call | tf_op jit(solution)/shard_map/pallas_call | solution.py:289
  20.0 1.9 %collective-permute-start.3 = (bf16[896,128]{1,0:T(8,128)(2,1)}, bf16[896,128]{1,0:T(8,128)(2,1)S(1)}, u32[]{:S(2)}, u32[]{:S(2)}) collective-permute-start(bf16[896,128]{1,0:T(8,128)(2,1)} %shard_map.79), channel_id=1, source_target_pairs={{0,32},{8,40},{16,48},{24,56},{32,64},{40,72},{48,80},{56,88},{64,... | collective-permute-start | bytes 688136 | tf_op jit(solution)/shard_map/ppermute | solution.py:305
  21.9 2.6 %collective-permute-start.2 = (bf16[384,128]{1,0:T(8,128)(2,1)S(1)}, bf16[384,128]{1,0:T(8,128)(2,1)S(1)}, u32[]{:S(2)}, u32[]{:S(2)}) collective-permute-start(bf16[384,128]{1,0:T(8,128)(2,1)S(1)} %get-tuple-element.15.s3_ref), channel_id=1, source_target_pairs={{0,24},{8,32},{16,40},{24,48},{32,56},{40,64},{48,72},{56,80},{64,... | collective-permute-start | bytes 294920 | tf_op jit(solution)/shard_map/ppermute | solution.py:305
  24.5 0.0 copy-done
  24.6 1.0 %shard_map.78.q_ref = bf16[384,192]{1,0:T(8,128)(2,1)S(1)} custom-call(bf16[384,2048]{1,0:T(8,128)(2,1)S(1)} %get-tuple-element.14.normed_ref, bf16[3,64,2048]{2,1,0:T(8,128)(2,1)S(1)} %copy-done), custom_call_target="tpu_custom_call" | custom-call | tf_op jit(solution)/shard_map/pallas_call | solution.py:289
  25.5 7.1 %collective-permute-done.2.r3_ref = bf16[384,128]{1,0:T(8,128)(2,1)S(1)} collective-permute-done((bf16[384,128]{1,0:T(8,128)(2,1)S(1)}, bf16[384,128]{1,0:T(8,128)(2,1)S(1)}, u32[]{:S(2)}, u32[]{:S(2)}) %collective-permute-start.2) | collective-permute-done | bytes 98336 | tf_op jit(solution)/shard_map/ppermute | solution.py:305
  32.6 2.3 %shard_map.80 = (f32[384,64]{1,0:T(8,128)S(1)}, f32[384,1]{1,0:T(8,128)S(1)}, f32[384,384]{1,0:T(8,128)S(1)}, f32[384,1]{1,0:T(8,128)S(1)}, f32[384,1]{1,0:T(8,128)S(1)}) custom-call(s32[1]{0:T(128)} %bitcast.sp_ref, s32[1]{0:T(128)} %bitcast.1.slot_ref, bf16[384,192]{1,0:T(8,128)(2,1)S(1)} %shard_map.78.q_ref, ...), custom_call_target="tpu_custom_call" | custom-call | tf_op jit(solution)/shard_map/pallas_call | solution.py:289
  34.9 0.0 collective-permute-done.3.r4_ref
  35.0 0.0 copy-start.1
  35.0 1.1 %shard_map.81 = (bf16[8,64,384]{2,1,0:T(8,128)(2,1)S(1)}, f32[384,1]{1,0:T(8,128)S(1)}) custom-call(s32[1]{0:T(128)} %bitcast.sp_ref, s32[1]{0:T(128)} %bitcast.1.slot_ref, bf16[384,192]{1,0:T(8,128)(2,1)S(1)} %shard_map.78.q_ref, bf16[384,128]{1,0:T(8,128)(2,1)S(1)} %get-tuple-element.15.s3_ref, bf16[896,128]{1,0:T(8,128)(2,1)S(1)} %collective-permute-done.r1_ref, ...), custom_call_target="tpu_custom_call" | custom-call | tf_op jit(solution)/shard_map/pallas_call | solution.py:289
  36.1 13.0 %all_to_all.5.mix_ref = bf16[8,64,384]{2,1,0:T(8,128)(2,1)S(1)} all-to-all(bf16[8,64,384]{2,1,0:T(8,128)(2,1)S(1)} %get-tuple-element.24), channel_id=1, replica_groups=mesh['sp'=128,'tp'=8] {'tp'}, dimensions={0} | all-to-all | bytes 786432 | tf_op jit(solution)/shard_map/all_to_all | solution.py:350
  49.1 0.0 copy-done.1
  49.1 1.0 %shard_map.82 = (bf16[384,256]{1,0:T(8,128)(2,1)}, f32[1,384]{1,0:T(1,128)}) custom-call(bf16[8,64,384]{2,1,0:T(8,128)(2,1)S(1)} %all_to_all.5.mix_ref, bf16[512,256]{1,0:T(8,128)(2,1)S(1)} %copy-done.1, f32[384,1]{1,0:T(8,128)S(1)} %get-tuple-element.25.lw_ref), custom_call_target="tpu_custom_call" | custom-call | tf_op jit(solution)/shard_map/pallas_call | solution.py:289
Async XLA Ops:
  0.6 23.9 %copy-start = (bf16[3,64,2048]{2,1,0:T(8,128)(2,1)S(1)}, bf16[3,64,2048]{2,1,0:T(8,128)(2,1)}, u32[]{:S(2)}) copy-start(bf16[3,64,2048]{2,1,0:T(8,128)(2,1)} %wq_ref.1) | copy-start | bytes 2359300
  3.9 15.4 %collective-permute-start = (bf16[896,128]{1,0:T(8,128)(2,1)S(1)}, bf16[896,128]{1,0:T(8,128)(2,1)S(1)}, u32[]{:S(2)}, u32[]{:S(2)}) collective-permute-start(bf16[896,128]{1,0:T(8,128)(2,1)S(1)} %get-tuple-element.16.s1_ref), channel_id=1, source_target_pairs={{0,8},{8,16},{16,24},{24,32},{32,40},{40,48},{48,56},{56,64},{64,7... | collective-permute-start | bytes 688136 | tf_op jit(solution)/shard_map/ppermute | solution.py:305
  7.4 11.9 %collective-permute-start.1 = (bf16[512,128]{1,0:T(8,128)(2,1)S(1)}, bf16[512,128]{1,0:T(8,128)(2,1)S(1)}, u32[]{:S(2)}, u32[]{:S(2)}) collective-permute-start(bf16[512,128]{1,0:T(8,128)(2,1)S(1)} %get-tuple-element.17), channel_id=1, source_target_pairs={{0,16},{8,24},{16,32},{24,40},{32,48},{40,56},{48,64},{56,72},{64,... | collective-permute-start | bytes 393224 | tf_op jit(solution)/shard_map/ppermute | solution.py:305
  20.0 14.9 %collective-permute-start.3 = (bf16[896,128]{1,0:T(8,128)(2,1)}, bf16[896,128]{1,0:T(8,128)(2,1)S(1)}, u32[]{:S(2)}, u32[]{:S(2)}) collective-permute-start(bf16[896,128]{1,0:T(8,128)(2,1)} %shard_map.79), channel_id=1, source_target_pairs={{0,32},{8,40},{16,48},{24,56},{32,64},{40,72},{48,80},{56,88},{64,... | collective-permute-start | bytes 688136 | tf_op jit(solution)/shard_map/ppermute | solution.py:305
  21.9 10.7 %collective-permute-start.2 = (bf16[384,128]{1,0:T(8,128)(2,1)S(1)}, bf16[384,128]{1,0:T(8,128)(2,1)S(1)}, u32[]{:S(2)}, u32[]{:S(2)}) collective-permute-start(bf16[384,128]{1,0:T(8,128)(2,1)S(1)} %get-tuple-element.15.s3_ref), channel_id=1, source_target_pairs={{0,24},{8,32},{16,40},{24,48},{32,56},{40,64},{48,72},{56,80},{64,... | collective-permute-start | bytes 294920 | tf_op jit(solution)/shard_map/ppermute | solution.py:305
  35.0 14.2 %copy-start.1 = (bf16[512,256]{1,0:T(8,128)(2,1)S(1)}, bf16[512,256]{1,0:T(8,128)(2,1)}, u32[]{:S(2)}) copy-start(bf16[512,256]{1,0:T(8,128)(2,1)} %w_ref.1) | copy-start | bytes 786436

commit v10 on v5

--- a/solution.py
+++ b/solution.py
@@ -122,9 +122,11 @@
     return jnp.exp2(-8.0 * n.astype(jnp.float32) / (GROUPS * SLOTS))
 
 
-def bias_of(distance, valid, slope):
-    ok = valid & (distance >= 0) & (distance <= STEPS)
-    return jnp.where(ok, -slope * distance.astype(jnp.float32), NEG_BIG)
+def bias_of(at_query, at_key, valid, slope, same=None):
+    at_key = jnp.where(valid, at_key.astype(jnp.float32), 1e9)
+    distance = at_query.astype(jnp.float32) - at_key
+    ok = jnp.abs(distance - STEPS / 2) <= STEPS / 2
+    return jnp.where(ok if same is None else ok & same, -slope * distance, NEG_BIG)
 
 
 def softmax_pieces(scores):
@@ -150,7 +152,7 @@
         ok.append(jnp.full_like(jh, halo_block) <= sp)
     js, at = jnp.concatenate(js, axis=1), jnp.concatenate(at, axis=1)
     ok = jnp.concatenate([o.astype(jnp.int32) for o in ok], axis=1) > 0
-    return bias_of(iq - at, (jq == js) & ok, slope)
+    return bias_of(iq, at, ok, slope, jq == js)
 
 
 def early_kernel(
@@ -164,7 +166,7 @@
     jh, ih = run_of_halo(per_residue, 1)
     tail = jnp.concatenate([16 * ih + 4 * jh + c - rows for c in range(CLASSES)], axis=1)
     tk = jnp.concatenate([positions(rows, 1), tail], axis=1)
-    bias = bias_of(positions(rows, 0) - tk, (tk >= 0) | (sp >= 1), slope_of(0, slot))
+    bias = bias_of(positions(rows, 0), tk, (tk >= 0) | (sp >= 1), slope_of(0, slot))
     keys = jnp.concatenate([kv0_ref[...], r1_ref[0:STEPS, :]], axis=0)
     p, l0 = softmax_pieces(dot(q_ref[:, 0:HEAD_DIM], keys[:, 0:HEAD_DIM], NT) + bias)
     o0 = dot(p, keys[:, HEAD_DIM:PAIR], NN)
@@ -173,7 +175,7 @@
     own = 4 * ik + jk
     tk = jnp.concatenate([own, own - per_class, 4 * ih + jh - 2 * per_class], axis=1)
     block = jnp.concatenate([jnp.zeros_like(own), jnp.full_like(own, 1), jnp.full_like(jh, 2)], axis=1)
-    bias = bias_of(4 * iq + jq - tk, block <= sp, slope_of(1, slot))
+    bias = bias_of(4 * iq + jq, tk, block <= sp, slope_of(1, slot))
     halo = STEPS // CLASSES
     keys = [
         jnp.concatenate(
@@ -269,19 +271,19 @@
     top = jnp.maximum(l01, l2)
     w01, w2 = jnp.exp(l01 - top), jnp.exp(l2 - top)
     both = w01 + w2
-    lw = top + jnp.log(both)
+    lw_ref[...] = top + jnp.log(both)
     both = 1.0 / both
     mixed = ((w01 * both) * o_ref[...] + (w2 * both) * jnp.concatenate(out, axis=0)).astype(jnp.bfloat16)
     pick = to_class_order(rows)
     mix = dot(mixed, pick.astype(jnp.bfloat16), TN).astype(jnp.bfloat16)
     for n in range(mix_ref.shape[0]):
         mix_ref[n] = mix
-    lw_ref[...] = jnp.sum(jnp.where(pick, lw, 0.0), axis=0, keepdims=True)
-
-
-def output_kernel(mix_ref, w_ref, out_ref):
-    mixed = mix_ref[...].reshape(-1, out_ref.shape[0])
-    out_ref[...] = dot(mixed, w_ref[...], TN).astype(jnp.bfloat16)
+
+
+def output_kernel(mix_ref, w_ref, lw_ref, out_ref, log_weight_ref):
+    rows = out_ref.shape[0]
+    log_weight_ref[...] = jnp.sum(jnp.where(to_class_order(rows), lw_ref[...], 0.0), axis=0, keepdims=True)
+    out_ref[...] = dot(mix_ref[...].reshape(-1, rows), w_ref[...], TN).astype(jnp.bfloat16)
 
 
 VMEM = pl.BlockSpec(memory_space=pltpu.VMEM)
@@ -346,14 +348,16 @@
         specs=[SMEM] * 2 + [VMEM] * 8,
     )
     devices = lax.axis_size("tp")
-    mix, log_weight = call(
+    mix, lw = call(
         late_kernel,
         (sp, slot, q, s3, r1, r2, r3, r4, far, o, l, e, top, total),
-        [((devices, HEAD_DIM, rows), bf16), ((1, rows), f32)],
+        [((devices, HEAD_DIM, rows), bf16), ((rows, 1), f32)],
         specs=[SMEM] * 2 + [VMEM] * 12,
     )
     everyone = lax.all_to_all(mix, "tp", 0, 0, tiled=True)
-    (projected,) = call(output_kernel, (everyone, w_out), [((rows, w_out.shape[1]), bf16)])
+    projected, log_weight = call(
+        output_kernel, (everyone, w_out, lw), [((rows, w_out.shape[1]), bf16), ((1, rows), f32)]
+    )
     return projected, log_weight
 
 

time: 54.9 us -> 54.2 us (0.987)
  the two profiles are of different devices: /device:TPU:320 before, /device:TPU:64 now
where the time goes in v10:
time: 54.2 us; the launch traced here: 54 us
  starting transfers between devices  20.3 us (37%)
  blocking collectives  13 us (24%)
  waiting for transfers between devices  10.3 us (19%)
  Pallas kernels  8.94 us (16%)
  between operations  0.77 us (1%)
  local copies, waits for them, and re-layouts  0.65 us (1%)
    ppermute x5, starting transfers between devices, from_behind(): return lax.ppermute(value, 'sp', [(i, i + by) for i in range(devices - by)])  20.3 us
    all_to_all x1, blocking collectives, layer(): everyone = lax.all_to_all(mix, 'tp', 0, 0, tiled=True)  13 us
    ppermute x5, waiting for transfers between devices, from_behind(): return lax.ppermute(value, 'sp', [(i, i + by) for i in range(devices - by)])  10.3 us
    pallas_call x6, Pallas kernels, call(): pl.pallas_call(body, in_specs=specs or [VMEM] * len(operands), out_specs=...  8.94 us
  transfers between devices with their start and end apart: 5, of which 2 were waited for; matrix products, arithmetic and copies ran while one was open for 0% of the time, Pallas kernels for 7%

profile of v10, /device:TPU:64, one launch (start us, length us, event | category | flops | bytes accessed | tf_op | source)
XLA Modules:
  0.0 54.0 jit_solution(2116802596612606191)
XLA Ops:
  0.6 0.0 copy-start
  0.6 3.3 %shard_map.77 = (bf16[384,128]{1,0:T(8,128)(2,1)S(1)}, bf16[896,128]{1,0:T(8,128)(2,1)S(1)}, bf16[512,128]{1,0:T(8,128)(2,1)S(1)}, bf16[384,128]{1,0:T(8,128)(2,1)S(1)}, bf16[384,2048]{1,0:T(8,128)(2,1)S(1)}) custom-call(bf16[384,2048]{1,0:T(8,128)(2,1)} %tokens_hbm.1, f32[1,2048]{1,0:T(1,128)} %bitcast.3, bf16[3,64,2048]{2,1,0:T(8,128)(2,1)} %wk_hbm.1, ...), custom_call_target="tpu_custom_call" | custom-call | tf_op jit(solution)/shard_map/pallas_call | solution.py:295
  3.9 0.0 copy-start.2
  3.9 0.6 %copy-done.2 = bf16[384,128]{1,0:T(8,128)(2,1)} copy-done((bf16[384,128]{1,0:T(8,128)(2,1)}, bf16[384,128]{1,0:T(8,128)(2,1)S(1)}, u32[]{:S(2)}) %copy-start.2) | copy-done | bytes 98328
  4.6 3.5 %collective-permute-start = (bf16[896,128]{1,0:T(8,128)(2,1)S(1)}, bf16[896,128]{1,0:T(8,128)(2,1)S(1)}, u32[]{:S(2)}, u32[]{:S(2)}) collective-permute-start(bf16[896,128]{1,0:T(8,128)(2,1)S(1)} %get-tuple-element.16.s1_ref), channel_id=1, source_target_pairs={{0,8},{8,16},{16,24},{24,32},{32,40},{40,48},{48,56},{56,64},{64,7... | collective-permute-start | bytes 688136 | tf_op jit(solution)/shard_map/ppermute | solution.py:311
  8.1 4.8 %collective-permute-start.1 = (bf16[512,128]{1,0:T(8,128)(2,1)S(1)}, bf16[512,128]{1,0:T(8,128)(2,1)S(1)}, u32[]{:S(2)}, u32[]{:S(2)}) collective-permute-start(bf16[512,128]{1,0:T(8,128)(2,1)S(1)} %get-tuple-element.17), channel_id=1, source_target_pairs={{0,16},{8,24},{16,32},{24,40},{32,48},{40,56},{48,64},{56,72},{64,... | collective-permute-start | bytes 393224 | tf_op jit(solution)/shard_map/ppermute | solution.py:311
  12.9 5.8 %collective-permute-done.1.r2_ref = bf16[512,128]{1,0:T(8,128)(2,1)S(1)} collective-permute-done((bf16[512,128]{1,0:T(8,128)(2,1)S(1)}, bf16[512,128]{1,0:T(8,128)(2,1)S(1)}, u32[]{:S(2)}, u32[]{:S(2)}) %collective-permute-start.1) | collective-permute-done | bytes 131104 | tf_op jit(solution)/shard_map/ppermute | solution.py:311
  18.7 0.0 collective-permute-done.r1_ref
  18.7 3.8 %collective-permute-start.4 = (bf16[512,128]{1,0:T(8,128)(2,1)S(1)}, bf16[512,128]{1,0:T(8,128)(2,1)S(1)}, u32[]{:S(2)}, u32[]{:S(2)}) collective-permute-start(bf16[512,128]{1,0:T(8,128)(2,1)S(1)} %shard_map.79), channel_id=1, source_target_pairs={{0,32},{8,40},{16,48},{24,56},{32,64},{40,72},{48,80},{56,88},{64,... | collective-permute-start | bytes 393224 | tf_op jit(solution)/shard_map/ppermute | solution.py:311
  22.6 6.3 %collective-permute-start.3 = (bf16[384,128]{1,0:T(8,128)(2,1)S(1)}, bf16[384,128]{1,0:T(8,128)(2,1)S(1)}, u32[]{:S(2)}, u32[]{:S(2)}) collective-permute-start(bf16[384,128]{1,0:T(8,128)(2,1)S(1)} %get-tuple-element.15.s3_ref), channel_id=1, source_target_pairs={{0,32},{8,40},{16,48},{24,56},{32,64},{40,72},{48,80},{56,88},{64,... | collective-permute-start | bytes 294920 | tf_op jit(solution)/shard_map/ppermute | solution.py:311
  28.8 1.9 %collective-permute-start.2 = (bf16[384,128]{1,0:T(8,128)(2,1)S(1)}, bf16[384,128]{1,0:T(8,128)(2,1)S(1)}, u32[]{:S(2)}, u32[]{:S(2)}) collective-permute-start(bf16[384,128]{1,0:T(8,128)(2,1)S(1)} %get-tuple-element.15.s3_ref), channel_id=1, source_target_pairs={{0,24},{8,32},{16,40},{24,48},{32,56},{40,64},{48,72},{56,80},{64,... | collective-permute-start | bytes 294920 | tf_op jit(solution)/shard_map/ppermute | solution.py:311
  30.8 0.0 copy-start.3
  30.8 0.0 copy-done
  30.8 1.0 %shard_map.78.q_ref = bf16[384,192]{1,0:T(8,128)(2,1)S(1)} custom-call(bf16[384,2048]{1,0:T(8,128)(2,1)S(1)} %get-tuple-element.14.normed_ref, bf16[3,64,2048]{2,1,0:T(8,128)(2,1)S(1)} %copy-done), custom_call_target="tpu_custom_call" | custom-call | tf_op jit(solution)/shard_map/pallas_call | solution.py:295
  31.8 0.0 collective-permute-done.3.r4_ref
  31.8 4.5 %collective-permute-done.2.r3_ref = bf16[384,128]{1,0:T(8,128)(2,1)S(1)} collective-permute-done((bf16[384,128]{1,0:T(8,128)(2,1)S(1)}, bf16[384,128]{1,0:T(8,128)(2,1)S(1)}, u32[]{:S(2)}, u32[]{:S(2)}) %collective-permute-start.2) | collective-permute-done | bytes 98336 | tf_op jit(solution)/shard_map/ppermute | solution.py:311
  36.2 0.0 copy-done.3
  36.2 2.6 %shard_map.80 = (f32[384,64]{1,0:T(8,128)S(1)}, f32[384,1]{1,0:T(8,128)S(1)}, f32[384,480]{1,0:T(8,128)S(1)}, f32[384,1]{1,0:T(8,128)S(1)}, f32[384,1]{1,0:T(8,128)S(1)}) custom-call(s32[1]{0:T(128)} %bitcast.sp_ref, s32[1]{0:T(128)} %bitcast.1.slot_ref, bf16[384,192]{1,0:T(8,128)(2,1)S(1)} %shard_map.78.q_ref, bf16[384,128]{1,0:T(8,128)(2,1)S(1)} %copy-done.3, ...), custom_call_target="tpu_custom_call" | custom-call | tf_op jit(solution)/shard_map/pallas_call | solution.py:295
  38.9 0.0 collective-permute-done.4.far_ref
  38.9 0.0 copy-start.1
  38.9 1.0 %shard_map.81 = (bf16[8,64,384]{2,1,0:T(8,128)(2,1)S(1)}, f32[384,1]{1,0:T(8,128)S(1)}) custom-call(s32[1]{0:T(128)} %bitcast.sp_ref, s32[1]{0:T(128)} %bitcast.1.slot_ref, bf16[384,192]{1,0:T(8,128)(2,1)S(1)} %shard_map.78.q_ref, bf16[384,128]{1,0:T(8,128)(2,1)S(1)} %get-tuple-element.15.s3_ref, bf16[896,128]{1,0:T(8,128)(2,1)S(1)} %collective-permute-done.r1_ref, ...), custom_call_target="tpu_custom_call" | custom-call | tf_op jit(solution)/shard_map/pallas_call | solution.py:295
  39.9 13.0 %all_to_all.5.mix_ref = bf16[8,64,384]{2,1,0:T(8,128)(2,1)S(1)} all-to-all(bf16[8,64,384]{2,1,0:T(8,128)(2,1)S(1)} %get-tuple-element.24), channel_id=1, replica_groups=mesh['sp'=128,'tp'=8] {'tp'}, dimensions={0} | all-to-all | bytes 786432 | tf_op jit(solution)/shard_map/all_to_all | solution.py:357
  53.0 0.0 copy-done.1
  53.0 1.0 %shard_map.82 = (bf16[384,256]{1,0:T(8,128)(2,1)}, f32[1,384]{1,0:T(1,128)}) custom-call(bf16[8,64,384]{2,1,0:T(8,128)(2,1)S(1)} %all_to_all.5.mix_ref, bf16[512,256]{1,0:T(8,128)(2,1)S(1)} %copy-done.1, f32[384,1]{1,0:T(8,128)S(1)} %get-tuple-element.25.lw_ref), custom_call_target="tpu_custom_call" | custom-call | tf_op jit(solution)/shard_map/pallas_call | solution.py:295
  (1 shorter events, 0.0 us)
Async XLA Ops:
  0.6 30.2 %copy-start = (bf16[3,64,2048]{2,1,0:T(8,128)(2,1)S(1)}, bf16[3,64,2048]{2,1,0:T(8,128)(2,1)}, u32[]{:S(2)}) copy-start(bf16[3,64,2048]{2,1,0:T(8,128)(2,1)} %wq_ref.1) | copy-start | bytes 2359300
  3.9 0.6 %copy-start.2 = (bf16[384,128]{1,0:T(8,128)(2,1)}, bf16[384,128]{1,0:T(8,128)(2,1)S(1)}, u32[]{:S(2)}) copy-start(bf16[384,128]{1,0:T(8,128)(2,1)S(1)} %get-tuple-element.18.kv0_ref) | copy-start | bytes 294916
  4.6 14.2 %collective-permute-start = (bf16[896,128]{1,0:T(8,128)(2,1)S(1)}, bf16[896,128]{1,0:T(8,128)(2,1)S(1)}, u32[]{:S(2)}, u32[]{:S(2)}) collective-permute-start(bf16[896,128]{1,0:T(8,128)(2,1)S(1)} %get-tuple-element.16.s1_ref), channel_id=1, source_target_pairs={{0,8},{8,16},{16,24},{24,32},{32,40},{40,48},{48,56},{56,64},{64,7... | collective-permute-start | bytes 688136 | tf_op jit(solution)/shard_map/ppermute | solution.py:311
  8.1 10.7 %collective-permute-start.1 = (bf16[512,128]{1,0:T(8,128)(2,1)S(1)}, bf16[512,128]{1,0:T(8,128)(2,1)S(1)}, u32[]{:S(2)}, u32[]{:S(2)}) collective-permute-start(bf16[512,128]{1,0:T(8,128)(2,1)S(1)} %get-tuple-element.17), channel_id=1, source_target_pairs={{0,16},{8,24},{16,32},{24,40},{32,48},{40,56},{48,64},{56,72},{64,... | collective-permute-start | bytes 393224 | tf_op jit(solution)/shard_map/ppermute | solution.py:311
  18.7 20.1 %collective-permute-start.4 = (bf16[512,128]{1,0:T(8,128)(2,1)S(1)}, bf16[512,128]{1,0:T(8,128)(2,1)S(1)}, u32[]{:S(2)}, u32[]{:S(2)}) collective-permute-start(bf16[512,128]{1,0:T(8,128)(2,1)S(1)} %shard_map.79), channel_id=1, source_target_pairs={{0,32},{8,40},{16,48},{24,56},{32,64},{40,72},{48,80},{56,88},{64,... | collective-permute-start | bytes 393224 | tf_op jit(solution)/shard_map/ppermute | solution.py:311
  22.6 9.2 %collective-permute-start.3 = (bf16[384,128]{1,0:T(8,128)(2,1)S(1)}, bf16[384,128]{1,0:T(8,128)(2,1)S(1)}, u32[]{:S(2)}, u32[]{:S(2)}) collective-permute-start(bf16[384,128]{1,0:T(8,128)(2,1)S(1)} %get-tuple-element.15.s3_ref), channel_id=1, source_target_pairs={{0,32},{8,40},{16,48},{24,56},{32,64},{40,72},{48,80},{56,88},{64,... | collective-permute-start | bytes 294920 | tf_op jit(solution)/shard_map/ppermute | solution.py:311
  28.8 7.4 %collective-permute-start.2 = (bf16[384,128]{1,0:T(8,128)(2,1)S(1)}, bf16[384,128]{1,0:T(8,128)(2,1)S(1)}, u32[]{:S(2)}, u32[]{:S(2)}) collective-permute-start(bf16[384,128]{1,0:T(8,128)(2,1)S(1)} %get-tuple-element.15.s3_ref), channel_id=1, source_target_pairs={{0,24},{8,32},{16,40},{24,48},{32,56},{40,64},{48,72},{56,80},{64,... | collective-permute-start | bytes 294920 | tf_op jit(solution)/shard_map/ppermute | solution.py:311
  30.8 5.5 %copy-start.3 = (bf16[384,128]{1,0:T(8,128)(2,1)S(1)}, bf16[384,128]{1,0:T(8,128)(2,1)}, u32[]{:S(2)}) copy-start(bf16[384,128]{1,0:T(8,128)(2,1)} %copy-done.2) | copy-start | bytes 294916
  38.9 14.1 %copy-start.1 = (bf16[512,256]{1,0:T(8,128)(2,1)S(1)}, bf16[512,256]{1,0:T(8,128)(2,1)}, u32[]{:S(2)}) copy-start(bf16[512,256]{1,0:T(8,128)(2,1)} %w_ref.1) | copy-start | bytes 786436

commit v11 on v9

--- a/solution.py
+++ b/solution.py
@@ -123,9 +123,11 @@
     return jnp.exp2(-8.0 * n.astype(jnp.float32) / (GROUPS * SLOTS))
 
 
-def bias_of(distance, valid, slope):
-    ok = valid & (distance >= 0) & (distance <= STEPS)
-    return jnp.where(ok, -slope * distance.astype(jnp.float32), NEG_BIG)
+def bias_of(at_query, at_key, valid, slope, same=None):
+    at_key = jnp.where(valid, at_key.astype(jnp.float32), 1e9)
+    distance = at_query.astype(jnp.float32) - at_key
+    ok = jnp.abs(distance - STEPS / 2) <= STEPS / 2
+    return jnp.where(ok if same is None else ok & same, -slope * distance, NEG_BIG)
 
 
 def softmax_pieces(scores):
@@ -151,7 +153,7 @@
         ok.append(jnp.full_like(jh, halo_block) <= sp)
     js, at = jnp.concatenate(js, axis=1), jnp.concatenate(at, axis=1)
     ok = jnp.concatenate([o.astype(jnp.int32) for o in ok], axis=1) > 0
-    return bias_of(iq - at, (jq == js) & ok, slope)
+    return bias_of(iq, at, ok, slope, jq == js)
 
 
 def early_kernel(
@@ -164,7 +166,7 @@
     jh, ih = run_of_halo(per_residue, 1)
     tail = jnp.concatenate([16 * ih + 4 * jh + c - rows for c in range(CLASSES)], axis=1)
     tk = jnp.concatenate([positions(rows, 1), tail], axis=1)
-    bias = bias_of(positions(rows, 0) - tk, (tk >= 0) | (sp >= 1), slope_of(0, slot))
+    bias = bias_of(positions(rows, 0), tk, (tk >= 0) | (sp >= 1), slope_of(0, slot))
     keys = jnp.concatenate([kv0_ref[...], r1_ref[0:STEPS, :]], axis=0)
     p, l0 = softmax_pieces(dot(q_ref[:, 0:HEAD_DIM], keys[:, 0:HEAD_DIM], NT) + bias)
     o0 = dot(p, keys[:, HEAD_DIM:PAIR], NN)
@@ -173,7 +175,7 @@
     own = 4 * ik + jk
     tk = jnp.concatenate([own, own - per_class, 4 * ih + jh - 2 * per_class], axis=1)
     block = jnp.concatenate([jnp.zeros_like(own), jnp.full_like(own, 1), jnp.full_like(jh, 2)], axis=1)
-    bias = bias_of(4 * iq + jq - tk, block <= sp, slope_of(1, slot))
+    bias = bias_of(4 * iq + jq, tk, block <= sp, slope_of(1, slot))
     halo = STEPS // CLASSES
     keys = [
         jnp.concatenate(

time: 50.4 us -> 50.5 us (level)
  no operation moved by 1% of the time
where the time goes in v11:
time: 50.5 us; the launch traced here: 50.3 us
  waiting for transfers between devices  14.1 us (28%)
  blocking collectives  13 us (26%)
  starting transfers between devices  12.8 us (25%)
  Pallas kernels  9.63 us (19%)
  between operations  0.72 us (1%)
    ppermute x4, waiting for transfers between devices, from_behind(): return lax.ppermute(value, 'sp', [(i, i + by) for i in range(devices - by)])  14.1 us
    all_to_all x1, blocking collectives, layer(): everyone = lax.all_to_all(mix, 'tp', 0, 0, tiled=True)  13 us
    ppermute x4, starting transfers between devices, from_behind(): return lax.ppermute(value, 'sp', [(i, i + by) for i in range(devices - by)])  12.8 us
    pallas_call x6, Pallas kernels, call(): pl.pallas_call(body, in_specs=specs or [VMEM] * len(operands), out_specs=...  9.63 us
  transfers between devices with their start and end apart: 4, of which 2 were waited for; matrix products, arithmetic and copies ran while one was open for 0% of the time, Pallas kernels for 7%

profile of v11, /device:TPU:896, one launch (start us, length us, event | category | flops | bytes accessed | tf_op | source)
XLA Modules:
  0.0 50.3 jit_solution(18345161066206450668)
XLA Ops:
  0.6 0.0 copy-start
  0.6 3.3 %shard_map.77 = (bf16[384,128]{1,0:T(8,128)(2,1)S(1)}, bf16[896,128]{1,0:T(8,128)(2,1)S(1)}, bf16[512,128]{1,0:T(8,128)(2,1)S(1)}, bf16[384,128]{1,0:T(8,128)(2,1)S(1)}, bf16[384,2048]{1,0:T(8,128)(2,1)S(1)}) custom-call(bf16[384,2048]{1,0:T(8,128)(2,1)} %tokens_hbm.1, f32[1,2048]{1,0:T(1,128)} %bitcast.3, bf16[3,64,2048]{2,1,0:T(8,128)(2,1)} %wk_hbm.1, ...), custom_call_target="tpu_custom_call" | custom-call | tf_op jit(solution)/shard_map/pallas_call | solution.py:291
  3.9 3.5 %collective-permute-start = (bf16[896,128]{1,0:T(8,128)(2,1)S(1)}, bf16[896,128]{1,0:T(8,128)(2,1)S(1)}, u32[]{:S(2)}, u32[]{:S(2)}) collective-permute-start(bf16[896,128]{1,0:T(8,128)(2,1)S(1)} %get-tuple-element.16.s1_ref), channel_id=1, source_target_pairs={{0,8},{8,16},{16,24},{24,32},{32,40},{40,48},{48,56},{56,64},{64,7... | collective-permute-start | bytes 688136 | tf_op jit(solution)/shard_map/ppermute | solution.py:307
  7.4 4.8 %collective-permute-start.1 = (bf16[512,128]{1,0:T(8,128)(2,1)S(1)}, bf16[512,128]{1,0:T(8,128)(2,1)S(1)}, u32[]{:S(2)}, u32[]{:S(2)}) collective-permute-start(bf16[512,128]{1,0:T(8,128)(2,1)S(1)} %get-tuple-element.17), channel_id=1, source_target_pairs={{0,16},{8,24},{16,32},{24,40},{32,48},{40,56},{48,64},{56,72},{64,... | collective-permute-start | bytes 393224 | tf_op jit(solution)/shard_map/ppermute | solution.py:307
  12.3 7.1 %collective-permute-done.1.r2_ref = bf16[512,128]{1,0:T(8,128)(2,1)S(1)} collective-permute-done((bf16[512,128]{1,0:T(8,128)(2,1)S(1)}, bf16[512,128]{1,0:T(8,128)(2,1)S(1)}, u32[]{:S(2)}, u32[]{:S(2)}) %collective-permute-start.1) | collective-permute-done | bytes 131104 | tf_op jit(solution)/shard_map/ppermute | solution.py:307
  19.3 0.0 collective-permute-done.r1_ref
  19.3 0.7 %shard_map.79 = bf16[896,128]{1,0:T(8,128)(2,1)} custom-call(bf16[384,128]{1,0:T(8,128)(2,1)S(1)} %get-tuple-element.15.s3_ref, bf16[896,128]{1,0:T(8,128)(2,1)S(1)} %collective-permute-done.r1_ref, bf16[512,128]{1,0:T(8,128)(2,1)S(1)} %collective-permute-done.1.r2_ref), custom_call_target="tpu_custom_call" | custom-call | tf_op jit(solution)/shard_map/pallas_call | solution.py:291
  20.0 1.9 %collective-permute-start.3 = (bf16[896,128]{1,0:T(8,128)(2,1)}, bf16[896,128]{1,0:T(8,128)(2,1)S(1)}, u32[]{:S(2)}, u32[]{:S(2)}) collective-permute-start(bf16[896,128]{1,0:T(8,128)(2,1)} %shard_map.79), channel_id=1, source_target_pairs={{0,32},{8,40},{16,48},{24,56},{32,64},{40,72},{48,80},{56,88},{64,... | collective-permute-start | bytes 688136 | tf_op jit(solution)/shard_map/ppermute | solution.py:307
  21.9 2.6 %collective-permute-start.2 = (bf16[384,128]{1,0:T(8,128)(2,1)S(1)}, bf16[384,128]{1,0:T(8,128)(2,1)S(1)}, u32[]{:S(2)}, u32[]{:S(2)}) collective-permute-start(bf16[384,128]{1,0:T(8,128)(2,1)S(1)} %get-tuple-element.15.s3_ref), channel_id=1, source_target_pairs={{0,24},{8,32},{16,40},{24,48},{32,56},{40,64},{48,72},{56,80},{64,... | collective-permute-start | bytes 294920 | tf_op jit(solution)/shard_map/ppermute | solution.py:307
  24.5 0.0 copy-done
  24.6 1.0 %shard_map.78.q_ref = bf16[384,192]{1,0:T(8,128)(2,1)S(1)} custom-call(bf16[384,2048]{1,0:T(8,128)(2,1)S(1)} %get-tuple-element.14.normed_ref, bf16[3,64,2048]{2,1,0:T(8,128)(2,1)S(1)} %copy-done), custom_call_target="tpu_custom_call" | custom-call | tf_op jit(solution)/shard_map/pallas_call | solution.py:291
  25.5 7.1 %collective-permute-done.2.r3_ref = bf16[384,128]{1,0:T(8,128)(2,1)S(1)} collective-permute-done((bf16[384,128]{1,0:T(8,128)(2,1)S(1)}, bf16[384,128]{1,0:T(8,128)(2,1)S(1)}, u32[]{:S(2)}, u32[]{:S(2)}) %collective-permute-start.2) | collective-permute-done | bytes 98336 | tf_op jit(solution)/shard_map/ppermute | solution.py:307
  32.6 2.5 %shard_map.80 = (f32[384,64]{1,0:T(8,128)S(1)}, f32[384,1]{1,0:T(8,128)S(1)}, f32[384,384]{1,0:T(8,128)S(1)}, f32[384,1]{1,0:T(8,128)S(1)}, f32[384,1]{1,0:T(8,128)S(1)}) custom-call(s32[1]{0:T(128)} %bitcast.sp_ref, s32[1]{0:T(128)} %bitcast.1.slot_ref, bf16[384,192]{1,0:T(8,128)(2,1)S(1)} %shard_map.78.q_ref, ...), custom_call_target="tpu_custom_call" | custom-call | tf_op jit(solution)/shard_map/pallas_call | solution.py:291
  35.1 0.0 collective-permute-done.3.r4_ref
  35.1 0.0 copy-start.1
  35.1 1.1 %shard_map.81 = (bf16[8,64,384]{2,1,0:T(8,128)(2,1)S(1)}, f32[384,1]{1,0:T(8,128)S(1)}) custom-call(s32[1]{0:T(128)} %bitcast.sp_ref, s32[1]{0:T(128)} %bitcast.1.slot_ref, bf16[384,192]{1,0:T(8,128)(2,1)S(1)} %shard_map.78.q_ref, bf16[384,128]{1,0:T(8,128)(2,1)S(1)} %get-tuple-element.15.s3_ref, bf16[896,128]{1,0:T(8,128)(2,1)S(1)} %collective-permute-done.r1_ref, ...), custom_call_target="tpu_custom_call" | custom-call | tf_op jit(solution)/shard_map/pallas_call | solution.py:291
  36.3 13.0 %all_to_all.5.mix_ref = bf16[8,64,384]{2,1,0:T(8,128)(2,1)S(1)} all-to-all(bf16[8,64,384]{2,1,0:T(8,128)(2,1)S(1)} %get-tuple-element.24), channel_id=1, replica_groups=mesh['sp'=128,'tp'=8] {'tp'}, dimensions={0} | all-to-all | bytes 786432 | tf_op jit(solution)/shard_map/all_to_all | solution.py:352
  49.3 0.0 copy-done.1
  49.3 1.0 %shard_map.82 = (bf16[384,256]{1,0:T(8,128)(2,1)}, f32[1,384]{1,0:T(1,128)}) custom-call(bf16[8,64,384]{2,1,0:T(8,128)(2,1)S(1)} %all_to_all.5.mix_ref, bf16[512,256]{1,0:T(8,128)(2,1)S(1)} %copy-done.1, f32[384,1]{1,0:T(8,128)S(1)} %get-tuple-element.25.lw_ref), custom_call_target="tpu_custom_call" | custom-call | tf_op jit(solution)/shard_map/pallas_call | solution.py:291
Async XLA Ops:
  0.6 23.9 %copy-start = (bf16[3,64,2048]{2,1,0:T(8,128)(2,1)S(1)}, bf16[3,64,2048]{2,1,0:T(8,128)(2,1)}, u32[]{:S(2)}) copy-start(bf16[3,64,2048]{2,1,0:T(8,128)(2,1)} %wq_ref.1) | copy-start | bytes 2359300
  3.9 15.4 %collective-permute-start = (bf16[896,128]{1,0:T(8,128)(2,1)S(1)}, bf16[896,128]{1,0:T(8,128)(2,1)S(1)}, u32[]{:S(2)}, u32[]{:S(2)}) collective-permute-start(bf16[896,128]{1,0:T(8,128)(2,1)S(1)} %get-tuple-element.16.s1_ref), channel_id=1, source_target_pairs={{0,8},{8,16},{16,24},{24,32},{32,40},{40,48},{48,56},{56,64},{64,7... | collective-permute-start | bytes 688136 | tf_op jit(solution)/shard_map/ppermute | solution.py:307
  7.4 11.9 %collective-permute-start.1 = (bf16[512,128]{1,0:T(8,128)(2,1)S(1)}, bf16[512,128]{1,0:T(8,128)(2,1)S(1)}, u32[]{:S(2)}, u32[]{:S(2)}) collective-permute-start(bf16[512,128]{1,0:T(8,128)(2,1)S(1)} %get-tuple-element.17), channel_id=1, source_target_pairs={{0,16},{8,24},{16,32},{24,40},{32,48},{40,56},{48,64},{56,72},{64,... | collective-permute-start | bytes 393224 | tf_op jit(solution)/shard_map/ppermute | solution.py:307
  20.0 15.1 %collective-permute-start.3 = (bf16[896,128]{1,0:T(8,128)(2,1)}, bf16[896,128]{1,0:T(8,128)(2,1)S(1)}, u32[]{:S(2)}, u32[]{:S(2)}) collective-permute-start(bf16[896,128]{1,0:T(8,128)(2,1)} %shard_map.79), channel_id=1, source_target_pairs={{0,32},{8,40},{16,48},{24,56},{32,64},{40,72},{48,80},{56,88},{64,... | collective-permute-start | bytes 688136 | tf_op jit(solution)/shard_map/ppermute | solution.py:307
  21.9 10.7 %collective-permute-start.2 = (bf16[384,128]{1,0:T(8,128)(2,1)S(1)}, bf16[384,128]{1,0:T(8,128)(2,1)S(1)}, u32[]{:S(2)}, u32[]{:S(2)}) collective-permute-start(bf16[384,128]{1,0:T(8,128)(2,1)S(1)} %get-tuple-element.15.s3_ref), channel_id=1, source_target_pairs={{0,24},{8,32},{16,40},{24,48},{32,56},{40,64},{48,72},{56,80},{64,... | collective-permute-start | bytes 294920 | tf_op jit(solution)/shard_map/ppermute | solution.py:307
  35.1 14.2 %copy-start.1 = (bf16[512,256]{1,0:T(8,128)(2,1)S(1)}, bf16[512,256]{1,0:T(8,128)(2,1)}, u32[]{:S(2)}) copy-start(bf16[512,256]{1,0:T(8,128)(2,1)} %w_ref.1) | copy-start | bytes 786436
